TPU v7x, 32 devices: a whole 2x2x4 slice. The times are simulated.
32 devices in a mesh: dp: 4 (over y, x), kv: 4 (over z), tp: 2 (over core).
Axes of the slice: x: 2, y: 2, z: 4, core: 2. Of those that a mesh axis runs over, the one named last changes fastest.
Arguments:
- resid: bfloat16 [16, 2048], P('dp', ('kv', 'tp')), may hold values from -45 to 45
- norm_gain: bfloat16 [3, 2048], P(None, ('kv', 'tp')), may hold values from 0.099609375 to 1.8984375
- ffn_gate: bfloat16 [2, 2048, 5632], P(None, None, ('kv', 'tp')), may hold values from -0.125 to 0.125
- ffn_up: bfloat16 [2, 2048, 5632], P(None, None, ('kv', 'tp')), may hold values from -0.125 to 0.125
- ffn_down: bfloat16 [2, 5632, 2048], P(None, ('kv', 'tp')), may hold values from -0.109375 to 0.109375
- w_x: bfloat16 [2048, 64, 64], P(None, 'kv', 'tp'), may hold values from -0.125 to 0.125
- w_z: bfloat16 [2048, 64, 64], P(None, 'kv', 'tp'), may hold values from -0.125 to 0.125
- w_bc: bfloat16 [2048, 2, 8, 128], P('kv'), may hold values from -0.125 to 0.125
- w_dt: bfloat16 [2048, 64], P('kv'), may hold values from -0.125 to 0.125
- dt_bias: float32 [64], replicated, may hold values from -2 to 0.5
- a_log: float32 [64], replicated, may hold values from -1.5 to 1.5
- d_skip: float32 [64], replicated, may hold values from 0.5 to 1.5
- conv_wx: bfloat16 [4, 64, 64], P(None, None, 'tp'), may hold values from -3 to 3
- conv_wbc: bfloat16 [4, 2, 8, 128], replicated, may hold values from -3 to 3
- conv_x: bfloat16 [16, 3, 64, 64], P(('dp', 'kv'), None, None, 'tp'), may hold values from -6 to 6
- conv_bc: bfloat16 [16, 3, 2, 8, 128], P(('dp', 'kv')), may hold values from -6 to 6
- ssm_state: float32 [16, 64, 64, 128], P(('dp', 'kv'), None, 'tp'), may hold values from -3 to 3
- w_out: bfloat16 [64, 64, 2048], P(None, 'tp', 'kv'), may hold values from -0.09375 to 0.09375
Outputs:
- final: bfloat16 [16, 2048], P('dp', ('kv', 'tp'))
All inputs are finite; a program needn't handle non-finite values.
Results may differ from a plain program's by a relative error of at most 0.018.
Values may be sent and summed in bfloat16 or wider, within the bound.
No kernel may reach another device: no remote copies, remote signals or barrier semaphores. Data moves between devices by JAX's collectives and lax.ppermute only.
A program may use at most 64 MiB of HBM per device.

v0:
```python
import functools

import jax
import jax.numpy as jnp
from jax import lax
from jax.experimental import pallas as pl
from jax.experimental.pallas import tpu as pltpu
from jax.sharding import PartitionSpec as P


EPS = 1e-06
F32 = jnp.float32
BF16 = jnp.bfloat16
NT = (((1,), (1,)), ((), ()))
ANY = pl.BlockSpec(memory_space=pl.ANY)
VMEM = pl.BlockSpec(memory_space=pltpu.VMEM)


def dot_nt(left, right):
    return lax.dot_general(left, right, NT, preferred_element_type=F32)


def dot_nn(left, right):
    return jnp.dot(left, right, preferred_element_type=F32)


def silu(value):
    return value * jax.nn.sigmoid(value)


def swap_kv(values):
    kv = len(values)
    got = list(values)
    for d in reversed(range(1, kv)):
        got[d] = lax.ppermute(values[d], "kv", [(i, i ^ d) for i in range(kv)])
    return got


def share_kv(value, kv):
    return swap_kv([value] * kv)


def swap_tp(value):
    return lax.ppermute(value, "tp", [(0, 1), (1, 0)])


def in_vmem(value):
    return pltpu.with_memory_space_constraint(value, pltpu.VMEM)


def run(body, outs, args, scratch=(), limit=16, in_specs=None, flops=10**10):
    return pl.pallas_call(
        body,
        out_shape=outs,
        in_specs=in_specs or [VMEM] * len(args),
        out_specs=jax.tree.map(lambda _: VMEM, outs),
        scratch_shapes=list(scratch),
        compiler_params=pltpu.CompilerParams(vmem_limit_bytes=limit * 2**20),
        cost_estimate=pl.CostEstimate(flops=flops, bytes_accessed=0, transcendentals=0),
    )(*args)


def f32(*shape):
    return jax.ShapeDtypeStruct(shape, F32)


def bf16(*shape):
    return jax.ShapeDtypeStruct(shape, BF16)


def split_body(state, high_out, low_out):
    values = state[...]
    high = values.astype(BF16)
    high_out[...] = high
    low_out[...] = (values - high.astype(F32)).astype(BF16)


def normed_rows(values, gain):
    scale = lax.rsqrt(jnp.mean(values * values, axis=1, keepdims=True) + EPS)
    return (values * scale * gain).astype(BF16)


def feed(normed, layer, gate, up, down):
    hidden = (silu(dot_nt(normed, gate[layer])) * dot_nt(normed, up[layer])).astype(BF16)
    return dot_nn(hidden, down[layer])


def pack_body(rows, gains, out):
    seqs = rows.shape[0]
    out[:seqs] = rows[...]
    out[seqs : seqs + gains.shape[0]] = gains[...]
    out[seqs + gains.shape[0] :] = gains[:1]


def first_body(kv, seqs, own, other, gate, up, down, sums_out, rows_out, slabs):
    here, side = lax.axis_index("kv"), lax.axis_index("tp")
    width = slabs.shape[2]
    for d in range(kv):
        peer = jnp.bitwise_xor(here, d)
        slabs[2 * peer + side] = own[:, d * width : (d + 1) * width]
        slabs[2 * peer + 1 - side] = other[:, d * width : (d + 1) * width]
    rows = jnp.concatenate([slabs[i] for i in range(slabs.shape[0])], axis=1)
    rows_out[...] = rows
    values = rows.astype(F32)
    sums = feed(normed_rows(values, values[seqs : seqs + 1]), 0, gate, up, down)
    sums_out[...] = sums[:seqs]


def mix_in_body(kv, seqs, s0, s1, s2, s3, rows, w_x, w_z, w_bc, w_dt, *rest):
    pays, (first_out, slabs, firsts, table) = rest[:kv], rest[kv:]
    here = lax.axis_index("kv")
    span = slabs.shape[2]
    total = s0[...].astype(F32) + s1[...].astype(F32) + s2[...].astype(F32) + s3[...].astype(F32)
    known = rows[...].astype(F32)
    first = (known[:seqs] + 0.5 * total).astype(BF16).astype(F32)
    padded = jnp.concatenate([first, first], axis=0)
    normed = normed_rows(padded, known[seqs + 1 : seqs + 2])
    for i in range(kv):
        slabs[i] = normed[:, i * span : (i + 1) * span].astype(F32)
        firsts[i] = padded[:, i * span : (i + 1) * span]
    slab = slabs[here].astype(BF16)
    first_out[...] = firsts[here][:seqs]
    xs = dot_nt(normed, w_x[...]).astype(BF16).astype(F32)
    zeta = dot_nt(normed, w_z[...]).astype(BF16).astype(F32)
    bc = dot_nn(slab, w_bc[...])
    dt = dot_nt(slab, w_dt[...])
    width = xs.shape[1]
    a = 2 * width
    b = a + bc.shape[1]
    table[:, :width] = xs
    table[:, width:a] = zeta
    table[:, a:b] = bc
    table[:, b : b + dt.shape[1]] = dt
    for d in range(kv):
        pays[d][...] = table[pl.ds(jnp.bitwise_xor(here, d), 1), :]


def state_body(kv, p0, p1, p2, p3, high, low, taps_x, past_x, taps_bc, past_bc, bias, a_log, d_skip, out, x_held, z_held, bc_held):
    here = lax.axis_index("kv")
    groups, wide = x_held.shape
    states = bc_held.shape[1]
    heads = bias.shape[1]
    pieces = (p0, p1, p2, p3)
    per = groups // kv
    width = per * wide
    for d, piece in enumerate(pieces):
        peer = jnp.bitwise_xor(here, d)
        for i in range(per):
            x_held[pl.ds(per * peer + i, 1), :] = piece[:, i * wide : (i + 1) * wide]
            z_held[pl.ds(per * peer + i, 1), :] = piece[:, width + i * wide : width + (i + 1) * wide]
    a = 2 * width
    for j in range(2 * groups):
        at = a + j * states
        bc_held[j : j + 1, :] = sum(piece[:, at : at + states] for piece in pieces)
    b = a + 2 * groups * states
    dt = sum(piece[:, b : b + heads] for piece in pieces) + bias[...]
    newest = bc_held[...].astype(BF16).astype(F32)
    steps = taps_bc.shape[0]
    mapped = newest * taps_bc[steps - 1].astype(F32)
    for k in range(steps - 1):
        mapped += past_bc[k].astype(F32) * taps_bc[k].astype(F32)
    mapped = silu(mapped)
    b_map, c_map = mapped[:groups], mapped[groups:]
    xconv = x_held[...] * taps_x[steps - 1].astype(F32)
    for k in range(steps - 1):
        xconv += past_x[k].astype(F32) * taps_x[k].astype(F32)
    xconv = silu(xconv)
    share = heads // groups
    own_group = lax.broadcasted_iota(jnp.int32, (groups, heads), 1) // share == lax.broadcasted_iota(
        jnp.int32, (groups, heads), 0
    )
    spread = (
        lax.broadcasted_iota(jnp.int32, (heads, wide), 0) % share
        == lax.broadcasted_iota(jnp.int32, (heads, wide), 1) // (wide // share)
    ).astype(F32)
    table = jnp.concatenate(
        [
            jnp.where(own_group, jnp.broadcast_to(v, (groups, heads)), 0.0)
            for v in (dt, a_log[...], d_skip[...])
        ],
        axis=0,
    )
    table = jnp.dot(table, spread, precision=lax.Precision.HIGHEST, preferred_element_type=F32)
    step = jax.nn.softplus(table[:groups])
    decay = jnp.exp(-step * jnp.exp(table[groups : 2 * groups]))
    skip = table[2 * groups :]
    c_high = c_map.astype(BF16)
    c_low = (c_map - c_high.astype(F32)).astype(BF16)
    read = dot_nt(c_high, high[...]) + dot_nt(c_low, high[...]) + dot_nt(c_high, low[...])
    read = jnp.concatenate(
        [read[g : g + 1, g * wide : (g + 1) * wide] for g in range(groups)], axis=0
    )
    inner = jnp.sum(b_map * c_map, axis=1, keepdims=True)
    mixed = (decay * read + xconv * (step * inner + skip)) * silu(z_held[...])
    mixed = mixed.astype(BF16).astype(F32)
    for g in range(groups):
        out[:, g * wide : (g + 1) * wide] = mixed[g : g + 1]


def mix_out_body(seqs, tp, m0, m1, m2, m3, w_out, first, out, table):
    here = lax.axis_index("kv")
    table[...] = jnp.zeros_like(table)
    for d, piece in enumerate((m0, m1, m2, m3)):
        table[pl.ds(jnp.bitwise_xor(here, d), 1), :] = piece[...]
    sums = dot_nn(table[...].astype(BF16), w_out[...])
    out[...] = sums[:seqs] + first[...] * (1.0 / tp)


def second_body(kv, seqs, s0, s1, s2, s3, rows, gate, up, down, *rest):
    outs, (own_out, slabs, sums_held) = rest[:kv], rest[kv:]
    here = lax.axis_index("kv")
    span = slabs.shape[2]
    for d, piece in enumerate((s0, s1, s2, s3)):
        slabs[jnp.bitwise_xor(here, d)] = piece[...].astype(F32)
    second = jnp.concatenate([slabs[i] for i in range(kv)], axis=1)
    padded = jnp.concatenate([second, second], axis=0)
    gain = rows[seqs + 2 : seqs + 3, :].astype(F32)
    sums = feed(normed_rows(padded, gain), 1, gate, up, down)[:seqs]
    for i in range(kv):
        sums_held[i] = sums[:, i * span : (i + 1) * span]
    for d in range(kv):
        outs[d][...] = sums_held[jnp.bitwise_xor(here, d)]
    own_out[...] = s0[...].astype(F32)


def small_mesh(kv, tp, *args):
    return small_step(kv, tp, *args)


def small_step(
    kv,
    tp,
    resid,
    norm_gain,
    ffn_gate,
    ffn_up,
    ffn_down,
    w_x,
    w_z,
    w_bc,
    w_dt,
    dt_bias,
    a_log,
    d_skip,
    conv_wx,
    conv_wbc,
    conv_x,
    conv_bc,
    ssm_state,
    w_out,
):
    seqs, width = resid.shape
    model = width * kv * tp
    span = model // kv
    gate, up = jnp.swapaxes(ffn_gate, 1, 2), jnp.swapaxes(ffn_up, 1, 2)
    heads = dt_bias.shape[0]
    groups, states = w_bc.shape[2:]
    half = w_x.shape[2]
    local = w_x.shape[1] * half
    wide = heads // groups * half
    flat = heads * half

    pack = run(pack_body, bf16(2 * seqs, width), (resid, norm_gain), flops=10**10)
    chip = jnp.concatenate(share_kv(pack, kv), axis=1)
    other = swap_tp(chip)
    weights = tuple(map(in_vmem, (gate, up, ffn_down)))
    sums, rows = run(
        functools.partial(first_body, kv, seqs),
        [f32(seqs, model), bf16(2 * seqs, model)],
        (chip, other, *weights),
        [pltpu.VMEM((kv * tp, 2 * seqs, width), BF16)],
    )
    sums = (sums + swap_tp(sums)).astype(BF16)
    sums = share_kv(sums, kv)

    w_xs, w_zs, w_maps, w_steps, w_join = map(
        in_vmem,
        (
            jnp.transpose(w_x, (1, 2, 0)).reshape(local, model),
            jnp.transpose(w_z, (1, 2, 0)).reshape(local, model),
            w_bc.reshape(span, 2 * groups * states),
            w_dt.T,
            w_out.reshape(flat, span),
        ),
    )
    high, low = run(
        split_body, [bf16(flat, states)] * 2, (in_vmem(ssm_state.reshape(flat, states)),)
    )
    bc_width = 2 * groups * states
    line = 2 * local + bc_width + max(heads, 128)
    *pays, first = run(
        functools.partial(mix_in_body, kv, seqs),
        [f32(1, line)] * kv + [f32(seqs, span)],
        (*sums, rows, w_xs, w_zs, w_maps, w_steps),
        [
            pltpu.VMEM((kv, 2 * seqs, span), F32),
            pltpu.VMEM((kv, 2 * seqs, span), F32),
            pltpu.VMEM((2 * seqs, line), F32),
        ],
    )
    pays = swap_kv(pays)
    mixed = run(
        functools.partial(state_body, kv),
        f32(1, flat),
        (
            *pays,
            high,
            low,
            conv_wx.reshape(-1, groups, wide),
            conv_x.reshape(-1, groups, wide),
            conv_wbc.reshape(-1, 2 * groups, states),
            conv_bc.reshape(-1, 2 * groups, states),
            dt_bias.reshape(1, heads),
            a_log.reshape(1, heads),
            d_skip.reshape(1, heads),
        ),
        [
            pltpu.VMEM((groups, wide), F32),
            pltpu.VMEM((groups, wide), F32),
            pltpu.VMEM((2 * groups, states), F32),
        ],
    )
    mixed = share_kv(mixed, kv)
    joined = run(
        functools.partial(mix_out_body, seqs, tp),
        f32(seqs, span),
        (*mixed, w_join, first),
        [pltpu.VMEM((2 * seqs, flat), F32)],
    )
    second = share_kv((joined + swap_tp(joined)).astype(BF16), kv)
    *sums, own = run(
        functools.partial(second_body, kv, seqs),
        [f32(seqs, span)] * kv + [f32(seqs, span)],
        (*second, rows, *weights),
        [pltpu.VMEM((kv, seqs, span), F32), pltpu.VMEM((kv, seqs, span), F32)],
    )
    total = sum(swap_kv(sums))
    side = lax.axis_index("tp")
    mine = lax.dynamic_slice_in_dim(total, side * width, width, 1)
    theirs = lax.dynamic_slice_in_dim(total, (1 - side) * width, width, 1)
    base = lax.dynamic_slice_in_dim(own, side * width, width, 1)
    return (base + 0.5 * (mine + swap_tp(theirs))).astype(BF16)


def normalize(rows, gain):
    values = rows.astype(jnp.float32)
    scale = lax.rsqrt(jnp.mean(values * values, axis=1, keepdims=True) + EPS)
    return (values * scale * gain.astype(jnp.float32).reshape(1, -1)).astype(jnp.bfloat16)


def feed_forward(normed, w_gate, w_up, w_down):
    gate = jnp.dot(normed, w_gate, preferred_element_type=jnp.float32)
    upper = jnp.dot(normed, w_up, preferred_element_type=jnp.float32)
    hidden = (jax.nn.silu(gate) * upper).astype(jnp.bfloat16)
    return jnp.dot(hidden, w_down, preferred_element_type=jnp.float32)


def add_half(base, sums):
    return (base.astype(jnp.float32) + 0.5 * sums).astype(jnp.bfloat16)


def ffn_totals(partial_value):
    return lax.psum(partial_value, ("kv", "tp"))


def short_conv(history, newest, taps):
    window = jnp.concatenate(
        [history.astype(jnp.float32), newest.astype(jnp.float32)[:, None]], axis=1
    )
    return jax.nn.silu(jnp.sum(window * taps.astype(jnp.float32)[None], axis=1))


def state_step(
    xs_new,
    zeta,
    bc_new,
    dt_raw,
    conv_x,
    conv_bc,
    ssm_state,
    conv_wx,
    conv_wbc,
    dt_bias,
    a_log,
    d_skip,
):
    xconv = short_conv(conv_x, xs_new, conv_wx)
    bconv = short_conv(conv_bc, bc_new, conv_wbc)
    heads = xconv.shape[1]
    groups = bconv.shape[2]
    bmat = jnp.repeat(bconv[:, 0], heads // groups, axis=1)
    cmat = jnp.repeat(bconv[:, 1], heads // groups, axis=1)
    step_size = jax.nn.softplus(dt_raw + dt_bias[None, :])
    decay = jnp.exp(-step_size * jnp.exp(a_log)[None, :])
    updated = (
        decay[:, :, None, None] * ssm_state
        + (step_size[:, :, None] * xconv)[..., None] * bmat[:, :, None, :]
    )
    mixed = (
        jnp.einsum("shpn,shn->shp", updated, cmat, precision=lax.Precision.HIGHEST)
        + d_skip[None, :, None] * xconv
    )
    return (mixed * jax.nn.silu(zeta.astype(jnp.float32))).astype(jnp.bfloat16)


def group_terms(slab, w_bc, w_dt):
    span = slab.shape[1]
    flat_bc = w_bc.reshape(span, -1)
    bc_part = jnp.dot(slab, flat_bc, preferred_element_type=jnp.float32)
    dt_part = jnp.dot(slab, w_dt, preferred_element_type=jnp.float32)
    return (
        lax.psum_scatter(bc_part, "kv", scatter_dimension=0, tiled=True),
        lax.psum_scatter(dt_part, "kv", scatter_dimension=0, tiled=True),
    )


def mix_partial(
    normed,
    w_x,
    w_z,
    w_bc,
    w_dt,
    dt_bias,
    a_log,
    d_skip,
    conv_wx,
    conv_wbc,
    conv_x,
    conv_bc,
    ssm_state,
    w_out,
):
    rows = normed.shape[0]
    local_heads = w_x.shape[1]
    half = w_x.shape[2]
    xs_part = (
        jnp.dot(normed, w_x.reshape(normed.shape[1], -1), preferred_element_type=jnp.float32)
        .astype(jnp.bfloat16)
        .reshape(rows, local_heads, half)
    )
    zeta_part = (
        jnp.dot(normed, w_z.reshape(normed.shape[1], -1), preferred_element_type=jnp.float32)
        .astype(jnp.bfloat16)
        .reshape(rows, local_heads, half)
    )
    xs_new, zeta = (
        lax.all_to_all(xs_part, "kv", split_axis=0, concat_axis=1, tiled=True),
        lax.all_to_all(zeta_part, "kv", split_axis=0, concat_axis=1, tiled=True),
    )
    span = w_bc.shape[0]
    slab = lax.dynamic_slice_in_dim(normed, lax.axis_index("kv") * span, span, 1)
    bc_sum, dt_raw = group_terms(slab, w_bc, w_dt)
    bc_new = bc_sum.astype(jnp.bfloat16).reshape((bc_sum.shape[0],) + w_bc.shape[1:])
    mixed = state_step(
        xs_new,
        zeta,
        bc_new,
        dt_raw,
        conv_x,
        conv_bc,
        ssm_state,
        conv_wx,
        conv_wbc,
        dt_bias,
        a_log,
        d_skip,
    )
    flat_out = w_out.reshape(-1, w_out.shape[2])
    piece = lax.all_gather(mixed, "kv", axis=0, tiled=True)
    return jnp.dot(piece.reshape(piece.shape[0], -1), flat_out, preferred_element_type=jnp.float32)


def per_device(
    resid,
    norm_gain,
    ffn_gate,
    ffn_up,
    ffn_down,
    w_x,
    w_z,
    w_bc,
    w_dt,
    dt_bias,
    a_log,
    d_skip,
    conv_wx,
    conv_wbc,
    conv_x,
    conv_bc,
    ssm_state,
    w_out,
):
    mixer_args = (
        w_x,
        w_z,
        w_bc,
        w_dt,
        dt_bias,
        a_log,
        d_skip,
        conv_wx,
        conv_wbc,
        conv_x,
        conv_bc,
        ssm_state,
        w_out,
    )
    rows, gains = (
        lax.all_gather(resid, ("kv", "tp"), axis=1, tiled=True),
        lax.all_gather(norm_gain, ("kv", "tp"), axis=1, tiled=True),
    )
    first = add_half(
        rows,
        ffn_totals(feed_forward(normalize(rows, gains[0]), ffn_gate[0], ffn_up[0], ffn_down[0])),
    )
    partial_value = mix_partial(normalize(first, gains[1]), *mixer_args)
    span = partial_value.shape[1]
    block = lax.dynamic_slice_in_dim(first, lax.axis_index("kv") * span, span, 1)
    joined = (block.astype(jnp.float32) + lax.psum(partial_value, "tp")).astype(jnp.bfloat16)
    second = lax.all_gather(joined, "kv", axis=1, tiled=True)
    final = add_half(
        second,
        ffn_totals(feed_forward(normalize(second, gains[2]), ffn_gate[1], ffn_up[1], ffn_down[1])),
    )
    width = resid.shape[1]
    return lax.dynamic_slice_in_dim(final, lax.axis_index(("kv", "tp")) * width, width, 1)


def solution(mesh):
    placed = (
        P("dp", ("kv", "tp")),
        P(None, ("kv", "tp")),
        P(None, None, ("kv", "tp")),
        P(None, None, ("kv", "tp")),
        P(None, ("kv", "tp"), None),
        P(None, "kv", "tp"),
        P(None, "kv", "tp"),
        P("kv", None, None, None),
        P("kv", None),
        P(),
        P(),
        P(),
        P(None, None, "tp"),
        P(),
        P(("dp", "kv"), None, None, "tp"),
        P(("dp", "kv"), None, None, None, None),
        P(("dp", "kv"), None, "tp", None),
        P(None, "tp", "kv"),
    )
    kv, tp = mesh.shape["kv"], mesh.shape["tp"]
    small = (kv, tp) == (4, 2)
    return jax.shard_map(
        functools.partial(small_mesh, kv, tp) if small else per_device,
        mesh=mesh,
        in_specs=placed,
        out_specs=P("dp", ("kv", "tp")),
        check_vma=False,
    )
```

profile of v0, /device:TPU:0, one launch (start us, length us, event | category | flops | bytes accessed | tf_op | source)
XLA Modules:
  0.0 63.5 jit_solution(2431367937121131730)
XLA Ops:
  0.0 0.8 %copy-done.10 = bf16[4,256]{1,0:T(4,128)(2,1)S(1)} copy-done((bf16[4,256]{1,0:T(4,128)(2,1)S(1)}, bf16[4,256]{1,0:T(4,128)(2,1)}, u32[]{:S(2)}) %copy-start.10) | copy-done | bytes 2072
  0.8 1.1 %copy-done.11 = bf16[3,256]{1,0:T(4,128)(2,1)S(1)} copy-done((bf16[3,256]{1,0:T(4,128)(2,1)S(1)}, bf16[3,256]{1,0:T(4,128)(2,1)}, u32[]{:S(2)}) %copy-start.11) | copy-done | bytes 1560
  1.9 3.1 %collective-permute-start = (bf16[8,256]{1,0:T(8,128)(2,1)S(1)}, bf16[8,256]{1,0:T(8,128)(2,1)S(1)}, u32[]{:S(2)}, u32[]{:S(2)}) collective-permute-start(bf16[8,256]{1,0:T(8,128)(2,1)S(1)} %shard_map.172), channel_id=1, source_target_pairs={{0,2},{2,0},{4,6},{6,4},{1,3},{3,1},{5,7},{7,5},{8,10},{10,8},{12,... | collective-permute-start | bytes 12296 | tf_op jit(solution)/shard_map/ppermute | solution.py:35
  5.0 2.6 %collective-permute-start.1 = (bf16[8,256]{1,0:T(8,128)(2,1)S(1)}, bf16[8,256]{1,0:T(8,128)(2,1)S(1)}, u32[]{:S(2)}, u32[]{:S(2)}) collective-permute-start(bf16[8,256]{1,0:T(8,128)(2,1)S(1)} %shard_map.172), channel_id=1, source_target_pairs={{0,4},{2,6},{4,0},{6,2},{1,5},{3,7},{5,1},{7,3},{8,12},{10,14},{12... | collective-permute-start | bytes 12296 | tf_op jit(solution)/shard_map/ppermute | solution.py:35
  7.6 1.9 %collective-permute-done.1 = bf16[8,256]{1,0:T(8,128)(2,1)S(1)} collective-permute-done((bf16[8,256]{1,0:T(8,128)(2,1)S(1)}, bf16[8,256]{1,0:T(8,128)(2,1)S(1)}, u32[]{:S(2)}, u32[]{:S(2)}) %collective-permute-start.1) | collective-permute-done | bytes 4128 | tf_op jit(solution)/shard_map/ppermute | solution.py:35
  9.5 3.5 %collective-permute-done.2 = bf16[8,256]{1,0:T(8,128)(2,1)S(1)} collective-permute-done((bf16[8,256]{1,0:T(8,128)(2,1)S(1)}, bf16[8,256]{1,0:T(8,128)(2,1)S(1)}, u32[]{:S(2)}, u32[]{:S(2)}) %collective-permute-start.2) | collective-permute-done | bytes 4128 | tf_op jit(solution)/shard_map/ppermute | solution.py:35
  13.0 1.2 %collective-permute-done.3.other = bf16[8,1024]{1,0:T(8,128)(2,1)S(1)} collective-permute-done((bf16[8,1024]{1,0:T(8,128)(2,1)S(1)}, bf16[8,1024]{1,0:T(8,128)(2,1)S(1)}, u32[]{:S(2)}, u32[]{:S(2)}) %collective-permute-start.3) | collective-permute-done | bytes 16416 | tf_op jit(solution)/shard_map/ppermute | solution.py:44
  14.3 2.1 %shard_map.173 = (f32[4,2048]{1,0:T(4,128)S(1)}, bf16[8,2048]{1,0:T(8,128)(2,1)S(1)}) custom-call(bf16[8,1024]{1,0:T(8,128)(2,1)S(1)} %pad_maximum_fusion.own, bf16[8,1024]{1,0:T(8,128)(2,1)S(1)} %collective-permute-done.3.other, bf16[2,704,2048]{2,1,0:T(8,128)(2,1)S(1)} %bitcast.24, bf16[2,704,2048]{2,1,0:T(8,128)(2,1)S(1)} %bitcast.28, ...), custom_call_target="tpu_custom_call" | custom-call | flops 10000000000 | tf_op jit(solution)/shard_map/pallas_call | solution.py:52
  16.5 1.0 %collective-permute-done.4 = f32[4,2048]{1,0:T(4,128)S(1)} collective-permute-done((f32[4,2048]{1,0:T(4,128)S(1)}, f32[4,2048]{1,0:T(4,128)S(1)}, u32[]{:S(2)}, u32[]{:S(2)}) %collective-permute-start.4) | collective-permute-done | bytes 32800 | tf_op jit(solution)/shard_map/ppermute | solution.py:44
  17.6 0.6 collective-permute-start.6
  18.2 3.8 %collective-permute-start.7 = (bf16[4,2048]{1,0:T(4,128)(2,1)S(1)}, bf16[4,2048]{1,0:T(4,128)(2,1)S(1)}, u32[]{:S(2)}, u32[]{:S(2)}) collective-permute-start(bf16[4,2048]{1,0:T(4,128)(2,1)S(1)} %add_convert_fusion.s0), channel_id=1, source_target_pairs={{0,6},{2,4},{4,2},{6,0},{1,7},{3,5},{5,3},{7,1},{8,14},{10,12},{12... | collective-permute-start | bytes 49160 | tf_op jit(solution)/shard_map/ppermute | solution.py:35
  22.6 1.3 %collective-permute-done.7.s3 = bf16[4,2048]{1,0:T(4,128)(2,1)S(1)} collective-permute-done((bf16[4,2048]{1,0:T(4,128)(2,1)S(1)}, bf16[4,2048]{1,0:T(4,128)(2,1)S(1)}, u32[]{:S(2)}, u32[]{:S(2)}) %collective-permute-start.7) | collective-permute-done | bytes 16416 | tf_op jit(solution)/shard_map/ppermute | solution.py:35
  24.2 1.6 %shard_map.174 = (f32[1,3200]{1,0:T(1,128)S(1)}, f32[1,3200]{1,0:T(1,128)S(1)}, f32[1,3200]{1,0:T(1,128)S(1)}, f32[1,3200]{1,0:T(1,128)S(1)}, f32[4,512]{1,0:T(4,128)S(1)}) custom-call(bf16[4,2048]{1,0:T(4,128)(2,1)S(1)} %add_convert_fusion.s0, bf16[4,2048]{1,0:T(4,128)(2,1)S(1)} %collective-permute-done.5.s1, ...), custom_call_target="tpu_custom_call" | custom-call | flops 10000000000 | tf_op jit(solution)/shard_map/pallas_call | solution.py:52
  25.8 3.4 %collective-permute-start.10 = (f32[1,3200]{1,0:T(1,128)S(1)}, f32[1,3200]{1,0:T(1,128)S(1)}, u32[]{:S(2)}, u32[]{:S(2)}) collective-permute-start(f32[1,3200]{1,0:T(1,128)S(1)} %get-tuple-element.24), channel_id=1, source_target_pairs={{0,6},{2,4},{4,2},{6,0},{1,7},{3,5},{5,3},{7,1},{8,14},{10,12},{12... | collective-permute-start | bytes 38408 | tf_op jit(solution)/shard_map/ppermute | solution.py:35
  29.2 1.0 %collective-permute-start.9 = (f32[1,3200]{1,0:T(1,128)S(1)}, f32[1,3200]{1,0:T(1,128)S(1)}, u32[]{:S(2)}, u32[]{:S(2)}) collective-permute-start(f32[1,3200]{1,0:T(1,128)S(1)} %get-tuple-element.23), channel_id=1, source_target_pairs={{0,4},{2,6},{4,0},{6,2},{1,5},{3,7},{5,1},{7,3},{8,12},{10,14},{12... | collective-permute-start | bytes 38408 | tf_op jit(solution)/shard_map/ppermute | solution.py:35
  31.5 1.4 %collective-permute-done.8.p1 = f32[1,3200]{1,0:T(1,128)S(1)} collective-permute-done((f32[1,3200]{1,0:T(1,128)S(1)}, f32[1,3200]{1,0:T(1,128)S(1)}, u32[]{:S(2)}, u32[]{:S(2)}) %collective-permute-start.8) | collective-permute-done | bytes 12832 | tf_op jit(solution)/shard_map/ppermute | solution.py:35
  32.9 0.9 %collective-permute-done.9.p2 = f32[1,3200]{1,0:T(1,128)S(1)} collective-permute-done((f32[1,3200]{1,0:T(1,128)S(1)}, f32[1,3200]{1,0:T(1,128)S(1)}, u32[]{:S(2)}, u32[]{:S(2)}) %collective-permute-start.9) | collective-permute-done | bytes 12832 | tf_op jit(solution)/shard_map/ppermute | solution.py:35
  33.9 0.6 shard_map.176.m0
  34.5 2.1 %collective-permute-start.11 = (f32[1,2048]{1,0:T(1,128)S(1)}, f32[1,2048]{1,0:T(1,128)S(1)}, u32[]{:S(2)}, u32[]{:S(2)}) collective-permute-start(f32[1,2048]{1,0:T(1,128)S(1)} %shard_map.176.m0), channel_id=1, source_target_pairs={{0,2},{2,0},{4,6},{6,4},{1,3},{3,1},{5,7},{7,5},{8,10},{10,8},{12,... | collective-permute-start | bytes 24584 | tf_op jit(solution)/shard_map/ppermute | solution.py:35
  36.6 2.4 %collective-permute-start.13 = (f32[1,2048]{1,0:T(1,128)S(1)}, f32[1,2048]{1,0:T(1,128)S(1)}, u32[]{:S(2)}, u32[]{:S(2)}) collective-permute-start(f32[1,2048]{1,0:T(1,128)S(1)} %shard_map.176.m0), channel_id=1, source_target_pairs={{0,6},{2,4},{4,2},{6,0},{1,7},{3,5},{5,3},{7,1},{8,14},{10,12},{12... | collective-permute-start | bytes 24584 | tf_op jit(solution)/shard_map/ppermute | solution.py:35
  39.1 2.1 %collective-permute-done.12.m2 = f32[1,2048]{1,0:T(1,128)S(1)} collective-permute-done((f32[1,2048]{1,0:T(1,128)S(1)}, f32[1,2048]{1,0:T(1,128)S(1)}, u32[]{:S(2)}, u32[]{:S(2)}) %collective-permute-start.12) | collective-permute-done | bytes 8224 | tf_op jit(solution)/shard_map/ppermute | solution.py:35
  41.2 0.9 %collective-permute-done.13.m3 = f32[1,2048]{1,0:T(1,128)S(1)} collective-permute-done((f32[1,2048]{1,0:T(1,128)S(1)}, f32[1,2048]{1,0:T(1,128)S(1)}, u32[]{:S(2)}, u32[]{:S(2)}) %collective-permute-start.13) | collective-permute-done | bytes 8224 | tf_op jit(solution)/shard_map/ppermute | solution.py:35
  42.5 1.2 %collective-permute-done.14 = f32[4,512]{1,0:T(4,128)S(1)} collective-permute-done((f32[4,512]{1,0:T(4,128)S(1)}, f32[4,512]{1,0:T(4,128)S(1)}, u32[]{:S(2)}, u32[]{:S(2)}) %collective-permute-start.14) | collective-permute-done | bytes 8224 | tf_op jit(solution)/shard_map/ppermute | solution.py:44
  43.7 3.0 %collective-permute-start.16 = (bf16[4,512]{1,0:T(4,128)(2,1)S(1)}, bf16[4,512]{1,0:T(4,128)(2,1)S(1)}, u32[]{:S(2)}, u32[]{:S(2)}) collective-permute-start(bf16[4,512]{1,0:T(4,128)(2,1)S(1)} %add_convert_fusion.1.s0), channel_id=1, source_target_pairs={{0,4},{2,6},{4,0},{6,2},{1,5},{3,7},{5,1},{7,3},{8,12},{10,14},{12... | collective-permute-start | bytes 12296 | tf_op jit(solution)/shard_map/ppermute | solution.py:35
  46.7 1.4 %collective-permute-start.17 = (bf16[4,512]{1,0:T(4,128)(2,1)S(1)}, bf16[4,512]{1,0:T(4,128)(2,1)S(1)}, u32[]{:S(2)}, u32[]{:S(2)}) collective-permute-start(bf16[4,512]{1,0:T(4,128)(2,1)S(1)} %add_convert_fusion.1.s0), channel_id=1, source_target_pairs={{0,6},{2,4},{4,2},{6,0},{1,7},{3,5},{5,3},{7,1},{8,14},{10,12},{12... | collective-permute-start | bytes 12296 | tf_op jit(solution)/shard_map/ppermute | solution.py:35
  48.2 3.8 %collective-permute-done.17.s3 = bf16[4,512]{1,0:T(4,128)(2,1)S(1)} collective-permute-done((bf16[4,512]{1,0:T(4,128)(2,1)S(1)}, bf16[4,512]{1,0:T(4,128)(2,1)S(1)}, u32[]{:S(2)}, u32[]{:S(2)}) %collective-permute-start.17) | collective-permute-done | bytes 4128 | tf_op jit(solution)/shard_map/ppermute | solution.py:35
  52.1 2.1 %shard_map.178 = (f32[4,512]{1,0:T(4,128)S(1)}, f32[4,512]{1,0:T(4,128)S(1)}, f32[4,512]{1,0:T(4,128)S(1)}, f32[4,512]{1,0:T(4,128)S(1)}, f32[4,512]{1,0:T(4,128)S(1)}) custom-call(bf16[4,512]{1,0:T(4,128)(2,1)S(1)} %add_convert_fusion.1.s0, bf16[4,512]{1,0:T(4,128)(2,1)S(1)} %collective-permute-done.15.s1, bf16[4,512]{1,0:T(4,128)(2,1)S(1)} %collective-permute-done.16.s2, ...), custom_call_target="tpu_custom_call" | custom-call | flops 10000000000 | tf_op jit(solution)/shard_map/pallas_call | solution.py:52
  54.2 2.0 %collective-permute-start.19 = (f32[4,512]{1,0:T(4,128)S(1)}, f32[4,512]{1,0:T(4,128)S(1)}, u32[]{:S(2)}, u32[]{:S(2)}) collective-permute-start(f32[4,512]{1,0:T(4,128)S(1)} %get-tuple-element.31), channel_id=1, source_target_pairs={{0,4},{2,6},{4,0},{6,2},{1,5},{3,7},{5,1},{7,3},{8,12},{10,14},{12... | collective-permute-start | bytes 24584 | tf_op jit(solution)/shard_map/ppermute | solution.py:35
  56.2 2.4 %collective-permute-start.20 = (f32[4,512]{1,0:T(4,128)S(1)}, f32[4,512]{1,0:T(4,128)S(1)}, u32[]{:S(2)}, u32[]{:S(2)}) collective-permute-start(f32[4,512]{1,0:T(4,128)S(1)} %get-tuple-element.32), channel_id=1, source_target_pairs={{0,6},{2,4},{4,2},{6,0},{1,7},{3,5},{5,3},{7,1},{8,14},{10,12},{12... | collective-permute-start | bytes 24584 | tf_op jit(solution)/shard_map/ppermute | solution.py:35
  58.8 2.8 %collective-permute-done.20 = f32[4,512]{1,0:T(4,128)S(1)} collective-permute-done((f32[4,512]{1,0:T(4,128)S(1)}, f32[4,512]{1,0:T(4,128)S(1)}, u32[]{:S(2)}, u32[]{:S(2)}) %collective-permute-start.20) | collective-permute-done | bytes 8224 | tf_op jit(solution)/shard_map/ppermute | solution.py:35
  61.7 1.1 %collective-permute-done.21 = f32[4,256]{1,0:T(4,128)S(1)} collective-permute-done((f32[4,256]{1,0:T(4,128)S(1)}, f32[4,256]{1,0:T(4,128)S(1)}, u32[]{:S(2)}, u32[]{:S(2)}) %collective-permute-start.21) | collective-permute-done | bytes 4128 | tf_op jit(solution)/shard_map/ppermute | solution.py:44
  62.9 0.6 add_convert_fusion.2
  (81 shorter events, 3.3 us)
Async XLA Ops:
  0.0 14.2 %copy-start = (bf16[2,2048,704]{1,2,0:T(8,128)(2,1)S(1)}, bf16[2,2048,704]{1,2,0:T(8,128)(2,1)}, u32[]{:S(2)}) copy-start(bf16[2,2048,704]{1,2,0:T(8,128)(2,1)} %param.20) | copy-start | bytes 17301508
  0.0 14.2 %copy-start.1 = (bf16[2,2048,704]{1,2,0:T(8,128)(2,1)S(1)}, bf16[2,2048,704]{1,2,0:T(8,128)(2,1)}, u32[]{:S(2)}) copy-start(bf16[2,2048,704]{1,2,0:T(8,128)(2,1)} %param.21) | copy-start | bytes 17301508
  0.0 14.2 %copy-start.2 = (bf16[2,704,2048]{2,1,0:T(8,128)(2,1)S(1)}, bf16[2,704,2048]{2,1,0:T(8,128)(2,1)}, u32[]{:S(2)}) copy-start(bf16[2,704,2048]{2,1,0:T(8,128)(2,1)} %down.3) | copy-start | bytes 17301508
  1.9 5.7 %collective-permute-start = (bf16[8,256]{1,0:T(8,128)(2,1)S(1)}, bf16[8,256]{1,0:T(8,128)(2,1)S(1)}, u32[]{:S(2)}, u32[]{:S(2)}) collective-permute-start(bf16[8,256]{1,0:T(8,128)(2,1)S(1)} %shard_map.172), channel_id=1, source_target_pairs={{0,2},{2,0},{4,6},{6,4},{1,3},{3,1},{5,7},{7,5},{8,10},{10,8},{12,... | collective-permute-start | bytes 12296 | tf_op jit(solution)/shard_map/ppermute | solution.py:35
  5.0 4.5 %collective-permute-start.1 = (bf16[8,256]{1,0:T(8,128)(2,1)S(1)}, bf16[8,256]{1,0:T(8,128)(2,1)S(1)}, u32[]{:S(2)}, u32[]{:S(2)}) collective-permute-start(bf16[8,256]{1,0:T(8,128)(2,1)S(1)} %shard_map.172), channel_id=1, source_target_pairs={{0,4},{2,6},{4,0},{6,2},{1,5},{3,7},{5,1},{7,3},{8,12},{10,14},{12... | collective-permute-start | bytes 12296 | tf_op jit(solution)/shard_map/ppermute | solution.py:35
  7.6 5.4 %collective-permute-start.2 = (bf16[8,256]{1,0:T(8,128)(2,1)S(1)}, bf16[8,256]{1,0:T(8,128)(2,1)S(1)}, u32[]{:S(2)}, u32[]{:S(2)}) collective-permute-start(bf16[8,256]{1,0:T(8,128)(2,1)S(1)} %shard_map.172), channel_id=1, source_target_pairs={{0,6},{2,4},{4,2},{6,0},{1,7},{3,5},{5,3},{7,1},{8,14},{10,12},{12... | collective-permute-start | bytes 12296 | tf_op jit(solution)/shard_map/ppermute | solution.py:35
  13.0 1.2 %collective-permute-start.3 = (bf16[8,1024]{1,0:T(8,128)(2,1)S(1)}, bf16[8,1024]{1,0:T(8,128)(2,1)S(1)}, u32[]{:S(2)}, u32[]{:S(2)}) collective-permute-start(bf16[8,1024]{1,0:T(8,128)(2,1)S(1)} %pad_maximum_fusion.own), channel_id=1, source_target_pairs={{0,1},{1,0},{2,3},{3,2},{4,5},{5,4},{6,7},{7,6},{8,9},{9,8},{10,11... | collective-permute-start | bytes 49160 | tf_op jit(solution)/shard_map/ppermute | solution.py:44
  14.2 9.7 %copy-start.7 = (bf16[512,64]{0,1:T(8,128)(2,1)S(1)}, bf16[512,64]{0,1:T(8,128)(2,1)}, u32[]{:S(2)}) copy-start(bf16[512,64]{0,1:T(8,128)(2,1)} %param.26) | copy-start | bytes 196612
  16.3 1.2 %collective-permute-start.4 = (f32[4,2048]{1,0:T(4,128)S(1)}, f32[4,2048]{1,0:T(4,128)S(1)}, u32[]{:S(2)}, u32[]{:S(2)}) collective-permute-start(f32[4,2048]{1,0:T(4,128)S(1)} %get-tuple-element.19), channel_id=1, source_target_pairs={{0,1},{1,0},{2,3},{3,2},{4,5},{5,4},{6,7},{7,6},{8,9},{9,8},{10,11... | collective-permute-start | bytes 98312 | tf_op jit(solution)/shard_map/ppermute | solution.py:44
  17.6 5.0 %collective-permute-start.5 = (bf16[4,2048]{1,0:T(4,128)(2,1)S(1)}, bf16[4,2048]{1,0:T(4,128)(2,1)S(1)}, u32[]{:S(2)}, u32[]{:S(2)}) collective-permute-start(bf16[4,2048]{1,0:T(4,128)(2,1)S(1)} %add_convert_fusion.s0), channel_id=1, source_target_pairs={{0,2},{2,0},{4,6},{6,4},{1,3},{3,1},{5,7},{7,5},{8,10},{10,8},{12,... | collective-permute-start | bytes 49160 | tf_op jit(solution)/shard_map/ppermute | solution.py:35
  17.6 4.9 %collective-permute-start.6 = (bf16[4,2048]{1,0:T(4,128)(2,1)S(1)}, bf16[4,2048]{1,0:T(4,128)(2,1)S(1)}, u32[]{:S(2)}, u32[]{:S(2)}) collective-permute-start(bf16[4,2048]{1,0:T(4,128)(2,1)S(1)} %add_convert_fusion.s0), channel_id=1, source_target_pairs={{0,4},{2,6},{4,0},{6,2},{1,5},{3,7},{5,1},{7,3},{8,12},{10,14},{12... | collective-permute-start | bytes 49160 | tf_op jit(solution)/shard_map/ppermute | solution.py:35
  18.2 5.7 %collective-permute-start.7 = (bf16[4,2048]{1,0:T(4,128)(2,1)S(1)}, bf16[4,2048]{1,0:T(4,128)(2,1)S(1)}, u32[]{:S(2)}, u32[]{:S(2)}) collective-permute-start(bf16[4,2048]{1,0:T(4,128)(2,1)S(1)} %add_convert_fusion.s0), channel_id=1, source_target_pairs={{0,6},{2,4},{4,2},{6,0},{1,7},{3,5},{5,3},{7,1},{8,14},{10,12},{12... | collective-permute-start | bytes 49160 | tf_op jit(solution)/shard_map/ppermute | solution.py:35
  25.8 5.7 %collective-permute-start.10 = (f32[1,3200]{1,0:T(1,128)S(1)}, f32[1,3200]{1,0:T(1,128)S(1)}, u32[]{:S(2)}, u32[]{:S(2)}) collective-permute-start(f32[1,3200]{1,0:T(1,128)S(1)} %get-tuple-element.24), channel_id=1, source_target_pairs={{0,6},{2,4},{4,2},{6,0},{1,7},{3,5},{5,3},{7,1},{8,14},{10,12},{12... | collective-permute-start | bytes 38408 | tf_op jit(solution)/shard_map/ppermute | solution.py:35
  29.2 3.7 %collective-permute-start.8 = (f32[1,3200]{1,0:T(1,128)S(1)}, f32[1,3200]{1,0:T(1,128)S(1)}, u32[]{:S(2)}, u32[]{:S(2)}) collective-permute-start(f32[1,3200]{1,0:T(1,128)S(1)} %get-tuple-element.22), channel_id=1, source_target_pairs={{0,2},{2,0},{4,6},{6,4},{1,3},{3,1},{5,7},{7,5},{8,10},{10,8},{12,... | collective-permute-start | bytes 38408 | tf_op jit(solution)/shard_map/ppermute | solution.py:35
  29.2 4.6 %collective-permute-start.9 = (f32[1,3200]{1,0:T(1,128)S(1)}, f32[1,3200]{1,0:T(1,128)S(1)}, u32[]{:S(2)}, u32[]{:S(2)}) collective-permute-start(f32[1,3200]{1,0:T(1,128)S(1)} %get-tuple-element.23), channel_id=1, source_target_pairs={{0,4},{2,6},{4,0},{6,2},{1,5},{3,7},{5,1},{7,3},{8,12},{10,14},{12... | collective-permute-start | bytes 38408 | tf_op jit(solution)/shard_map/ppermute | solution.py:35
  33.9 18.2 %slice-start = ((s8[5767168]{0:T(1024)(128)(4,1)}), s8[4194304]{0:T(1024)(128)(4,1)S(1)}, s32[]{:S(2)}) async-start(s8[5767168]{0:T(1024)(128)(4,1)} %bitcast.25), calls=%async_computation | async-start | bytes 8388608
  33.9 18.2 %slice-start.2 = ((s8[5767168]{0:T(1024)(128)(4,1)}), s8[4194304]{0:T(1024)(128)(4,1)S(1)}, s32[]{:S(2)}) async-start(s8[5767168]{0:T(1024)(128)(4,1)} %bitcast.29), calls=%async_computation.2 | async-start | bytes 8388608
  33.9 18.2 %slice-start.4 = ((s8[5767168]{0:T(1024)(128)(4,1)}), s8[4194304]{0:T(1024)(128)(4,1)S(1)}, s32[]{:S(2)}) async-start(s8[5767168]{0:T(1024)(128)(4,1)} %bitcast.32), calls=%async_computation.4 | async-start | bytes 8388608
  34.5 4.6 %collective-permute-start.11 = (f32[1,2048]{1,0:T(1,128)S(1)}, f32[1,2048]{1,0:T(1,128)S(1)}, u32[]{:S(2)}, u32[]{:S(2)}) collective-permute-start(f32[1,2048]{1,0:T(1,128)S(1)} %shard_map.176.m0), channel_id=1, source_target_pairs={{0,2},{2,0},{4,6},{6,4},{1,3},{3,1},{5,7},{7,5},{8,10},{10,8},{12,... | collective-permute-start | bytes 24584 | tf_op jit(solution)/shard_map/ppermute | solution.py:35
  36.6 4.5 %collective-permute-start.12 = (f32[1,2048]{1,0:T(1,128)S(1)}, f32[1,2048]{1,0:T(1,128)S(1)}, u32[]{:S(2)}, u32[]{:S(2)}) collective-permute-start(f32[1,2048]{1,0:T(1,128)S(1)} %shard_map.176.m0), channel_id=1, source_target_pairs={{0,4},{2,6},{4,0},{6,2},{1,5},{3,7},{5,1},{7,3},{8,12},{10,14},{12... | collective-permute-start | bytes 24584 | tf_op jit(solution)/shard_map/ppermute | solution.py:35
  36.6 5.4 %collective-permute-start.13 = (f32[1,2048]{1,0:T(1,128)S(1)}, f32[1,2048]{1,0:T(1,128)S(1)}, u32[]{:S(2)}, u32[]{:S(2)}) collective-permute-start(f32[1,2048]{1,0:T(1,128)S(1)} %shard_map.176.m0), channel_id=1, source_target_pairs={{0,6},{2,4},{4,2},{6,0},{1,7},{3,5},{5,3},{7,1},{8,14},{10,12},{12... | collective-permute-start | bytes 24584 | tf_op jit(solution)/shard_map/ppermute | solution.py:35
  42.1 10.0 %slice-start.1 = ((s8[5767168]{0:T(1024)(128)(4,1)}), s8[1572864]{0:T(1024)(128)(4,1)S(1)}, s32[]{:S(2)}) async-start(s8[5767168]{0:T(1024)(128)(4,1)} %bitcast.25), calls=%async_computation.1 | async-start | bytes 3145728
  42.1 10.0 %slice-start.3 = ((s8[5767168]{0:T(1024)(128)(4,1)}), s8[1572864]{0:T(1024)(128)(4,1)S(1)}, s32[]{:S(2)}) async-start(s8[5767168]{0:T(1024)(128)(4,1)} %bitcast.29), calls=%async_computation.3 | async-start | bytes 3145728
  42.1 10.0 %slice-start.5 = ((s8[5767168]{0:T(1024)(128)(4,1)}), s8[1572864]{0:T(1024)(128)(4,1)S(1)}, s32[]{:S(2)}) async-start(s8[5767168]{0:T(1024)(128)(4,1)} %bitcast.32), calls=%async_computation.5 | async-start | bytes 3145728
  42.5 1.2 %collective-permute-start.14 = (f32[4,512]{1,0:T(4,128)S(1)}, f32[4,512]{1,0:T(4,128)S(1)}, u32[]{:S(2)}, u32[]{:S(2)}) collective-permute-start(f32[4,512]{1,0:T(4,128)S(1)} %shard_map.177), channel_id=1, source_target_pairs={{0,1},{1,0},{2,3},{3,2},{4,5},{5,4},{6,7},{7,6},{8,9},{9,8},{10,11... | collective-permute-start | bytes 24584 | tf_op jit(solution)/shard_map/ppermute | solution.py:44
  43.7 4.4 %collective-permute-start.15 = (bf16[4,512]{1,0:T(4,128)(2,1)S(1)}, bf16[4,512]{1,0:T(4,128)(2,1)S(1)}, u32[]{:S(2)}, u32[]{:S(2)}) collective-permute-start(bf16[4,512]{1,0:T(4,128)(2,1)S(1)} %add_convert_fusion.1.s0), channel_id=1, source_target_pairs={{0,2},{2,0},{4,6},{6,4},{1,3},{3,1},{5,7},{7,5},{8,10},{10,8},{12,... | collective-permute-start | bytes 12296 | tf_op jit(solution)/shard_map/ppermute | solution.py:35
  43.7 4.6 %collective-permute-start.16 = (bf16[4,512]{1,0:T(4,128)(2,1)S(1)}, bf16[4,512]{1,0:T(4,128)(2,1)S(1)}, u32[]{:S(2)}, u32[]{:S(2)}) collective-permute-start(bf16[4,512]{1,0:T(4,128)(2,1)S(1)} %add_convert_fusion.1.s0), channel_id=1, source_target_pairs={{0,4},{2,6},{4,0},{6,2},{1,5},{3,7},{5,1},{7,3},{8,12},{10,14},{12... | collective-permute-start | bytes 12296 | tf_op jit(solution)/shard_map/ppermute | solution.py:35
  46.7 5.4 %collective-permute-start.17 = (bf16[4,512]{1,0:T(4,128)(2,1)S(1)}, bf16[4,512]{1,0:T(4,128)(2,1)S(1)}, u32[]{:S(2)}, u32[]{:S(2)}) collective-permute-start(bf16[4,512]{1,0:T(4,128)(2,1)S(1)} %add_convert_fusion.1.s0), channel_id=1, source_target_pairs={{0,6},{2,4},{4,2},{6,0},{1,7},{3,5},{5,3},{7,1},{8,14},{10,12},{12... | collective-permute-start | bytes 12296 | tf_op jit(solution)/shard_map/ppermute | solution.py:35
  54.2 4.4 %collective-permute-start.18 = (f32[4,512]{1,0:T(4,128)S(1)}, f32[4,512]{1,0:T(4,128)S(1)}, u32[]{:S(2)}, u32[]{:S(2)}) collective-permute-start(f32[4,512]{1,0:T(4,128)S(1)} %get-tuple-element.30), channel_id=1, source_target_pairs={{0,2},{2,0},{4,6},{6,4},{1,3},{3,1},{5,7},{7,5},{8,10},{10,8},{12,... | collective-permute-start | bytes 24584 | tf_op jit(solution)/shard_map/ppermute | solution.py:35
  54.2 4.6 %collective-permute-start.19 = (f32[4,512]{1,0:T(4,128)S(1)}, f32[4,512]{1,0:T(4,128)S(1)}, u32[]{:S(2)}, u32[]{:S(2)}) collective-permute-start(f32[4,512]{1,0:T(4,128)S(1)} %get-tuple-element.31), channel_id=1, source_target_pairs={{0,4},{2,6},{4,0},{6,2},{1,5},{3,7},{5,1},{7,3},{8,12},{10,14},{12... | collective-permute-start | bytes 24584 | tf_op jit(solution)/shard_map/ppermute | solution.py:35
  56.2 5.4 %collective-permute-start.20 = (f32[4,512]{1,0:T(4,128)S(1)}, f32[4,512]{1,0:T(4,128)S(1)}, u32[]{:S(2)}, u32[]{:S(2)}) collective-permute-start(f32[4,512]{1,0:T(4,128)S(1)} %get-tuple-element.32), channel_id=1, source_target_pairs={{0,6},{2,4},{4,2},{6,0},{1,7},{3,5},{5,3},{7,1},{8,14},{10,12},{12... | collective-permute-start | bytes 24584 | tf_op jit(solution)/shard_map/ppermute | solution.py:35
  61.6 1.2 %collective-permute-start.21 = (f32[4,256]{1,0:T(4,128)S(1)}, f32[4,256]{1,0:T(4,128)S(1)}, u32[]{:S(2)}, u32[]{:S(2)}) collective-permute-start(f32[4,256]{1,0:T(4,128)S(1)} %constant_dynamic-slice_fusion), channel_id=1, source_target_pairs={{0,1},{1,0},{2,3},{3,2},{4,5},{5,4},{6,7},{7,6},{8,9},{9,8},{10,11... | collective-permute-start | bytes 12296 | tf_op jit(solution)/shard_map/ppermute | solution.py:44
  (14 other events, 47.5 us)
where the time goes:
time: 63.6 us; the launch traced here: 63.5 us
  starting transfers between devices  28.2 us (44%)
  waiting for transfers between devices  23.6 us (37%)
  Pallas kernels  6.84 us (11%)
  local copies, waits for them, and re-layouts  3.87 us (6%)
    ppermute x18, starting transfers between devices, swap_kv(): got[d] = lax.ppermute(values[d], 'kv', [(i, i ^ d) for i in range(kv)])  27.9 us
    ppermute x18, waiting for transfers between devices, swap_kv(): got[d] = lax.ppermute(values[d], 'kv', [(i, i ^ d) for i in range(kv)])  19.1 us
    pallas_call x7, Pallas kernels, run(): pl.pallas_call(body, out_shape=outs, in_specs=in_specs or [VMEM] * len(ar...  6.84 us
    ppermute x4, waiting for transfers between devices, swap_tp(): return lax.ppermute(value, 'tp', [(0, 1), (1, 0)])  4.54 us
    unnamed x51, local copies, waits for them, and re-layouts  3.65 us
  transfers between devices with their start and end apart: 22, of which 15 were waited for; matrix products, arithmetic and copies ran while one was open for 2% of the time, Pallas kernels for 0%

commit v1 on v0

--- a/solution.py
+++ b/solution.py
@@ -12,7 +12,7 @@
 F32 = jnp.float32
 BF16 = jnp.bfloat16
 NT = (((1,), (1,)), ((), ()))
-ANY = pl.BlockSpec(memory_space=pl.ANY)
+HBM = pl.BlockSpec(memory_space=pltpu.HBM)
 VMEM = pl.BlockSpec(memory_space=pltpu.VMEM)
 
 
@@ -46,6 +46,10 @@
 
 def in_vmem(value):
     return pltpu.with_memory_space_constraint(value, pltpu.VMEM)
+
+
+def in_hbm(value):
+    return pltpu.with_memory_space_constraint(value, pltpu.HBM)
 
 
 def run(body, outs, args, scratch=(), limit=16, in_specs=None, flops=10**10):
@@ -81,15 +85,71 @@
 
 
 def feed(normed, layer, gate, up, down):
-    hidden = (silu(dot_nt(normed, gate[layer])) * dot_nt(normed, up[layer])).astype(BF16)
-    return dot_nn(hidden, down[layer])
-
-
-def pack_body(rows, gains, out):
-    seqs = rows.shape[0]
-    out[:seqs] = rows[...]
-    out[seqs : seqs + gains.shape[0]] = gains[...]
-    out[seqs + gains.shape[0] :] = gains[:1]
+    if len(gate.shape) == 3:
+        gated, upper = dot_nt(normed, gate[layer]), dot_nt(normed, up[layer])
+    else:
+        gated, upper = dot_nn(normed, gate[...]), dot_nn(normed, up[...])
+    return dot_nn((silu(gated) * upper).astype(BF16), down[layer])
+
+
+def pack_body(rows, gains, out, rows_held, gains_held, sems):
+    copies = (
+        pltpu.make_async_copy(rows, rows_held, sems.at[0]),
+        pltpu.make_async_copy(gains, gains_held, sems.at[1]),
+    )
+    for copy in copies:
+        copy.start()
+    for copy in copies:
+        copy.wait()
+    seqs, count = rows_held.shape[0], gains_held.shape[0]
+    out[:seqs] = rows_held[...]
+    out[seqs : seqs + count] = gains_held[...]
+    out[seqs + count :] = gains_held[:1]
+
+
+def turn_body(*refs):
+    count = len(refs) // 2
+    for source, target in zip(refs[:count], refs[count:]):
+        target[...] = source[...].T
+
+
+def turned(sources):
+    outs = run(
+        turn_body, [bf16(*source.shape[::-1]) for source in sources], tuple(map(in_vmem, sources))
+    )
+    return [in_vmem(out) for out in outs]
+
+
+TURN = 256
+
+
+def turn_layer_body(layer, source, target, held, sems):
+    height = held.shape[0]
+    blocks = [pl.ds(i, min(TURN, height - i)) for i in range(0, height, TURN)]
+    copies = [
+        pltpu.make_async_copy(source.at[layer, rows], held.at[rows], sems.at[i])
+        for i, rows in enumerate(blocks)
+    ]
+    for copy in copies:
+        copy.start()
+    for copy, rows in zip(copies, blocks):
+        copy.wait()
+        target[:, rows] = held[rows].T
+
+
+def turned_layer(source, layer):
+    height, wide = source.shape[1:]
+    out = run(
+        functools.partial(turn_layer_body, layer),
+        bf16(wide, height),
+        (in_hbm(source),),
+        [
+            pltpu.VMEM((height, wide), BF16),
+            pltpu.SemaphoreType.DMA((pl.cdiv(height, TURN),)),
+        ],
+        in_specs=[HBM],
+    )
+    return in_vmem(out)
 
 
 def first_body(kv, seqs, own, other, gate, up, down, sums_out, rows_out, slabs):
@@ -120,8 +180,8 @@
         firsts[i] = padded[:, i * span : (i + 1) * span]
     slab = slabs[here].astype(BF16)
     first_out[...] = firsts[here][:seqs]
-    xs = dot_nt(normed, w_x[...]).astype(BF16).astype(F32)
-    zeta = dot_nt(normed, w_z[...]).astype(BF16).astype(F32)
+    xs = dot_nn(normed, w_x[...]).astype(BF16).astype(F32)
+    zeta = dot_nn(normed, w_z[...]).astype(BF16).astype(F32)
     bc = dot_nn(slab, w_bc[...])
     dt = dot_nt(slab, w_dt[...])
     width = xs.shape[1]
@@ -260,24 +320,34 @@
     wide = heads // groups * half
     flat = heads * half
 
-    pack = run(pack_body, bf16(2 * seqs, width), (resid, norm_gain), flops=10**10)
+    pack = run(
+        pack_body,
+        bf16(2 * seqs, width),
+        (in_hbm(resid), in_hbm(norm_gain)),
+        [
+            pltpu.VMEM(resid.shape, BF16),
+            pltpu.VMEM(norm_gain.shape, BF16),
+            pltpu.SemaphoreType.DMA((2,)),
+        ],
+        in_specs=[HBM] * 2,
+    )
     chip = jnp.concatenate(share_kv(pack, kv), axis=1)
     other = swap_tp(chip)
-    weights = tuple(map(in_vmem, (gate, up, ffn_down)))
+    down = in_vmem(ffn_down)
+
     sums, rows = run(
         functools.partial(first_body, kv, seqs),
         [f32(seqs, model), bf16(2 * seqs, model)],
-        (chip, other, *weights),
+        (chip, other, in_vmem(gate), in_vmem(up), down),
         [pltpu.VMEM((kv * tp, 2 * seqs, width), BF16)],
     )
     sums = (sums + swap_tp(sums)).astype(BF16)
     sums = share_kv(sums, kv)
 
-    w_xs, w_zs, w_maps, w_steps, w_join = map(
+    w_xs, w_zs = turned([jnp.transpose(w, (1, 2, 0)).reshape(local, model) for w in (w_x, w_z)])
+    w_maps, w_steps, w_join = map(
         in_vmem,
         (
-            jnp.transpose(w_x, (1, 2, 0)).reshape(local, model),
-            jnp.transpose(w_z, (1, 2, 0)).reshape(local, model),
             w_bc.reshape(span, 2 * groups * states),
             w_dt.T,
             w_out.reshape(flat, span),
@@ -328,10 +398,12 @@
         [pltpu.VMEM((2 * seqs, flat), F32)],
     )
     second = share_kv((joined + swap_tp(joined)).astype(BF16), kv)
+    gate_two = turned_layer(gate, 1)
+    up_two = turned_layer(up, 1)
     *sums, own = run(
         functools.partial(second_body, kv, seqs),
         [f32(seqs, span)] * kv + [f32(seqs, span)],
-        (*second, rows, *weights),
+        (*second, rows, gate_two, up_two, down),
         [pltpu.VMEM((kv, seqs, span), F32), pltpu.VMEM((kv, seqs, span), F32)],
     )
     total = sum(swap_kv(sums))

time: 63.6 us -> 62.6 us (0.984)
  Pallas kernels: 6.84 us -> 12.2 us
  waiting for transfers between devices: 23.6 us -> 18.7 us
  local copies, waits for them, and re-layouts: 3.87 us -> 2.33 us
    pallas_call x7 -> x10, Pallas kernels: 6.84 us -> 12.2 us  [run(): pl.pallas_call(body, out_shape=outs, in_specs=in_specs or [VMEM] * len(ar...]
    ppermute x18, waiting for transfers between devices: 19.1 us -> 15.3 us  [swap_kv(): got[d] = lax.ppermute(values[d], 'kv', [(i, i ^ d) for i in range(kv)])]
    unnamed x51 -> x39, local copies, waits for them, and re-layouts: 3.65 us -> 2.11 us
    ppermute x4, waiting for transfers between devices: 4.54 us -> 3.38 us  [swap_tp(): return lax.ppermute(value, 'tp', [(0, 1), (1, 0)])]
  transfers between devices with their start and end apart: 22 -> 22, of which waited for: 15 -> 12; matrix products, arithmetic and copies ran while one was open for 2% -> 2% of each run, Pallas kernels for 0% -> 9%
where the time goes in v1:
time: 62.6 us; the launch traced here: 62.3 us
  starting transfers between devices  28.2 us (45%)
  waiting for transfers between devices  18.7 us (30%)
  Pallas kernels  12.2 us (19%)
  local copies, waits for them, and re-layouts  2.33 us (4%)
    ppermute x18, starting transfers between devices, swap_kv(): got[d] = lax.ppermute(values[d], 'kv', [(i, i ^ d) for i in range(kv)])  28 us
    ppermute x18, waiting for transfers between devices, swap_kv(): got[d] = lax.ppermute(values[d], 'kv', [(i, i ^ d) for i in range(kv)])  15.3 us
    pallas_call x10, Pallas kernels, run(): pl.pallas_call(body, out_shape=outs, in_specs=in_specs or [VMEM] * len(ar...  12.2 us
    ppermute x4, waiting for transfers between devices, swap_tp(): return lax.ppermute(value, 'tp', [(0, 1), (1, 0)])  3.38 us
    unnamed x39, local copies, waits for them, and re-layouts  2.11 us
  transfers between devices with their start and end apart: 22, of which 12 were waited for; matrix products, arithmetic and copies ran while one was open for 2% of the time, Pallas kernels for 9%

profile of v1, /device:TPU:0, one launch (start us, length us, event | category | flops | bytes accessed | tf_op | source)
XLA Modules:
  0.0 62.3 jit_solution(18093885906235487002)
XLA Ops:
  0.0 0.9 %shard_map.172 = bf16[8,256]{1,0:T(8,128)(2,1)S(1)} custom-call(bf16[4,256]{1,0:T(4,128)(2,1)} %rows.1, bf16[3,256]{1,0:T(4,128)(2,1)} %gains.1), custom_call_target="tpu_custom_call" | custom-call | flops 10000000000 | tf_op jit(solution)/shard_map/pallas_call | solution.py:56
  0.9 3.1 %collective-permute-start = (bf16[8,256]{1,0:T(8,128)(2,1)S(1)}, bf16[8,256]{1,0:T(8,128)(2,1)S(1)}, u32[]{:S(2)}, u32[]{:S(2)}) collective-permute-start(bf16[8,256]{1,0:T(8,128)(2,1)S(1)} %shard_map.172), channel_id=1, source_target_pairs={{0,2},{2,0},{4,6},{6,4},{1,3},{3,1},{5,7},{7,5},{8,10},{10,8},{12,... | collective-permute-start | bytes 12296 | tf_op jit(solution)/shard_map/ppermute | solution.py:35
  4.0 2.6 %collective-permute-start.1 = (bf16[8,256]{1,0:T(8,128)(2,1)S(1)}, bf16[8,256]{1,0:T(8,128)(2,1)S(1)}, u32[]{:S(2)}, u32[]{:S(2)}) collective-permute-start(bf16[8,256]{1,0:T(8,128)(2,1)S(1)} %shard_map.172), channel_id=1, source_target_pairs={{0,4},{2,6},{4,0},{6,2},{1,5},{3,7},{5,1},{7,3},{8,12},{10,14},{12... | collective-permute-start | bytes 12296 | tf_op jit(solution)/shard_map/ppermute | solution.py:35
  6.6 1.9 %collective-permute-done.1 = bf16[8,256]{1,0:T(8,128)(2,1)S(1)} collective-permute-done((bf16[8,256]{1,0:T(8,128)(2,1)S(1)}, bf16[8,256]{1,0:T(8,128)(2,1)S(1)}, u32[]{:S(2)}, u32[]{:S(2)}) %collective-permute-start.1) | collective-permute-done | bytes 4128 | tf_op jit(solution)/shard_map/ppermute | solution.py:35
  8.5 3.5 %collective-permute-done.2 = bf16[8,256]{1,0:T(8,128)(2,1)S(1)} collective-permute-done((bf16[8,256]{1,0:T(8,128)(2,1)S(1)}, bf16[8,256]{1,0:T(8,128)(2,1)S(1)}, u32[]{:S(2)}, u32[]{:S(2)}) %collective-permute-start.2) | collective-permute-done | bytes 4128 | tf_op jit(solution)/shard_map/ppermute | solution.py:35
  12.0 1.2 %collective-permute-done.3.other = bf16[8,1024]{1,0:T(8,128)(2,1)S(1)} collective-permute-done((bf16[8,1024]{1,0:T(8,128)(2,1)S(1)}, bf16[8,1024]{1,0:T(8,128)(2,1)S(1)}, u32[]{:S(2)}, u32[]{:S(2)}) %collective-permute-start.3) | collective-permute-done | bytes 16416 | tf_op jit(solution)/shard_map/ppermute | solution.py:44
  13.2 2.1 %shard_map.173 = (f32[4,2048]{1,0:T(4,128)S(1)}, bf16[8,2048]{1,0:T(8,128)(2,1)S(1)}) custom-call(bf16[8,1024]{1,0:T(8,128)(2,1)S(1)} %pad_maximum_fusion.own, bf16[8,1024]{1,0:T(8,128)(2,1)S(1)} %collective-permute-done.3.other, bf16[2,704,2048]{2,1,0:T(8,128)(2,1)S(1)} %bitcast.25, bf16[2,704,2048]{2,1,0:T(8,128)(2,1)S(1)} %bitcast.27, ...), custom_call_target="tpu_custom_call" | custom-call | flops 10000000000 | tf_op jit(solution)/shard_map/pallas_call | solution.py:56
  15.5 1.0 %collective-permute-done.4 = f32[4,2048]{1,0:T(4,128)S(1)} collective-permute-done((f32[4,2048]{1,0:T(4,128)S(1)}, f32[4,2048]{1,0:T(4,128)S(1)}, u32[]{:S(2)}, u32[]{:S(2)}) %collective-permute-start.4) | collective-permute-done | bytes 32800 | tf_op jit(solution)/shard_map/ppermute | solution.py:44
  16.6 0.6 collective-permute-start.6
  17.2 3.8 %collective-permute-start.7 = (bf16[4,2048]{1,0:T(4,128)(2,1)S(1)}, bf16[4,2048]{1,0:T(4,128)(2,1)S(1)}, u32[]{:S(2)}, u32[]{:S(2)}) collective-permute-start(bf16[4,2048]{1,0:T(4,128)(2,1)S(1)} %add_convert_fusion.s0), channel_id=1, source_target_pairs={{0,6},{2,4},{4,2},{6,0},{1,7},{3,5},{5,3},{7,1},{8,14},{10,12},{12... | collective-permute-start | bytes 49160 | tf_op jit(solution)/shard_map/ppermute | solution.py:35
  21.0 1.1 %shard_map.174 = (bf16[2048,512]{1,0:T(8,128)(2,1)S(1)}, bf16[2048,512]{1,0:T(8,128)(2,1)S(1)}) custom-call(bf16[512,2048]{1,0:T(8,128)(2,1)S(1)} %bitcast.30, bf16[512,2048]{1,0:T(8,128)(2,1)S(1)} %bitcast.31), custom_call_target="tpu_custom_call" | custom-call | flops 10000000000 | tf_op jit(solution)/shard_map/pallas_call | solution.py:56
  23.4 1.1 %shard_map.175 = (f32[1,3200]{1,0:T(1,128)S(1)}, f32[1,3200]{1,0:T(1,128)S(1)}, f32[1,3200]{1,0:T(1,128)S(1)}, f32[1,3200]{1,0:T(1,128)S(1)}, f32[4,512]{1,0:T(4,128)S(1)}) custom-call(bf16[4,2048]{1,0:T(4,128)(2,1)S(1)} %add_convert_fusion.s0, bf16[4,2048]{1,0:T(4,128)(2,1)S(1)} %collective-permute-done.5.s1, ...), custom_call_target="tpu_custom_call" | custom-call | flops 10000000000 | tf_op jit(solution)/shard_map/pallas_call | solution.py:56
  24.5 3.2 %collective-permute-start.10 = (f32[1,3200]{1,0:T(1,128)S(1)}, f32[1,3200]{1,0:T(1,128)S(1)}, u32[]{:S(2)}, u32[]{:S(2)}) collective-permute-start(f32[1,3200]{1,0:T(1,128)S(1)} %get-tuple-element.28), channel_id=1, source_target_pairs={{0,6},{2,4},{4,2},{6,0},{1,7},{3,5},{5,3},{7,1},{8,14},{10,12},{12... | collective-permute-start | bytes 38408 | tf_op jit(solution)/shard_map/ppermute | solution.py:35
  27.7 1.3 %collective-permute-start.9 = (f32[1,3200]{1,0:T(1,128)S(1)}, f32[1,3200]{1,0:T(1,128)S(1)}, u32[]{:S(2)}, u32[]{:S(2)}) collective-permute-start(f32[1,3200]{1,0:T(1,128)S(1)} %get-tuple-element.27), channel_id=1, source_target_pairs={{0,4},{2,6},{4,0},{6,2},{1,5},{3,7},{5,1},{7,3},{8,12},{10,14},{12... | collective-permute-start | bytes 38408 | tf_op jit(solution)/shard_map/ppermute | solution.py:35
  30.2 1.2 %collective-permute-done.8.p1 = f32[1,3200]{1,0:T(1,128)S(1)} collective-permute-done((f32[1,3200]{1,0:T(1,128)S(1)}, f32[1,3200]{1,0:T(1,128)S(1)}, u32[]{:S(2)}, u32[]{:S(2)}) %collective-permute-start.8) | collective-permute-done | bytes 12832 | tf_op jit(solution)/shard_map/ppermute | solution.py:35
  31.4 0.9 %collective-permute-done.9.p2 = f32[1,3200]{1,0:T(1,128)S(1)} collective-permute-done((f32[1,3200]{1,0:T(1,128)S(1)}, f32[1,3200]{1,0:T(1,128)S(1)}, u32[]{:S(2)}, u32[]{:S(2)}) %collective-permute-start.9) | collective-permute-done | bytes 12832 | tf_op jit(solution)/shard_map/ppermute | solution.py:35
  32.3 0.6 shard_map.177.m0
  32.9 2.1 %collective-permute-start.11 = (f32[1,2048]{1,0:T(1,128)S(1)}, f32[1,2048]{1,0:T(1,128)S(1)}, u32[]{:S(2)}, u32[]{:S(2)}) collective-permute-start(f32[1,2048]{1,0:T(1,128)S(1)} %shard_map.177.m0), channel_id=1, source_target_pairs={{0,2},{2,0},{4,6},{6,4},{1,3},{3,1},{5,7},{7,5},{8,10},{10,8},{12,... | collective-permute-start | bytes 24584 | tf_op jit(solution)/shard_map/ppermute | solution.py:35
  35.0 2.4 %collective-permute-start.13 = (f32[1,2048]{1,0:T(1,128)S(1)}, f32[1,2048]{1,0:T(1,128)S(1)}, u32[]{:S(2)}, u32[]{:S(2)}) collective-permute-start(f32[1,2048]{1,0:T(1,128)S(1)} %shard_map.177.m0), channel_id=1, source_target_pairs={{0,6},{2,4},{4,2},{6,0},{1,7},{3,5},{5,3},{7,1},{8,14},{10,12},{12... | collective-permute-start | bytes 24584 | tf_op jit(solution)/shard_map/ppermute | solution.py:35
  37.4 2.1 %collective-permute-done.12.m2 = f32[1,2048]{1,0:T(1,128)S(1)} collective-permute-done((f32[1,2048]{1,0:T(1,128)S(1)}, f32[1,2048]{1,0:T(1,128)S(1)}, u32[]{:S(2)}, u32[]{:S(2)}) %collective-permute-start.12) | collective-permute-done | bytes 8224 | tf_op jit(solution)/shard_map/ppermute | solution.py:35
  39.6 0.9 %collective-permute-done.13.m3 = f32[1,2048]{1,0:T(1,128)S(1)} collective-permute-done((f32[1,2048]{1,0:T(1,128)S(1)}, f32[1,2048]{1,0:T(1,128)S(1)}, u32[]{:S(2)}, u32[]{:S(2)}) %collective-permute-start.13) | collective-permute-done | bytes 8224 | tf_op jit(solution)/shard_map/ppermute | solution.py:35
  40.9 2.2 %shard_map.179.gate = bf16[2048,704]{1,0:T(8,128)(2,1)S(1)} custom-call(bf16[2,704,2048]{2,1,0:T(8,128)(2,1)} %bitcast.24), custom_call_target="tpu_custom_call" | custom-call | flops 10000000000 | tf_op jit(solution)/shard_map/pallas_call | solution.py:56
  43.3 3.0 %collective-permute-start.16 = (bf16[4,512]{1,0:T(4,128)(2,1)S(1)}, bf16[4,512]{1,0:T(4,128)(2,1)S(1)}, u32[]{:S(2)}, u32[]{:S(2)}) collective-permute-start(bf16[4,512]{1,0:T(4,128)(2,1)S(1)} %add_convert_fusion.1.s0), channel_id=1, source_target_pairs={{0,4},{2,6},{4,0},{6,2},{1,5},{3,7},{5,1},{7,3},{8,12},{10,14},{12... | collective-permute-start | bytes 12296 | tf_op jit(solution)/shard_map/ppermute | solution.py:35
  46.2 1.4 %collective-permute-start.17 = (bf16[4,512]{1,0:T(4,128)(2,1)S(1)}, bf16[4,512]{1,0:T(4,128)(2,1)S(1)}, u32[]{:S(2)}, u32[]{:S(2)}) collective-permute-start(bf16[4,512]{1,0:T(4,128)(2,1)S(1)} %add_convert_fusion.1.s0), channel_id=1, source_target_pairs={{0,6},{2,4},{4,2},{6,0},{1,7},{3,5},{5,3},{7,1},{8,14},{10,12},{12... | collective-permute-start | bytes 12296 | tf_op jit(solution)/shard_map/ppermute | solution.py:35
  47.6 2.2 %shard_map.180.up = bf16[2048,704]{1,0:T(8,128)(2,1)S(1)} custom-call(bf16[2,704,2048]{2,1,0:T(8,128)(2,1)} %bitcast.26), custom_call_target="tpu_custom_call" | custom-call | flops 10000000000 | tf_op jit(solution)/shard_map/pallas_call | solution.py:56
  49.9 1.7 %collective-permute-done.17.s3 = bf16[4,512]{1,0:T(4,128)(2,1)S(1)} collective-permute-done((bf16[4,512]{1,0:T(4,128)(2,1)S(1)}, bf16[4,512]{1,0:T(4,128)(2,1)S(1)}, u32[]{:S(2)}, u32[]{:S(2)}) %collective-permute-start.17) | collective-permute-done | bytes 4128 | tf_op jit(solution)/shard_map/ppermute | solution.py:35
  51.7 1.4 %shard_map.181 = (f32[4,512]{1,0:T(4,128)S(1)}, f32[4,512]{1,0:T(4,128)S(1)}, f32[4,512]{1,0:T(4,128)S(1)}, f32[4,512]{1,0:T(4,128)S(1)}, f32[4,512]{1,0:T(4,128)S(1)}) custom-call(bf16[4,512]{1,0:T(4,128)(2,1)S(1)} %add_convert_fusion.1.s0, bf16[4,512]{1,0:T(4,128)(2,1)S(1)} %collective-permute-done.15.s1, bf16[4,512]{1,0:T(4,128)(2,1)S(1)} %collective-permute-done.16.s2, ...), custom_call_target="tpu_custom_call" | custom-call | flops 10000000000 | tf_op jit(solution)/shard_map/pallas_call | solution.py:56
  53.1 2.0 %collective-permute-start.19 = (f32[4,512]{1,0:T(4,128)S(1)}, f32[4,512]{1,0:T(4,128)S(1)}, u32[]{:S(2)}, u32[]{:S(2)}) collective-permute-start(f32[4,512]{1,0:T(4,128)S(1)} %get-tuple-element.35), channel_id=1, source_target_pairs={{0,4},{2,6},{4,0},{6,2},{1,5},{3,7},{5,1},{7,3},{8,12},{10,14},{12... | collective-permute-start | bytes 24584 | tf_op jit(solution)/shard_map/ppermute | solution.py:35
  55.1 2.4 %collective-permute-start.20 = (f32[4,512]{1,0:T(4,128)S(1)}, f32[4,512]{1,0:T(4,128)S(1)}, u32[]{:S(2)}, u32[]{:S(2)}) collective-permute-start(f32[4,512]{1,0:T(4,128)S(1)} %get-tuple-element.36), channel_id=1, source_target_pairs={{0,6},{2,4},{4,2},{6,0},{1,7},{3,5},{5,3},{7,1},{8,14},{10,12},{12... | collective-permute-start | bytes 24584 | tf_op jit(solution)/shard_map/ppermute | solution.py:35
  57.7 2.8 %collective-permute-done.20 = f32[4,512]{1,0:T(4,128)S(1)} collective-permute-done((f32[4,512]{1,0:T(4,128)S(1)}, f32[4,512]{1,0:T(4,128)S(1)}, u32[]{:S(2)}, u32[]{:S(2)}) %collective-permute-start.20) | collective-permute-done | bytes 8224 | tf_op jit(solution)/shard_map/ppermute | solution.py:35
  60.6 1.1 %collective-permute-done.21 = f32[4,256]{1,0:T(4,128)S(1)} collective-permute-done((f32[4,256]{1,0:T(4,128)S(1)}, f32[4,256]{1,0:T(4,128)S(1)}, u32[]{:S(2)}, u32[]{:S(2)}) %collective-permute-start.21) | collective-permute-done | bytes 4128 | tf_op jit(solution)/shard_map/ppermute | solution.py:44
  61.7 0.6 add_convert_fusion.2
  (70 shorter events, 3.5 us)
Async XLA Ops:
  0.0 13.2 %copy-start = (bf16[2,2048,704]{1,2,0:T(8,128)(2,1)S(1)}, bf16[2,2048,704]{1,2,0:T(8,128)(2,1)}, u32[]{:S(2)}) copy-start(bf16[2,2048,704]{1,2,0:T(8,128)(2,1)} %param.20) | copy-start | bytes 17301508
  0.0 13.2 %copy-start.1 = (bf16[2,2048,704]{1,2,0:T(8,128)(2,1)S(1)}, bf16[2,2048,704]{1,2,0:T(8,128)(2,1)}, u32[]{:S(2)}) copy-start(bf16[2,2048,704]{1,2,0:T(8,128)(2,1)} %param.21) | copy-start | bytes 17301508
  0.0 13.2 %copy-start.2 = (bf16[2,704,2048]{2,1,0:T(8,128)(2,1)S(1)}, bf16[2,704,2048]{2,1,0:T(8,128)(2,1)}, u32[]{:S(2)}) copy-start(bf16[2,704,2048]{2,1,0:T(8,128)(2,1)} %down.3) | copy-start | bytes 17301508
  0.9 5.7 %collective-permute-start = (bf16[8,256]{1,0:T(8,128)(2,1)S(1)}, bf16[8,256]{1,0:T(8,128)(2,1)S(1)}, u32[]{:S(2)}, u32[]{:S(2)}) collective-permute-start(bf16[8,256]{1,0:T(8,128)(2,1)S(1)} %shard_map.172), channel_id=1, source_target_pairs={{0,2},{2,0},{4,6},{6,4},{1,3},{3,1},{5,7},{7,5},{8,10},{10,8},{12,... | collective-permute-start | bytes 12296 | tf_op jit(solution)/shard_map/ppermute | solution.py:35
  4.0 4.5 %collective-permute-start.1 = (bf16[8,256]{1,0:T(8,128)(2,1)S(1)}, bf16[8,256]{1,0:T(8,128)(2,1)S(1)}, u32[]{:S(2)}, u32[]{:S(2)}) collective-permute-start(bf16[8,256]{1,0:T(8,128)(2,1)S(1)} %shard_map.172), channel_id=1, source_target_pairs={{0,4},{2,6},{4,0},{6,2},{1,5},{3,7},{5,1},{7,3},{8,12},{10,14},{12... | collective-permute-start | bytes 12296 | tf_op jit(solution)/shard_map/ppermute | solution.py:35
  6.6 5.4 %collective-permute-start.2 = (bf16[8,256]{1,0:T(8,128)(2,1)S(1)}, bf16[8,256]{1,0:T(8,128)(2,1)S(1)}, u32[]{:S(2)}, u32[]{:S(2)}) collective-permute-start(bf16[8,256]{1,0:T(8,128)(2,1)S(1)} %shard_map.172), channel_id=1, source_target_pairs={{0,6},{2,4},{4,2},{6,0},{1,7},{3,5},{5,3},{7,1},{8,14},{10,12},{12... | collective-permute-start | bytes 12296 | tf_op jit(solution)/shard_map/ppermute | solution.py:35
  12.0 1.2 %collective-permute-start.3 = (bf16[8,1024]{1,0:T(8,128)(2,1)S(1)}, bf16[8,1024]{1,0:T(8,128)(2,1)S(1)}, u32[]{:S(2)}, u32[]{:S(2)}) collective-permute-start(bf16[8,1024]{1,0:T(8,128)(2,1)S(1)} %pad_maximum_fusion.own), channel_id=1, source_target_pairs={{0,1},{1,0},{2,3},{3,2},{4,5},{5,4},{6,7},{7,6},{8,9},{9,8},{10,11... | collective-permute-start | bytes 49160 | tf_op jit(solution)/shard_map/ppermute | solution.py:44
  13.2 7.8 %copy-start.3 = (bf16[2048,16,32]{0,2,1:T(8,128)(2,1)S(1)}, bf16[2048,16,32]{0,2,1:T(8,128)(2,1)}, u32[]{:S(2)}) copy-start(bf16[2048,16,32]{0,2,1:T(8,128)(2,1)} %param.23) | copy-start | bytes 6291460
  13.2 7.8 %copy-start.4 = (bf16[2048,16,32]{0,2,1:T(8,128)(2,1)S(1)}, bf16[2048,16,32]{0,2,1:T(8,128)(2,1)}, u32[]{:S(2)}) copy-start(bf16[2048,16,32]{0,2,1:T(8,128)(2,1)} %param.24) | copy-start | bytes 6291460
  15.3 1.2 %collective-permute-start.4 = (f32[4,2048]{1,0:T(4,128)S(1)}, f32[4,2048]{1,0:T(4,128)S(1)}, u32[]{:S(2)}, u32[]{:S(2)}) collective-permute-start(f32[4,2048]{1,0:T(4,128)S(1)} %get-tuple-element.21), channel_id=1, source_target_pairs={{0,1},{1,0},{2,3},{3,2},{4,5},{5,4},{6,7},{7,6},{8,9},{9,8},{10,11... | collective-permute-start | bytes 98312 | tf_op jit(solution)/shard_map/ppermute | solution.py:44
  16.5 6.6 %collective-permute-start.5 = (bf16[4,2048]{1,0:T(4,128)(2,1)S(1)}, bf16[4,2048]{1,0:T(4,128)(2,1)S(1)}, u32[]{:S(2)}, u32[]{:S(2)}) collective-permute-start(bf16[4,2048]{1,0:T(4,128)(2,1)S(1)} %add_convert_fusion.s0), channel_id=1, source_target_pairs={{0,2},{2,0},{4,6},{6,4},{1,3},{3,1},{5,7},{7,5},{8,10},{10,8},{12,... | collective-permute-start | bytes 49160 | tf_op jit(solution)/shard_map/ppermute | solution.py:35
  16.6 6.5 %collective-permute-start.6 = (bf16[4,2048]{1,0:T(4,128)(2,1)S(1)}, bf16[4,2048]{1,0:T(4,128)(2,1)S(1)}, u32[]{:S(2)}, u32[]{:S(2)}) collective-permute-start(bf16[4,2048]{1,0:T(4,128)(2,1)S(1)} %add_convert_fusion.s0), channel_id=1, source_target_pairs={{0,4},{2,6},{4,0},{6,2},{1,5},{3,7},{5,1},{7,3},{8,12},{10,14},{12... | collective-permute-start | bytes 49160 | tf_op jit(solution)/shard_map/ppermute | solution.py:35
  17.2 5.9 %collective-permute-start.7 = (bf16[4,2048]{1,0:T(4,128)(2,1)S(1)}, bf16[4,2048]{1,0:T(4,128)(2,1)S(1)}, u32[]{:S(2)}, u32[]{:S(2)}) collective-permute-start(bf16[4,2048]{1,0:T(4,128)(2,1)S(1)} %add_convert_fusion.s0), channel_id=1, source_target_pairs={{0,6},{2,4},{4,2},{6,0},{1,7},{3,5},{5,3},{7,1},{8,14},{10,12},{12... | collective-permute-start | bytes 49160 | tf_op jit(solution)/shard_map/ppermute | solution.py:35
  23.4 5.5 %copy-start.6 = (f32[1,64,32,128]{3,2,1,0:T(8,128)S(1)}, f32[1,64,32,128]{3,2,1,0:T(8,128)}, u32[]{:S(2)}) copy-start(f32[1,64,32,128]{3,2,1,0:T(8,128)} %param.34) | copy-start | bytes 3145732
  24.5 5.7 %collective-permute-start.10 = (f32[1,3200]{1,0:T(1,128)S(1)}, f32[1,3200]{1,0:T(1,128)S(1)}, u32[]{:S(2)}, u32[]{:S(2)}) collective-permute-start(f32[1,3200]{1,0:T(1,128)S(1)} %get-tuple-element.28), channel_id=1, source_target_pairs={{0,6},{2,4},{4,2},{6,0},{1,7},{3,5},{5,3},{7,1},{8,14},{10,12},{12... | collective-permute-start | bytes 38408 | tf_op jit(solution)/shard_map/ppermute | solution.py:35
  27.7 3.7 %collective-permute-start.8 = (f32[1,3200]{1,0:T(1,128)S(1)}, f32[1,3200]{1,0:T(1,128)S(1)}, u32[]{:S(2)}, u32[]{:S(2)}) collective-permute-start(f32[1,3200]{1,0:T(1,128)S(1)} %get-tuple-element.26), channel_id=1, source_target_pairs={{0,2},{2,0},{4,6},{6,4},{1,3},{3,1},{5,7},{7,5},{8,10},{10,8},{12,... | collective-permute-start | bytes 38408 | tf_op jit(solution)/shard_map/ppermute | solution.py:35
  27.7 4.6 %collective-permute-start.9 = (f32[1,3200]{1,0:T(1,128)S(1)}, f32[1,3200]{1,0:T(1,128)S(1)}, u32[]{:S(2)}, u32[]{:S(2)}) collective-permute-start(f32[1,3200]{1,0:T(1,128)S(1)} %get-tuple-element.27), channel_id=1, source_target_pairs={{0,4},{2,6},{4,0},{6,2},{1,5},{3,7},{5,1},{7,3},{8,12},{10,14},{12... | collective-permute-start | bytes 38408 | tf_op jit(solution)/shard_map/ppermute | solution.py:35
  29.0 3.3 %copy-start.8 = (bf16[4,2,8,128]{3,2,1,0:T(8,128)(2,1)S(1)}, bf16[4,2,8,128]{3,2,1,0:T(8,128)(2,1)}, u32[]{:S(2)}) copy-start(bf16[4,2,8,128]{3,2,1,0:T(8,128)(2,1)} %param.31) | copy-start | bytes 49156
  32.3 8.2 %copy-start.5 = (bf16[64,32,512]{2,1,0:T(8,128)(2,1)S(1)}, bf16[64,32,512]{2,1,0:T(8,128)(2,1)}, u32[]{:S(2)}) copy-start(bf16[64,32,512]{2,1,0:T(8,128)(2,1)} %param.35) | copy-start | bytes 6291460
  32.9 4.5 %collective-permute-start.11 = (f32[1,2048]{1,0:T(1,128)S(1)}, f32[1,2048]{1,0:T(1,128)S(1)}, u32[]{:S(2)}, u32[]{:S(2)}) collective-permute-start(f32[1,2048]{1,0:T(1,128)S(1)} %shard_map.177.m0), channel_id=1, source_target_pairs={{0,2},{2,0},{4,6},{6,4},{1,3},{3,1},{5,7},{7,5},{8,10},{10,8},{12,... | collective-permute-start | bytes 24584 | tf_op jit(solution)/shard_map/ppermute | solution.py:35
  35.0 4.5 %collective-permute-start.12 = (f32[1,2048]{1,0:T(1,128)S(1)}, f32[1,2048]{1,0:T(1,128)S(1)}, u32[]{:S(2)}, u32[]{:S(2)}) collective-permute-start(f32[1,2048]{1,0:T(1,128)S(1)} %shard_map.177.m0), channel_id=1, source_target_pairs={{0,4},{2,6},{4,0},{6,2},{1,5},{3,7},{5,1},{7,3},{8,12},{10,14},{12... | collective-permute-start | bytes 24584 | tf_op jit(solution)/shard_map/ppermute | solution.py:35
  35.0 5.4 %collective-permute-start.13 = (f32[1,2048]{1,0:T(1,128)S(1)}, f32[1,2048]{1,0:T(1,128)S(1)}, u32[]{:S(2)}, u32[]{:S(2)}) collective-permute-start(f32[1,2048]{1,0:T(1,128)S(1)} %shard_map.177.m0), channel_id=1, source_target_pairs={{0,6},{2,4},{4,2},{6,0},{1,7},{3,5},{5,3},{7,1},{8,14},{10,12},{12... | collective-permute-start | bytes 24584 | tf_op jit(solution)/shard_map/ppermute | solution.py:35
  40.8 2.3 %collective-permute-start.14 = (f32[4,512]{1,0:T(4,128)S(1)}, f32[4,512]{1,0:T(4,128)S(1)}, u32[]{:S(2)}, u32[]{:S(2)}) collective-permute-start(f32[4,512]{1,0:T(4,128)S(1)} %shard_map.178), channel_id=1, source_target_pairs={{0,1},{1,0},{2,3},{3,2},{4,5},{5,4},{6,7},{7,6},{8,9},{9,8},{10,11... | collective-permute-start | bytes 24584 | tf_op jit(solution)/shard_map/ppermute | solution.py:44
  43.1 8.5 %slice-start = ((s8[5767168]{0:T(1024)(128)(4,1)}), s8[4194304]{0:T(1024)(128)(4,1)S(1)}, s32[]{:S(2)}) async-start(s8[5767168]{0:T(1024)(128)(4,1)} %bitcast.28), calls=%async_computation | async-start | bytes 8388608
  43.2 8.5 %slice-start.1 = ((s8[5767168]{0:T(1024)(128)(4,1)}), s8[1572864]{0:T(1024)(128)(4,1)S(1)}, s32[]{:S(2)}) async-start(s8[5767168]{0:T(1024)(128)(4,1)} %bitcast.28), calls=%async_computation.1 | async-start | bytes 3145728
  43.2 6.7 %collective-permute-start.15 = (bf16[4,512]{1,0:T(4,128)(2,1)S(1)}, bf16[4,512]{1,0:T(4,128)(2,1)S(1)}, u32[]{:S(2)}, u32[]{:S(2)}) collective-permute-start(bf16[4,512]{1,0:T(4,128)(2,1)S(1)} %add_convert_fusion.1.s0), channel_id=1, source_target_pairs={{0,2},{2,0},{4,6},{6,4},{1,3},{3,1},{5,7},{7,5},{8,10},{10,8},{12,... | collective-permute-start | bytes 12296 | tf_op jit(solution)/shard_map/ppermute | solution.py:35
  43.3 6.6 %collective-permute-start.16 = (bf16[4,512]{1,0:T(4,128)(2,1)S(1)}, bf16[4,512]{1,0:T(4,128)(2,1)S(1)}, u32[]{:S(2)}, u32[]{:S(2)}) collective-permute-start(bf16[4,512]{1,0:T(4,128)(2,1)S(1)} %add_convert_fusion.1.s0), channel_id=1, source_target_pairs={{0,4},{2,6},{4,0},{6,2},{1,5},{3,7},{5,1},{7,3},{8,12},{10,14},{12... | collective-permute-start | bytes 12296 | tf_op jit(solution)/shard_map/ppermute | solution.py:35
  46.2 5.4 %collective-permute-start.17 = (bf16[4,512]{1,0:T(4,128)(2,1)S(1)}, bf16[4,512]{1,0:T(4,128)(2,1)S(1)}, u32[]{:S(2)}, u32[]{:S(2)}) collective-permute-start(bf16[4,512]{1,0:T(4,128)(2,1)S(1)} %add_convert_fusion.1.s0), channel_id=1, source_target_pairs={{0,6},{2,4},{4,2},{6,0},{1,7},{3,5},{5,3},{7,1},{8,14},{10,12},{12... | collective-permute-start | bytes 12296 | tf_op jit(solution)/shard_map/ppermute | solution.py:35
  53.1 4.4 %collective-permute-start.18 = (f32[4,512]{1,0:T(4,128)S(1)}, f32[4,512]{1,0:T(4,128)S(1)}, u32[]{:S(2)}, u32[]{:S(2)}) collective-permute-start(f32[4,512]{1,0:T(4,128)S(1)} %get-tuple-element.34), channel_id=1, source_target_pairs={{0,2},{2,0},{4,6},{6,4},{1,3},{3,1},{5,7},{7,5},{8,10},{10,8},{12,... | collective-permute-start | bytes 24584 | tf_op jit(solution)/shard_map/ppermute | solution.py:35
  53.1 4.6 %collective-permute-start.19 = (f32[4,512]{1,0:T(4,128)S(1)}, f32[4,512]{1,0:T(4,128)S(1)}, u32[]{:S(2)}, u32[]{:S(2)}) collective-permute-start(f32[4,512]{1,0:T(4,128)S(1)} %get-tuple-element.35), channel_id=1, source_target_pairs={{0,4},{2,6},{4,0},{6,2},{1,5},{3,7},{5,1},{7,3},{8,12},{10,14},{12... | collective-permute-start | bytes 24584 | tf_op jit(solution)/shard_map/ppermute | solution.py:35
  55.1 5.4 %collective-permute-start.20 = (f32[4,512]{1,0:T(4,128)S(1)}, f32[4,512]{1,0:T(4,128)S(1)}, u32[]{:S(2)}, u32[]{:S(2)}) collective-permute-start(f32[4,512]{1,0:T(4,128)S(1)} %get-tuple-element.36), channel_id=1, source_target_pairs={{0,6},{2,4},{4,2},{6,0},{1,7},{3,5},{5,3},{7,1},{8,14},{10,12},{12... | collective-permute-start | bytes 24584 | tf_op jit(solution)/shard_map/ppermute | solution.py:35
  60.5 1.2 %collective-permute-start.21 = (f32[4,256]{1,0:T(4,128)S(1)}, f32[4,256]{1,0:T(4,128)S(1)}, u32[]{:S(2)}, u32[]{:S(2)}) collective-permute-start(f32[4,256]{1,0:T(4,128)S(1)} %constant_dynamic-slice_fusion), channel_id=1, source_target_pairs={{0,1},{1,0},{2,3},{3,2},{4,5},{5,4},{6,7},{7,6},{8,9},{9,8},{10,11... | collective-permute-start | bytes 12296 | tf_op jit(solution)/shard_map/ppermute | solution.py:44
  (8 other events, 17.4 us)

commit v2 on v1

--- a/solution.py
+++ b/solution.py
@@ -42,6 +42,26 @@
 
 def swap_tp(value):
     return lax.ppermute(value, "tp", [(0, 1), (1, 0)])
+
+
+def swap_far(value):
+    pairs = [(2 * c + t, 2 * (c ^ (2 + t)) + t) for c in range(4) for t in range(2)]
+    return lax.ppermute(value, ("kv", "tp"), pairs)
+
+
+def swap_near(value):
+    pairs = [(2 * c + t, 2 * (c ^ 1) + t) for c in range(4) for t in range(2)]
+    return lax.ppermute(value, ("kv", "tp"), pairs)
+
+
+def share_chip(value):
+    far = swap_far(value)
+    near = swap_near(value)
+    return [value, near, far, swap_tp(far)]
+
+
+def peers(here, side):
+    return [jnp.bitwise_xor(here, d) for d in (0, 1, 2 + side, 3 - side)]
 
 
 def in_vmem(value):
@@ -84,11 +104,14 @@
     return (values * scale * gain).astype(BF16)
 
 
+def project(normed, layer, weights):
+    if len(weights.shape) == 3:
+        return dot_nt(normed, weights[layer])
+    return dot_nn(normed, weights[...])
+
+
 def feed(normed, layer, gate, up, down):
-    if len(gate.shape) == 3:
-        gated, upper = dot_nt(normed, gate[layer]), dot_nt(normed, up[layer])
-    else:
-        gated, upper = dot_nn(normed, gate[...]), dot_nn(normed, up[...])
+    gated, upper = project(normed, layer, gate), project(normed, layer, up)
     return dot_nn((silu(gated) * upper).astype(BF16), down[layer])
 
 
@@ -137,6 +160,17 @@
         target[:, rows] = held[rows].T
 
 
+def turn_held_body(layer, source, target):
+    target[...] = source[layer].T
+
+
+def turned_held(source, layer):
+    out = run(
+        functools.partial(turn_held_body, layer), bf16(*source.shape[:0:-1]), (in_vmem(source),)
+    )
+    return in_vmem(out)
+
+
 def turned_layer(source, layer):
     height, wide = source.shape[1:]
     out = run(
@@ -152,13 +186,12 @@
     return in_vmem(out)
 
 
-def first_body(kv, seqs, own, other, gate, up, down, sums_out, rows_out, slabs):
+def first_body(seqs, c0, c1, c2, c3, gate, up, down, sums_out, rows_out, slabs):
     here, side = lax.axis_index("kv"), lax.axis_index("tp")
     width = slabs.shape[2]
-    for d in range(kv):
-        peer = jnp.bitwise_xor(here, d)
-        slabs[2 * peer + side] = own[:, d * width : (d + 1) * width]
-        slabs[2 * peer + 1 - side] = other[:, d * width : (d + 1) * width]
+    for peer, piece, first in zip(peers(here, side), (c0, c1, c2, c3), (side, side, side, 1 - side)):
+        slabs[2 * peer + first] = piece[:, :width]
+        slabs[2 * peer + 1 - first] = piece[:, width:]
     rows = jnp.concatenate([slabs[i] for i in range(slabs.shape[0])], axis=1)
     rows_out[...] = rows
     values = rows.astype(F32)
@@ -266,21 +299,25 @@
     out[...] = sums[:seqs] + first[...] * (1.0 / tp)
 
 
-def second_body(kv, seqs, s0, s1, s2, s3, rows, gate, up, down, *rest):
-    outs, (own_out, slabs, sums_held) = rest[:kv], rest[kv:]
-    here = lax.axis_index("kv")
-    span = slabs.shape[2]
-    for d, piece in enumerate((s0, s1, s2, s3)):
-        slabs[jnp.bitwise_xor(here, d)] = piece[...].astype(F32)
-    second = jnp.concatenate([slabs[i] for i in range(kv)], axis=1)
+def second_body(seqs, s0, s1, s2, s3, rows, gate, up, down, keep, give, own_out, halves, sums_held):
+    here, side = lax.axis_index("kv"), lax.axis_index("tp")
+    count, _, width = halves.shape
+    for peer, piece in zip(peers(here, side), (s0, s1, s2, s3)):
+        piece = piece[...].astype(F32)
+        halves[2 * peer] = piece[:, :width]
+        halves[2 * peer + 1] = piece[:, width:]
+    second = jnp.concatenate([halves[i] for i in range(count)], axis=1)
     padded = jnp.concatenate([second, second], axis=0)
     gain = rows[seqs + 2 : seqs + 3, :].astype(F32)
     sums = feed(normed_rows(padded, gain), 1, gate, up, down)[:seqs]
-    for i in range(kv):
-        sums_held[i] = sums[:, i * span : (i + 1) * span]
-    for d in range(kv):
-        outs[d][...] = sums_held[jnp.bitwise_xor(here, d)]
-    own_out[...] = s0[...].astype(F32)
+    for i in range(count):
+        sums_held[i] = sums[:, i * width : (i + 1) * width]
+    for out, core in ((keep, side), (give, 1 - side)):
+        _, near, far, _ = peers(here, core)
+        picks = (2 * far + core, 2 * far + 1 - core, 2 * near + core, 2 * here + core)
+        for i, pick in enumerate(picks):
+            out[:, i * width : (i + 1) * width] = sums_held[pick]
+    own_out[...] = halves[2 * here + side]
 
 
 def small_mesh(kv, tp, *args):
@@ -331,24 +368,26 @@
         ],
         in_specs=[HBM] * 2,
     )
-    chip = jnp.concatenate(share_kv(pack, kv), axis=1)
-    other = swap_tp(chip)
+    chips = share_chip(jnp.concatenate([pack, swap_tp(pack)], axis=1))
     down = in_vmem(ffn_down)
+    gate_one = turned_held(gate, 0)
+    up_one = turned_held(up, 0)
 
     sums, rows = run(
-        functools.partial(first_body, kv, seqs),
+        functools.partial(first_body, seqs),
         [f32(seqs, model), bf16(2 * seqs, model)],
-        (chip, other, in_vmem(gate), in_vmem(up), down),
+        (*chips, gate_one, up_one, down),
         [pltpu.VMEM((kv * tp, 2 * seqs, width), BF16)],
     )
     sums = (sums + swap_tp(sums)).astype(BF16)
-    sums = share_kv(sums, kv)
+    sums = share_chip(sums)
 
     w_xs, w_zs = turned([jnp.transpose(w, (1, 2, 0)).reshape(local, model) for w in (w_x, w_z)])
+    flat_bc = w_bc.reshape(span, 2 * groups * states)
     w_maps, w_steps, w_join = map(
         in_vmem,
         (
-            w_bc.reshape(span, 2 * groups * states),
+            flat_bc,
             w_dt.T,
             w_out.reshape(flat, span),
         ),
@@ -397,21 +436,20 @@
         (*mixed, w_join, first),
         [pltpu.VMEM((2 * seqs, flat), F32)],
     )
-    second = share_kv((joined + swap_tp(joined)).astype(BF16), kv)
+    second = share_chip((joined + swap_tp(joined)).astype(BF16))
     gate_two = turned_layer(gate, 1)
     up_two = turned_layer(up, 1)
-    *sums, own = run(
-        functools.partial(second_body, kv, seqs),
-        [f32(seqs, span)] * kv + [f32(seqs, span)],
+    keep, give, base = run(
+        functools.partial(second_body, seqs),
+        [f32(seqs, 4 * width), f32(seqs, 4 * width), f32(seqs, width)],
         (*second, rows, gate_two, up_two, down),
-        [pltpu.VMEM((kv, seqs, span), F32), pltpu.VMEM((kv, seqs, span), F32)],
-    )
-    total = sum(swap_kv(sums))
-    side = lax.axis_index("tp")
-    mine = lax.dynamic_slice_in_dim(total, side * width, width, 1)
-    theirs = lax.dynamic_slice_in_dim(total, (1 - side) * width, width, 1)
-    base = lax.dynamic_slice_in_dim(own, side * width, width, 1)
-    return (base + 0.5 * (mine + swap_tp(theirs))).astype(BF16)
+        [pltpu.VMEM((kv * tp, seqs, width), F32), pltpu.VMEM((kv * tp, seqs, width), F32)],
+    )
+    total = keep + swap_tp(give)
+    far = swap_far(total[:, : 2 * width])
+    near = swap_near(total[:, 2 * width : 3 * width])
+    rest = total[:, 3 * width :] + far[:, :width] + near + swap_tp(far[:, width:])
+    return (base + 0.5 * rest).astype(BF16)
 
 
 def normalize(rows, gain):

time: 62.6 us -> 55.5 us (0.89)
  starting transfers between devices: 28.2 us -> 23.6 us
  waiting for transfers between devices: 18.7 us -> 15.1 us
  Pallas kernels: 12.2 us -> 13.5 us
    ppermute x18 -> x6, starting transfers between devices: 28 us -> 8.98 us  [swap_kv(): got[d] = lax.ppermute(values[d], 'kv', [(i, i ^ d) for i in range(kv)])]
    ppermute x0 -> x8, starting transfers between devices: none -> 13.3 us  [the longest x4 7.32 us: swap_far(): return lax.ppermute(value, ('kv', 'tp'), pairs)]
    ppermute x18 -> x6, waiting for transfers between devices: 15.3 us -> 5.02 us  [swap_kv(): got[d] = lax.ppermute(values[d], 'kv', [(i, i ^ d) for i in range(kv)])]
    ppermute x0 -> x8, waiting for transfers between devices: none -> 5.8 us  [the longest x4 3.91 us: swap_far(): return lax.ppermute(value, ('kv', 'tp'), pairs)]
    pallas_call x10 -> x12, Pallas kernels: 12.2 us -> 13.5 us  [run(): pl.pallas_call(body, out_shape=outs, in_specs=in_specs or [VMEM] * len(ar...]
    ppermute x4 -> x8, starting transfers between devices: 0.26 us -> 1.26 us  [swap_tp(): return lax.ppermute(value, 'tp', [(0, 1), (1, 0)])]
    ppermute x4 -> x8, waiting for transfers between devices: 3.38 us -> 4.31 us  [swap_tp(): return lax.ppermute(value, 'tp', [(0, 1), (1, 0)])]
    unnamed x39 -> x43, local copies, waits for them, and re-layouts: 2.11 us -> 1.83 us
  transfers between devices with their start and end apart: 22 -> 22, of which waited for: 12 -> 13; matrix products, arithmetic and copies ran while one was open for 2% -> 2% of each run, Pallas kernels for 9% -> 14%
where the time goes in v2:
time: 55.5 us; the launch traced here: 55.2 us
  starting transfers between devices  23.6 us (43%)
  waiting for transfers between devices  15.1 us (27%)
  Pallas kernels  13.5 us (24%)
  local copies, waits for them, and re-layouts  2.06 us (4%)
  other arithmetic  0.61 us (1%)
    pallas_call x12, Pallas kernels, run(): pl.pallas_call(body, out_shape=outs, in_specs=in_specs or [VMEM] * len(ar...  13.5 us
    ppermute x6, starting transfers between devices, swap_kv(): got[d] = lax.ppermute(values[d], 'kv', [(i, i ^ d) for i in range(kv)])  8.98 us
    ppermute x4, starting transfers between devices, swap_far(): return lax.ppermute(value, ('kv', 'tp'), pairs)  7.32 us
    ppermute x4, starting transfers between devices, swap_near(): return lax.ppermute(value, ('kv', 'tp'), pairs)  6.02 us
    ppermute x6, waiting for transfers between devices, swap_kv(): got[d] = lax.ppermute(values[d], 'kv', [(i, i ^ d) for i in range(kv)])  5.02 us
    ppermute x8, waiting for transfers between devices, swap_tp(): return lax.ppermute(value, 'tp', [(0, 1), (1, 0)])  4.31 us
    ppermute x4, waiting for transfers between devices, swap_far(): return lax.ppermute(value, ('kv', 'tp'), pairs)  3.91 us
    ppermute x4, waiting for transfers between devices, swap_near(): return lax.ppermute(value, ('kv', 'tp'), pairs)  1.89 us
  transfers between devices with their start and end apart: 22, of which 13 were waited for; matrix products, arithmetic and copies ran while one was open for 2% of the time, Pallas kernels for 14%

profile of v2, /device:TPU:0, one launch (start us, length us, event | category | flops | bytes accessed | tf_op | source)
XLA Modules:
  0.0 55.2 jit_solution(12865170438646783529)
XLA Ops:
  0.0 0.9 %shard_map.172 = bf16[8,256]{1,0:T(8,128)(2,1)S(1)} custom-call(bf16[4,256]{1,0:T(4,128)(2,1)} %rows.1, bf16[3,256]{1,0:T(4,128)(2,1)} %gains.1), custom_call_target="tpu_custom_call" | custom-call | flops 10000000000 | tf_op jit(solution)/shard_map/pallas_call | solution.py:76
  1.5 0.8 %collective-permute-done = bf16[8,256]{1,0:T(8,128)(2,1)S(1)} collective-permute-done((bf16[8,256]{1,0:T(8,128)(2,1)S(1)}, bf16[8,256]{1,0:T(8,128)(2,1)S(1)}, u32[]{:S(2)}, u32[]{:S(2)}) %collective-permute-start) | collective-permute-done | bytes 4128 | tf_op jit(solution)/shard_map/ppermute | solution.py:44
  2.3 3.9 %collective-permute-start.2 = (bf16[8,512]{1,0:T(8,128)(2,1)S(1)}, bf16[8,512]{1,0:T(8,128)(2,1)S(1)}, u32[]{:S(2)}, u32[]{:S(2)}) collective-permute-start(bf16[8,512]{1,0:T(8,128)(2,1)S(1)} %pad_maximum_fusion.c0), channel_id=1, source_target_pairs={{0,4},{1,7},{2,6},{3,5},{4,0},{5,3},{6,2},{7,1},{8,12},{9,15},{10,... | collective-permute-start | bytes 24584 | tf_op jit(solution)/shard_map/ppermute | solution.py:49
  6.2 0.9 %shard_map.173.gate = bf16[2048,704]{1,0:T(8,128)(2,1)S(1)} custom-call(bf16[2,704,2048]{2,1,0:T(8,128)(2,1)S(1)} %bitcast.25), custom_call_target="tpu_custom_call" | custom-call | flops 10000000000 | tf_op jit(solution)/shard_map/pallas_call | solution.py:76
  7.1 1.6 %collective-permute-start.1 = (bf16[8,512]{1,0:T(8,128)(2,1)S(1)}, bf16[8,512]{1,0:T(8,128)(2,1)S(1)}, u32[]{:S(2)}, u32[]{:S(2)}) collective-permute-start(bf16[8,512]{1,0:T(8,128)(2,1)S(1)} %pad_maximum_fusion.c0), channel_id=1, source_target_pairs={{0,2},{1,3},{2,0},{3,1},{4,6},{5,7},{6,4},{7,5},{8,10},{9,11},{10,... | collective-permute-start | bytes 24584 | tf_op jit(solution)/shard_map/ppermute | solution.py:54
  8.8 0.9 %shard_map.174.up = bf16[2048,704]{1,0:T(8,128)(2,1)S(1)} custom-call(bf16[2,704,2048]{2,1,0:T(8,128)(2,1)S(1)} %bitcast.29), custom_call_target="tpu_custom_call" | custom-call | flops 10000000000 | tf_op jit(solution)/shard_map/pallas_call | solution.py:76
  9.7 1.1 %collective-permute-done.1.c1 = bf16[8,512]{1,0:T(8,128)(2,1)S(1)} collective-permute-done((bf16[8,512]{1,0:T(8,128)(2,1)S(1)}, bf16[8,512]{1,0:T(8,128)(2,1)S(1)}, u32[]{:S(2)}, u32[]{:S(2)}) %collective-permute-start.1) | collective-permute-done | bytes 8224 | tf_op jit(solution)/shard_map/ppermute | solution.py:54
  10.9 1.4 %shard_map.175 = (f32[4,2048]{1,0:T(4,128)S(1)}, bf16[8,2048]{1,0:T(8,128)(2,1)S(1)}) custom-call(bf16[8,512]{1,0:T(8,128)(2,1)S(1)} %pad_maximum_fusion.c0, bf16[8,512]{1,0:T(8,128)(2,1)S(1)} %collective-permute-done.1.c1, bf16[8,512]{1,0:T(8,128)(2,1)S(1)} %collective-permute-done.2.c2, bf16[8,512]{1,0:T(8,128)(2,1)S(1)} %collective-permute-done.3.c3, ...), custom_call_target="tpu_custom_call" | custom-call | flops 10000000000 | tf_op jit(solution)/shard_map/pallas_call | solution.py:76
  12.4 1.2 %collective-permute-done.4 = f32[4,2048]{1,0:T(4,128)S(1)} collective-permute-done((f32[4,2048]{1,0:T(4,128)S(1)}, f32[4,2048]{1,0:T(4,128)S(1)}, u32[]{:S(2)}, u32[]{:S(2)}) %collective-permute-start.4) | collective-permute-done | bytes 32800 | tf_op jit(solution)/shard_map/ppermute | solution.py:44
  13.5 1.1 %collective-permute-start.6 = (bf16[4,2048]{1,0:T(4,128)(2,1)S(1)}, bf16[4,2048]{1,0:T(4,128)(2,1)S(1)}, u32[]{:S(2)}, u32[]{:S(2)}) collective-permute-start(bf16[4,2048]{1,0:T(4,128)(2,1)S(1)} %add_convert_fusion.s0), channel_id=1, source_target_pairs={{0,4},{1,7},{2,6},{3,5},{4,0},{5,3},{6,2},{7,1},{8,12},{9,15},{10,... | collective-permute-start | bytes 49160 | tf_op jit(solution)/shard_map/ppermute | solution.py:49
  14.7 1.6 %collective-permute-start.5 = (bf16[4,2048]{1,0:T(4,128)(2,1)S(1)}, bf16[4,2048]{1,0:T(4,128)(2,1)S(1)}, u32[]{:S(2)}, u32[]{:S(2)}) collective-permute-start(bf16[4,2048]{1,0:T(4,128)(2,1)S(1)} %add_convert_fusion.s0), channel_id=1, source_target_pairs={{0,2},{1,3},{2,0},{3,1},{4,6},{5,7},{6,4},{7,5},{8,10},{9,11},{10,... | collective-permute-start | bytes 49160 | tf_op jit(solution)/shard_map/ppermute | solution.py:54
  16.2 2.0 %collective-permute-done.6.s2 = bf16[4,2048]{1,0:T(4,128)(2,1)S(1)} collective-permute-done((bf16[4,2048]{1,0:T(4,128)(2,1)S(1)}, bf16[4,2048]{1,0:T(4,128)(2,1)S(1)}, u32[]{:S(2)}, u32[]{:S(2)}) %collective-permute-start.6) | collective-permute-done | bytes 16416 | tf_op jit(solution)/shard_map/ppermute | solution.py:49
  18.3 1.1 %shard_map.176 = (bf16[2048,512]{1,0:T(8,128)(2,1)S(1)}, bf16[2048,512]{1,0:T(8,128)(2,1)S(1)}) custom-call(bf16[512,2048]{1,0:T(8,128)(2,1)S(1)} %bitcast.34, bf16[512,2048]{1,0:T(8,128)(2,1)S(1)} %bitcast.35), custom_call_target="tpu_custom_call" | custom-call | flops 10000000000 | tf_op jit(solution)/shard_map/pallas_call | solution.py:76
  20.4 1.1 %shard_map.177 = (f32[1,3200]{1,0:T(1,128)S(1)}, f32[1,3200]{1,0:T(1,128)S(1)}, f32[1,3200]{1,0:T(1,128)S(1)}, f32[1,3200]{1,0:T(1,128)S(1)}, f32[4,512]{1,0:T(4,128)S(1)}) custom-call(bf16[4,2048]{1,0:T(4,128)(2,1)S(1)} %add_convert_fusion.s0, bf16[4,2048]{1,0:T(4,128)(2,1)S(1)} %collective-permute-done.5.s1, ...), custom_call_target="tpu_custom_call" | custom-call | flops 10000000000 | tf_op jit(solution)/shard_map/pallas_call | solution.py:76
  21.5 2.4 %collective-permute-start.10 = (f32[1,3200]{1,0:T(1,128)S(1)}, f32[1,3200]{1,0:T(1,128)S(1)}, u32[]{:S(2)}, u32[]{:S(2)}) collective-permute-start(f32[1,3200]{1,0:T(1,128)S(1)} %get-tuple-element.26), channel_id=1, source_target_pairs={{0,6},{2,4},{4,2},{6,0},{1,7},{3,5},{5,3},{7,1},{8,14},{10,12},{12... | collective-permute-start | bytes 38408 | tf_op jit(solution)/shard_map/ppermute | solution.py:35
  23.9 2.1 %collective-permute-start.9 = (f32[1,3200]{1,0:T(1,128)S(1)}, f32[1,3200]{1,0:T(1,128)S(1)}, u32[]{:S(2)}, u32[]{:S(2)}) collective-permute-start(f32[1,3200]{1,0:T(1,128)S(1)} %get-tuple-element.25), channel_id=1, source_target_pairs={{0,4},{2,6},{4,0},{6,2},{1,5},{3,7},{5,1},{7,3},{8,12},{10,14},{12... | collective-permute-start | bytes 38408 | tf_op jit(solution)/shard_map/ppermute | solution.py:35
  27.6 0.9 %collective-permute-done.9.p2 = f32[1,3200]{1,0:T(1,128)S(1)} collective-permute-done((f32[1,3200]{1,0:T(1,128)S(1)}, f32[1,3200]{1,0:T(1,128)S(1)}, u32[]{:S(2)}, u32[]{:S(2)}) %collective-permute-start.9) | collective-permute-done | bytes 12832 | tf_op jit(solution)/shard_map/ppermute | solution.py:35
  29.1 2.1 %collective-permute-start.11 = (f32[1,2048]{1,0:T(1,128)S(1)}, f32[1,2048]{1,0:T(1,128)S(1)}, u32[]{:S(2)}, u32[]{:S(2)}) collective-permute-start(f32[1,2048]{1,0:T(1,128)S(1)} %shard_map.179.m0), channel_id=1, source_target_pairs={{0,2},{2,0},{4,6},{6,4},{1,3},{3,1},{5,7},{7,5},{8,10},{10,8},{12,... | collective-permute-start | bytes 24584 | tf_op jit(solution)/shard_map/ppermute | solution.py:35
  31.2 0.7 %collective-permute-start.12 = (f32[1,2048]{1,0:T(1,128)S(1)}, f32[1,2048]{1,0:T(1,128)S(1)}, u32[]{:S(2)}, u32[]{:S(2)}) collective-permute-start(f32[1,2048]{1,0:T(1,128)S(1)} %shard_map.179.m0), channel_id=1, source_target_pairs={{0,4},{2,6},{4,0},{6,2},{1,5},{3,7},{5,1},{7,3},{8,12},{10,14},{12... | collective-permute-start | bytes 24584 | tf_op jit(solution)/shard_map/ppermute | solution.py:35
  31.9 1.7 %collective-permute-start.13 = (f32[1,2048]{1,0:T(1,128)S(1)}, f32[1,2048]{1,0:T(1,128)S(1)}, u32[]{:S(2)}, u32[]{:S(2)}) collective-permute-start(f32[1,2048]{1,0:T(1,128)S(1)} %shard_map.179.m0), channel_id=1, source_target_pairs={{0,6},{2,4},{4,2},{6,0},{1,7},{3,5},{5,3},{7,1},{8,14},{10,12},{12... | collective-permute-start | bytes 24584 | tf_op jit(solution)/shard_map/ppermute | solution.py:35
  33.7 2.1 %collective-permute-done.12.m2 = f32[1,2048]{1,0:T(1,128)S(1)} collective-permute-done((f32[1,2048]{1,0:T(1,128)S(1)}, f32[1,2048]{1,0:T(1,128)S(1)}, u32[]{:S(2)}, u32[]{:S(2)}) %collective-permute-start.12) | collective-permute-done | bytes 8224 | tf_op jit(solution)/shard_map/ppermute | solution.py:35
  35.8 1.6 %collective-permute-done.13.m3 = f32[1,2048]{1,0:T(1,128)S(1)} collective-permute-done((f32[1,2048]{1,0:T(1,128)S(1)}, f32[1,2048]{1,0:T(1,128)S(1)}, u32[]{:S(2)}, u32[]{:S(2)}) %collective-permute-start.13) | collective-permute-done | bytes 8224 | tf_op jit(solution)/shard_map/ppermute | solution.py:35
  37.8 1.2 %collective-permute-done.14 = f32[4,512]{1,0:T(4,128)S(1)} collective-permute-done((f32[4,512]{1,0:T(4,128)S(1)}, f32[4,512]{1,0:T(4,128)S(1)}, u32[]{:S(2)}, u32[]{:S(2)}) %collective-permute-start.14) | collective-permute-done | bytes 8224 | tf_op jit(solution)/shard_map/ppermute | solution.py:44
  39.4 2.4 %shard_map.181.gate = bf16[2048,704]{1,0:T(8,128)(2,1)S(1)} custom-call(bf16[2,704,2048]{2,1,0:T(8,128)(2,1)} %bitcast.24), custom_call_target="tpu_custom_call" | custom-call | flops 10000000000 | tf_op jit(solution)/shard_map/pallas_call | solution.py:76
  41.8 1.9 %collective-permute-start.15 = (bf16[4,512]{1,0:T(4,128)(2,1)S(1)}, bf16[4,512]{1,0:T(4,128)(2,1)S(1)}, u32[]{:S(2)}, u32[]{:S(2)}) collective-permute-start(bf16[4,512]{1,0:T(4,128)(2,1)S(1)} %add_convert_fusion.1.s0), channel_id=1, source_target_pairs={{0,2},{1,3},{2,0},{3,1},{4,6},{5,7},{6,4},{7,5},{8,10},{9,11},{10,... | collective-permute-start | bytes 12296 | tf_op jit(solution)/shard_map/ppermute | solution.py:54
  43.7 2.2 %shard_map.182.up = bf16[2048,704]{1,0:T(8,128)(2,1)S(1)} custom-call(bf16[2,704,2048]{2,1,0:T(8,128)(2,1)} %bitcast.26), custom_call_target="tpu_custom_call" | custom-call | flops 10000000000 | tf_op jit(solution)/shard_map/pallas_call | solution.py:76
  46.0 1.4 %shard_map.183 = (f32[4,1024]{1,0:T(4,128)S(1)}, f32[4,1024]{1,0:T(4,128)S(1)}, f32[4,256]{1,0:T(4,128)S(1)}) custom-call(bf16[4,512]{1,0:T(4,128)(2,1)S(1)} %add_convert_fusion.1.s0, bf16[4,512]{1,0:T(4,128)(2,1)S(1)} %collective-permute-done.15.s1, bf16[4,512]{1,0:T(4,128)(2,1)S(1)} %collective-permute-done.16.s2, ...), custom_call_target="tpu_custom_call" | custom-call | flops 10000000000 | tf_op jit(solution)/shard_map/pallas_call | solution.py:76
  48.0 0.8 %collective-permute-done.18 = f32[4,1024]{1,0:T(4,128)S(1)} collective-permute-done((f32[4,1024]{1,0:T(4,128)S(1)}, f32[4,1024]{1,0:T(4,128)S(1)}, u32[]{:S(2)}, u32[]{:S(2)}) %collective-permute-start.18) | collective-permute-done | bytes 16416 | tf_op jit(solution)/shard_map/ppermute | solution.py:44
  48.8 1.8 %collective-permute-start.19 = (f32[4,512]{1,0:T(4,128)S(1)}, f32[4,512]{1,0:T(4,128)S(1)}, u32[]{:S(2)}, u32[]{:S(2)}) collective-permute-start(f32[4,512]{1,0:T(4,128)S(1)} %slice.21), channel_id=1, source_target_pairs={{0,4},{1,7},{2,6},{3,5},{4,0},{5,3},{6,2},{7,1},{8,12},{9,15},{10,... | collective-permute-start | bytes 24584 | tf_op jit(solution)/shard_map/ppermute | solution.py:49
  50.7 0.9 %collective-permute-start.20 = (f32[4,256]{1,0:T(4,128)S(1)}, f32[4,256]{1,0:T(4,128)S(1)}, u32[]{:S(2)}, u32[]{:S(2)}) collective-permute-start(f32[4,256]{1,0:T(4,128)S(1)} %slice.23), channel_id=1, source_target_pairs={{0,2},{1,3},{2,0},{3,1},{4,6},{5,7},{6,4},{7,5},{8,10},{9,11},{10,... | collective-permute-start | bytes 12296 | tf_op jit(solution)/shard_map/ppermute | solution.py:54
  51.6 1.9 %collective-permute-done.19 = f32[4,512]{1,0:T(4,128)S(1)} collective-permute-done((f32[4,512]{1,0:T(4,128)S(1)}, f32[4,512]{1,0:T(4,128)S(1)}, u32[]{:S(2)}, u32[]{:S(2)}) %collective-permute-start.19) | collective-permute-done | bytes 8224 | tf_op jit(solution)/shard_map/ppermute | solution.py:49
  53.6 0.7 %collective-permute-done.20 = f32[4,256]{1,0:T(4,128)S(1)} collective-permute-done((f32[4,256]{1,0:T(4,128)S(1)}, f32[4,256]{1,0:T(4,128)S(1)}, u32[]{:S(2)}, u32[]{:S(2)}) %collective-permute-start.20) | collective-permute-done | bytes 4128 | tf_op jit(solution)/shard_map/ppermute | solution.py:54
  (80 shorter events, 6.2 us)
Async XLA Ops:
  0.0 6.2 %copy-start = (bf16[2,2048,704]{1,2,0:T(8,128)(2,1)S(1)}, bf16[2,2048,704]{1,2,0:T(8,128)(2,1)}, u32[]{:S(2)}) copy-start(bf16[2,2048,704]{1,2,0:T(8,128)(2,1)} %param.20) | copy-start | bytes 17301508
  0.0 8.8 %slice-start = ((s8[5767168]{0:T(1024)(128)(4,1)}), s8[4194304]{0:T(1024)(128)(4,1)S(1)}, s32[]{:S(2)}) async-start(s8[5767168]{0:T(1024)(128)(4,1)} %bitcast.27), calls=%async_computation | async-start | bytes 8388608
  0.9 7.9 %slice-start.1 = ((s8[5767168]{0:T(1024)(128)(4,1)}), s8[1572864]{0:T(1024)(128)(4,1)S(1)}, s32[]{:S(2)}) async-start(s8[5767168]{0:T(1024)(128)(4,1)} %bitcast.27), calls=%async_computation.1 | async-start | bytes 3145728
  0.9 1.4 %collective-permute-start = (bf16[8,256]{1,0:T(8,128)(2,1)S(1)}, bf16[8,256]{1,0:T(8,128)(2,1)S(1)}, u32[]{:S(2)}, u32[]{:S(2)}) collective-permute-start(bf16[8,256]{1,0:T(8,128)(2,1)S(1)} %shard_map.172), channel_id=1, source_target_pairs={{0,1},{1,0},{2,3},{3,2},{4,5},{5,4},{6,7},{7,6},{8,9},{9,8},{10,11... | collective-permute-start | bytes 12296 | tf_op jit(solution)/shard_map/ppermute | solution.py:44
  2.3 6.5 %collective-permute-start.2 = (bf16[8,512]{1,0:T(8,128)(2,1)S(1)}, bf16[8,512]{1,0:T(8,128)(2,1)S(1)}, u32[]{:S(2)}, u32[]{:S(2)}) collective-permute-start(bf16[8,512]{1,0:T(8,128)(2,1)S(1)} %pad_maximum_fusion.c0), channel_id=1, source_target_pairs={{0,4},{1,7},{2,6},{3,5},{4,0},{5,3},{6,2},{7,1},{8,12},{9,15},{10,... | collective-permute-start | bytes 24584 | tf_op jit(solution)/shard_map/ppermute | solution.py:49
  6.2 4.6 %slice-start.2 = ((s8[5767168]{0:T(1024)(128)(4,1)}), s8[4194304]{0:T(1024)(128)(4,1)S(1)}, s32[]{:S(2)}) async-start(s8[5767168]{0:T(1024)(128)(4,1)} %bitcast.30), calls=%async_computation.2 | async-start | bytes 8388608
  7.1 3.7 %collective-permute-start.1 = (bf16[8,512]{1,0:T(8,128)(2,1)S(1)}, bf16[8,512]{1,0:T(8,128)(2,1)S(1)}, u32[]{:S(2)}, u32[]{:S(2)}) collective-permute-start(bf16[8,512]{1,0:T(8,128)(2,1)S(1)} %pad_maximum_fusion.c0), channel_id=1, source_target_pairs={{0,2},{1,3},{2,0},{3,1},{4,6},{5,7},{6,4},{7,5},{8,10},{9,11},{10,... | collective-permute-start | bytes 24584 | tf_op jit(solution)/shard_map/ppermute | solution.py:54
  8.8 2.1 %collective-permute-start.3 = (bf16[8,512]{1,0:T(8,128)(2,1)S(1)}, bf16[8,512]{1,0:T(8,128)(2,1)S(1)}, u32[]{:S(2)}, u32[]{:S(2)}) collective-permute-start(bf16[8,512]{1,0:T(8,128)(2,1)S(1)} %collective-permute-done.2.c2), channel_id=1, source_target_pairs={{0,1},{1,0},{2,3},{3,2},{4,5},{5,4},{6,7},{7,6},{8,9},{9,8},{10,11... | collective-permute-start | bytes 24584 | tf_op jit(solution)/shard_map/ppermute | solution.py:44
  9.7 8.6 %copy-start.1 = (bf16[2048,16,32]{0,2,1:T(8,128)(2,1)S(1)}, bf16[2048,16,32]{0,2,1:T(8,128)(2,1)}, u32[]{:S(2)}) copy-start(bf16[2048,16,32]{0,2,1:T(8,128)(2,1)} %param.23) | copy-start | bytes 6291460
  9.7 8.6 %copy-start.2 = (bf16[2048,16,32]{0,2,1:T(8,128)(2,1)S(1)}, bf16[2048,16,32]{0,2,1:T(8,128)(2,1)}, u32[]{:S(2)}) copy-start(bf16[2048,16,32]{0,2,1:T(8,128)(2,1)} %param.24) | copy-start | bytes 6291460
  12.3 1.2 %collective-permute-start.4 = (f32[4,2048]{1,0:T(4,128)S(1)}, f32[4,2048]{1,0:T(4,128)S(1)}, u32[]{:S(2)}, u32[]{:S(2)}) collective-permute-start(f32[4,2048]{1,0:T(4,128)S(1)} %get-tuple-element.19), channel_id=1, source_target_pairs={{0,1},{1,0},{2,3},{3,2},{4,5},{5,4},{6,7},{7,6},{8,9},{9,8},{10,11... | collective-permute-start | bytes 98312 | tf_op jit(solution)/shard_map/ppermute | solution.py:44
  13.5 4.7 %collective-permute-start.6 = (bf16[4,2048]{1,0:T(4,128)(2,1)S(1)}, bf16[4,2048]{1,0:T(4,128)(2,1)S(1)}, u32[]{:S(2)}, u32[]{:S(2)}) collective-permute-start(bf16[4,2048]{1,0:T(4,128)(2,1)S(1)} %add_convert_fusion.s0), channel_id=1, source_target_pairs={{0,4},{1,7},{2,6},{3,5},{4,0},{5,3},{6,2},{7,1},{8,12},{9,15},{10,... | collective-permute-start | bytes 49160 | tf_op jit(solution)/shard_map/ppermute | solution.py:49
  14.7 5.7 %collective-permute-start.5 = (bf16[4,2048]{1,0:T(4,128)(2,1)S(1)}, bf16[4,2048]{1,0:T(4,128)(2,1)S(1)}, u32[]{:S(2)}, u32[]{:S(2)}) collective-permute-start(bf16[4,2048]{1,0:T(4,128)(2,1)S(1)} %add_convert_fusion.s0), channel_id=1, source_target_pairs={{0,2},{1,3},{2,0},{3,1},{4,6},{5,7},{6,4},{7,5},{8,10},{9,11},{10,... | collective-permute-start | bytes 49160 | tf_op jit(solution)/shard_map/ppermute | solution.py:54
  18.2 2.2 %collective-permute-start.7 = (bf16[4,2048]{1,0:T(4,128)(2,1)S(1)}, bf16[4,2048]{1,0:T(4,128)(2,1)S(1)}, u32[]{:S(2)}, u32[]{:S(2)}) collective-permute-start(bf16[4,2048]{1,0:T(4,128)(2,1)S(1)} %collective-permute-done.6.s2), channel_id=1, source_target_pairs={{0,1},{1,0},{2,3},{3,2},{4,5},{5,4},{6,7},{7,6},{8,9},{9,8},{10,11... | collective-permute-start | bytes 49160 | tf_op jit(solution)/shard_map/ppermute | solution.py:44
  20.4 5.5 %copy-start.4 = (f32[1,64,32,128]{3,2,1,0:T(8,128)S(1)}, f32[1,64,32,128]{3,2,1,0:T(8,128)}, u32[]{:S(2)}) copy-start(f32[1,64,32,128]{3,2,1,0:T(8,128)} %param.34) | copy-start | bytes 3145732
  21.5 5.7 %collective-permute-start.10 = (f32[1,3200]{1,0:T(1,128)S(1)}, f32[1,3200]{1,0:T(1,128)S(1)}, u32[]{:S(2)}, u32[]{:S(2)}) collective-permute-start(f32[1,3200]{1,0:T(1,128)S(1)} %get-tuple-element.26), channel_id=1, source_target_pairs={{0,6},{2,4},{4,2},{6,0},{1,7},{3,5},{5,3},{7,1},{8,14},{10,12},{12... | collective-permute-start | bytes 38408 | tf_op jit(solution)/shard_map/ppermute | solution.py:35
  23.9 3.7 %collective-permute-start.8 = (f32[1,3200]{1,0:T(1,128)S(1)}, f32[1,3200]{1,0:T(1,128)S(1)}, u32[]{:S(2)}, u32[]{:S(2)}) collective-permute-start(f32[1,3200]{1,0:T(1,128)S(1)} %get-tuple-element.24), channel_id=1, source_target_pairs={{0,2},{2,0},{4,6},{6,4},{1,3},{3,1},{5,7},{7,5},{8,10},{10,8},{12,... | collective-permute-start | bytes 38408 | tf_op jit(solution)/shard_map/ppermute | solution.py:35
  23.9 4.6 %collective-permute-start.9 = (f32[1,3200]{1,0:T(1,128)S(1)}, f32[1,3200]{1,0:T(1,128)S(1)}, u32[]{:S(2)}, u32[]{:S(2)}) collective-permute-start(f32[1,3200]{1,0:T(1,128)S(1)} %get-tuple-element.25), channel_id=1, source_target_pairs={{0,4},{2,6},{4,0},{6,2},{1,5},{3,7},{5,1},{7,3},{8,12},{10,14},{12... | collective-permute-start | bytes 38408 | tf_op jit(solution)/shard_map/ppermute | solution.py:35
  28.5 8.9 %copy-start.3 = (bf16[64,32,512]{2,1,0:T(8,128)(2,1)S(1)}, bf16[64,32,512]{2,1,0:T(8,128)(2,1)}, u32[]{:S(2)}) copy-start(bf16[64,32,512]{2,1,0:T(8,128)(2,1)} %param.35) | copy-start | bytes 6291460
  29.1 4.5 %collective-permute-start.11 = (f32[1,2048]{1,0:T(1,128)S(1)}, f32[1,2048]{1,0:T(1,128)S(1)}, u32[]{:S(2)}, u32[]{:S(2)}) collective-permute-start(f32[1,2048]{1,0:T(1,128)S(1)} %shard_map.179.m0), channel_id=1, source_target_pairs={{0,2},{2,0},{4,6},{6,4},{1,3},{3,1},{5,7},{7,5},{8,10},{10,8},{12,... | collective-permute-start | bytes 24584 | tf_op jit(solution)/shard_map/ppermute | solution.py:35
  31.2 4.5 %collective-permute-start.12 = (f32[1,2048]{1,0:T(1,128)S(1)}, f32[1,2048]{1,0:T(1,128)S(1)}, u32[]{:S(2)}, u32[]{:S(2)}) collective-permute-start(f32[1,2048]{1,0:T(1,128)S(1)} %shard_map.179.m0), channel_id=1, source_target_pairs={{0,4},{2,6},{4,0},{6,2},{1,5},{3,7},{5,1},{7,3},{8,12},{10,14},{12... | collective-permute-start | bytes 24584 | tf_op jit(solution)/shard_map/ppermute | solution.py:35
  31.9 5.4 %collective-permute-start.13 = (f32[1,2048]{1,0:T(1,128)S(1)}, f32[1,2048]{1,0:T(1,128)S(1)}, u32[]{:S(2)}, u32[]{:S(2)}) collective-permute-start(f32[1,2048]{1,0:T(1,128)S(1)} %shard_map.179.m0), channel_id=1, source_target_pairs={{0,6},{2,4},{4,2},{6,0},{1,7},{3,5},{5,3},{7,1},{8,14},{10,12},{12... | collective-permute-start | bytes 24584 | tf_op jit(solution)/shard_map/ppermute | solution.py:35
  37.8 1.2 %collective-permute-start.14 = (f32[4,512]{1,0:T(4,128)S(1)}, f32[4,512]{1,0:T(4,128)S(1)}, u32[]{:S(2)}, u32[]{:S(2)}) collective-permute-start(f32[4,512]{1,0:T(4,128)S(1)} %shard_map.180), channel_id=1, source_target_pairs={{0,1},{1,0},{2,3},{3,2},{4,5},{5,4},{6,7},{7,6},{8,9},{9,8},{10,11... | collective-permute-start | bytes 24584 | tf_op jit(solution)/shard_map/ppermute | solution.py:44
  39.0 4.8 %collective-permute-start.16 = (bf16[4,512]{1,0:T(4,128)(2,1)S(1)}, bf16[4,512]{1,0:T(4,128)(2,1)S(1)}, u32[]{:S(2)}, u32[]{:S(2)}) collective-permute-start(bf16[4,512]{1,0:T(4,128)(2,1)S(1)} %add_convert_fusion.1.s0), channel_id=1, source_target_pairs={{0,4},{1,7},{2,6},{3,5},{4,0},{5,3},{6,2},{7,1},{8,12},{9,15},{10,... | collective-permute-start | bytes 12296 | tf_op jit(solution)/shard_map/ppermute | solution.py:49
  39.4 6.6 %slice-start.4 = ((s8[5767168]{0:T(1024)(128)(4,1)}), s8[4194304]{0:T(1024)(128)(4,1)S(1)}, s32[]{:S(2)}) async-start(s8[5767168]{0:T(1024)(128)(4,1)} %bitcast.32), calls=%async_computation.4 | async-start | bytes 8388608
  41.8 4.2 %slice-start.5 = ((s8[5767168]{0:T(1024)(128)(4,1)}), s8[1572864]{0:T(1024)(128)(4,1)S(1)}, s32[]{:S(2)}) async-start(s8[5767168]{0:T(1024)(128)(4,1)} %bitcast.32), calls=%async_computation.5 | async-start | bytes 3145728
  41.8 4.2 %collective-permute-start.15 = (bf16[4,512]{1,0:T(4,128)(2,1)S(1)}, bf16[4,512]{1,0:T(4,128)(2,1)S(1)}, u32[]{:S(2)}, u32[]{:S(2)}) collective-permute-start(bf16[4,512]{1,0:T(4,128)(2,1)S(1)} %add_convert_fusion.1.s0), channel_id=1, source_target_pairs={{0,2},{1,3},{2,0},{3,1},{4,6},{5,7},{6,4},{7,5},{8,10},{9,11},{10,... | collective-permute-start | bytes 12296 | tf_op jit(solution)/shard_map/ppermute | solution.py:54
  43.7 2.3 %collective-permute-start.17 = (bf16[4,512]{1,0:T(4,128)(2,1)S(1)}, bf16[4,512]{1,0:T(4,128)(2,1)S(1)}, u32[]{:S(2)}, u32[]{:S(2)}) collective-permute-start(bf16[4,512]{1,0:T(4,128)(2,1)S(1)} %collective-permute-done.16.s2), channel_id=1, source_target_pairs={{0,1},{1,0},{2,3},{3,2},{4,5},{5,4},{6,7},{7,6},{8,9},{9,8},{10,11... | collective-permute-start | bytes 12296 | tf_op jit(solution)/shard_map/ppermute | solution.py:44
  47.5 1.4 %collective-permute-start.18 = (f32[4,1024]{1,0:T(4,128)S(1)}, f32[4,1024]{1,0:T(4,128)S(1)}, u32[]{:S(2)}, u32[]{:S(2)}) collective-permute-start(f32[4,1024]{1,0:T(4,128)S(1)} %get-tuple-element.32), channel_id=1, source_target_pairs={{0,1},{1,0},{2,3},{3,2},{4,5},{5,4},{6,7},{7,6},{8,9},{9,8},{10,11... | collective-permute-start | bytes 49160 | tf_op jit(solution)/shard_map/ppermute | solution.py:44
  48.8 4.6 %collective-permute-start.19 = (f32[4,512]{1,0:T(4,128)S(1)}, f32[4,512]{1,0:T(4,128)S(1)}, u32[]{:S(2)}, u32[]{:S(2)}) collective-permute-start(f32[4,512]{1,0:T(4,128)S(1)} %slice.21), channel_id=1, source_target_pairs={{0,4},{1,7},{2,6},{3,5},{4,0},{5,3},{6,2},{7,1},{8,12},{9,15},{10,... | collective-permute-start | bytes 24584 | tf_op jit(solution)/shard_map/ppermute | solution.py:49
  50.7 3.6 %collective-permute-start.20 = (f32[4,256]{1,0:T(4,128)S(1)}, f32[4,256]{1,0:T(4,128)S(1)}, u32[]{:S(2)}, u32[]{:S(2)}) collective-permute-start(f32[4,256]{1,0:T(4,128)S(1)} %slice.23), channel_id=1, source_target_pairs={{0,2},{1,3},{2,0},{3,1},{4,6},{5,7},{6,4},{7,5},{8,10},{9,11},{10,... | collective-permute-start | bytes 12296 | tf_op jit(solution)/shard_map/ppermute | solution.py:54
  53.5 1.2 %collective-permute-start.21 = (f32[4,256]{1,0:T(4,128)S(1)}, f32[4,256]{1,0:T(4,128)S(1)}, u32[]{:S(2)}, u32[]{:S(2)}) collective-permute-start(f32[4,256]{1,0:T(4,128)S(1)} %slice.24), channel_id=1, source_target_pairs={{0,1},{1,0},{2,3},{3,2},{4,5},{5,4},{6,7},{7,6},{8,9},{9,8},{10,11... | collective-permute-start | bytes 12296 | tf_op jit(solution)/shard_map/ppermute | solution.py:44
  (10 other events, 20.6 us)

commit v3 on v2

--- a/solution.py
+++ b/solution.py
@@ -101,7 +101,7 @@
 
 def normed_rows(values, gain):
     scale = lax.rsqrt(jnp.mean(values * values, axis=1, keepdims=True) + EPS)
-    return (values * scale * gain).astype(BF16)
+    return (values * gain).astype(BF16), scale
 
 
 def project(normed, layer, weights):
@@ -110,8 +110,8 @@
     return dot_nn(normed, weights[...])
 
 
-def feed(normed, layer, gate, up, down):
-    gated, upper = project(normed, layer, gate), project(normed, layer, up)
+def feed(normed, scale, layer, gate, up, down):
+    gated, upper = project(normed, layer, gate) * scale, project(normed, layer, up) * scale
     return dot_nn((silu(gated) * upper).astype(BF16), down[layer])
 
 
@@ -195,7 +195,7 @@
     rows = jnp.concatenate([slabs[i] for i in range(slabs.shape[0])], axis=1)
     rows_out[...] = rows
     values = rows.astype(F32)
-    sums = feed(normed_rows(values, values[seqs : seqs + 1]), 0, gate, up, down)
+    sums = feed(*normed_rows(values, values[seqs : seqs + 1]), 0, gate, up, down)
     sums_out[...] = sums[:seqs]
 
 
@@ -207,16 +207,16 @@
     known = rows[...].astype(F32)
     first = (known[:seqs] + 0.5 * total).astype(BF16).astype(F32)
     padded = jnp.concatenate([first, first], axis=0)
-    normed = normed_rows(padded, known[seqs + 1 : seqs + 2])
+    normed, scale = normed_rows(padded, known[seqs + 1 : seqs + 2])
     for i in range(kv):
         slabs[i] = normed[:, i * span : (i + 1) * span].astype(F32)
         firsts[i] = padded[:, i * span : (i + 1) * span]
     slab = slabs[here].astype(BF16)
     first_out[...] = firsts[here][:seqs]
-    xs = dot_nn(normed, w_x[...]).astype(BF16).astype(F32)
-    zeta = dot_nn(normed, w_z[...]).astype(BF16).astype(F32)
-    bc = dot_nn(slab, w_bc[...])
-    dt = dot_nt(slab, w_dt[...])
+    xs = (dot_nn(normed, w_x[...]) * scale).astype(BF16).astype(F32)
+    zeta = (dot_nn(normed, w_z[...]) * scale).astype(BF16).astype(F32)
+    bc = dot_nn(slab, w_bc[...]) * scale
+    dt = dot_nt(slab, w_dt[...]) * scale
     width = xs.shape[1]
     a = 2 * width
     b = a + bc.shape[1]
@@ -309,7 +309,7 @@
     second = jnp.concatenate([halves[i] for i in range(count)], axis=1)
     padded = jnp.concatenate([second, second], axis=0)
     gain = rows[seqs + 2 : seqs + 3, :].astype(F32)
-    sums = feed(normed_rows(padded, gain), 1, gate, up, down)[:seqs]
+    sums = feed(*normed_rows(padded, gain), 1, gate, up, down)[:seqs]
     for i in range(count):
         sums_held[i] = sums[:, i * width : (i + 1) * width]
     for out, core in ((keep, side), (give, 1 - side)):

time: 55.5 us -> 55.2 us (level)
  no operation moved by 1% of the time
where the time goes in v3:
time: 55.2 us; the launch traced here: 54.9 us
  starting transfers between devices  23.6 us (43%)
  waiting for transfers between devices  15.1 us (27%)
  Pallas kernels  13.2 us (24%)
  local copies, waits for them, and re-layouts  2.06 us (4%)
  other arithmetic  0.61 us (1%)
    pallas_call x12, Pallas kernels, run(): pl.pallas_call(body, out_shape=outs, in_specs=in_specs or [VMEM] * len(ar...  13.2 us
    ppermute x6, starting transfers between devices, swap_kv(): got[d] = lax.ppermute(values[d], 'kv', [(i, i ^ d) for i in range(kv)])  8.98 us
    ppermute x4, starting transfers between devices, swap_far(): return lax.ppermute(value, ('kv', 'tp'), pairs)  7.32 us
    ppermute x4, starting transfers between devices, swap_near(): return lax.ppermute(value, ('kv', 'tp'), pairs)  6.02 us
    ppermute x6, waiting for transfers between devices, swap_kv(): got[d] = lax.ppermute(values[d], 'kv', [(i, i ^ d) for i in range(kv)])  5.02 us
    ppermute x8, waiting for transfers between devices, swap_tp(): return lax.ppermute(value, 'tp', [(0, 1), (1, 0)])  4.31 us
    ppermute x4, waiting for transfers between devices, swap_far(): return lax.ppermute(value, ('kv', 'tp'), pairs)  3.91 us
    ppermute x4, waiting for transfers between devices, swap_near(): return lax.ppermute(value, ('kv', 'tp'), pairs)  1.89 us
  transfers between devices with their start and end apart: 22, of which 13 were waited for; matrix products, arithmetic and copies ran while one was open for 2% of the time, Pallas kernels for 14%

profile of v3, /device:TPU:0, one launch (start us, length us, event | category | flops | bytes accessed | tf_op | source)
XLA Modules:
  0.0 54.9 jit_solution(16251519358742168424)
XLA Ops:
  0.0 0.9 %shard_map.172 = bf16[8,256]{1,0:T(8,128)(2,1)S(1)} custom-call(bf16[4,256]{1,0:T(4,128)(2,1)} %rows.1, bf16[3,256]{1,0:T(4,128)(2,1)} %gains.1), custom_call_target="tpu_custom_call" | custom-call | flops 10000000000 | tf_op jit(solution)/shard_map/pallas_call | solution.py:76
  1.5 0.8 %collective-permute-done = bf16[8,256]{1,0:T(8,128)(2,1)S(1)} collective-permute-done((bf16[8,256]{1,0:T(8,128)(2,1)S(1)}, bf16[8,256]{1,0:T(8,128)(2,1)S(1)}, u32[]{:S(2)}, u32[]{:S(2)}) %collective-permute-start) | collective-permute-done | bytes 4128 | tf_op jit(solution)/shard_map/ppermute | solution.py:44
  2.3 3.9 %collective-permute-start.2 = (bf16[8,512]{1,0:T(8,128)(2,1)S(1)}, bf16[8,512]{1,0:T(8,128)(2,1)S(1)}, u32[]{:S(2)}, u32[]{:S(2)}) collective-permute-start(bf16[8,512]{1,0:T(8,128)(2,1)S(1)} %pad_maximum_fusion.c0), channel_id=1, source_target_pairs={{0,4},{1,7},{2,6},{3,5},{4,0},{5,3},{6,2},{7,1},{8,12},{9,15},{10,... | collective-permute-start | bytes 24584 | tf_op jit(solution)/shard_map/ppermute | solution.py:49
  6.2 0.9 %shard_map.173.gate = bf16[2048,704]{1,0:T(8,128)(2,1)S(1)} custom-call(bf16[2,704,2048]{2,1,0:T(8,128)(2,1)S(1)} %bitcast.25), custom_call_target="tpu_custom_call" | custom-call | flops 10000000000 | tf_op jit(solution)/shard_map/pallas_call | solution.py:76
  7.1 1.6 %collective-permute-start.1 = (bf16[8,512]{1,0:T(8,128)(2,1)S(1)}, bf16[8,512]{1,0:T(8,128)(2,1)S(1)}, u32[]{:S(2)}, u32[]{:S(2)}) collective-permute-start(bf16[8,512]{1,0:T(8,128)(2,1)S(1)} %pad_maximum_fusion.c0), channel_id=1, source_target_pairs={{0,2},{1,3},{2,0},{3,1},{4,6},{5,7},{6,4},{7,5},{8,10},{9,11},{10,... | collective-permute-start | bytes 24584 | tf_op jit(solution)/shard_map/ppermute | solution.py:54
  8.8 0.9 %shard_map.174.up = bf16[2048,704]{1,0:T(8,128)(2,1)S(1)} custom-call(bf16[2,704,2048]{2,1,0:T(8,128)(2,1)S(1)} %bitcast.29), custom_call_target="tpu_custom_call" | custom-call | flops 10000000000 | tf_op jit(solution)/shard_map/pallas_call | solution.py:76
  9.7 1.1 %collective-permute-done.1.c1 = bf16[8,512]{1,0:T(8,128)(2,1)S(1)} collective-permute-done((bf16[8,512]{1,0:T(8,128)(2,1)S(1)}, bf16[8,512]{1,0:T(8,128)(2,1)S(1)}, u32[]{:S(2)}, u32[]{:S(2)}) %collective-permute-start.1) | collective-permute-done | bytes 8224 | tf_op jit(solution)/shard_map/ppermute | solution.py:54
  10.9 1.3 %shard_map.175 = (f32[4,2048]{1,0:T(4,128)S(1)}, bf16[8,2048]{1,0:T(8,128)(2,1)S(1)}) custom-call(bf16[8,512]{1,0:T(8,128)(2,1)S(1)} %pad_maximum_fusion.c0, bf16[8,512]{1,0:T(8,128)(2,1)S(1)} %collective-permute-done.1.c1, bf16[8,512]{1,0:T(8,128)(2,1)S(1)} %collective-permute-done.2.c2, bf16[8,512]{1,0:T(8,128)(2,1)S(1)} %collective-permute-done.3.c3, ...), custom_call_target="tpu_custom_call" | custom-call | flops 10000000000 | tf_op jit(solution)/shard_map/pallas_call | solution.py:76
  12.3 1.2 %collective-permute-done.4 = f32[4,2048]{1,0:T(4,128)S(1)} collective-permute-done((f32[4,2048]{1,0:T(4,128)S(1)}, f32[4,2048]{1,0:T(4,128)S(1)}, u32[]{:S(2)}, u32[]{:S(2)}) %collective-permute-start.4) | collective-permute-done | bytes 32800 | tf_op jit(solution)/shard_map/ppermute | solution.py:44
  13.4 1.1 %collective-permute-start.6 = (bf16[4,2048]{1,0:T(4,128)(2,1)S(1)}, bf16[4,2048]{1,0:T(4,128)(2,1)S(1)}, u32[]{:S(2)}, u32[]{:S(2)}) collective-permute-start(bf16[4,2048]{1,0:T(4,128)(2,1)S(1)} %add_convert_fusion.s0), channel_id=1, source_target_pairs={{0,4},{1,7},{2,6},{3,5},{4,0},{5,3},{6,2},{7,1},{8,12},{9,15},{10,... | collective-permute-start | bytes 49160 | tf_op jit(solution)/shard_map/ppermute | solution.py:49
  14.6 1.6 %collective-permute-start.5 = (bf16[4,2048]{1,0:T(4,128)(2,1)S(1)}, bf16[4,2048]{1,0:T(4,128)(2,1)S(1)}, u32[]{:S(2)}, u32[]{:S(2)}) collective-permute-start(bf16[4,2048]{1,0:T(4,128)(2,1)S(1)} %add_convert_fusion.s0), channel_id=1, source_target_pairs={{0,2},{1,3},{2,0},{3,1},{4,6},{5,7},{6,4},{7,5},{8,10},{9,11},{10,... | collective-permute-start | bytes 49160 | tf_op jit(solution)/shard_map/ppermute | solution.py:54
  16.2 2.0 %collective-permute-done.6.s2 = bf16[4,2048]{1,0:T(4,128)(2,1)S(1)} collective-permute-done((bf16[4,2048]{1,0:T(4,128)(2,1)S(1)}, bf16[4,2048]{1,0:T(4,128)(2,1)S(1)}, u32[]{:S(2)}, u32[]{:S(2)}) %collective-permute-start.6) | collective-permute-done | bytes 16416 | tf_op jit(solution)/shard_map/ppermute | solution.py:49
  18.2 1.1 %shard_map.176 = (bf16[2048,512]{1,0:T(8,128)(2,1)S(1)}, bf16[2048,512]{1,0:T(8,128)(2,1)S(1)}) custom-call(bf16[512,2048]{1,0:T(8,128)(2,1)S(1)} %bitcast.34, bf16[512,2048]{1,0:T(8,128)(2,1)S(1)} %bitcast.35), custom_call_target="tpu_custom_call" | custom-call | flops 10000000000 | tf_op jit(solution)/shard_map/pallas_call | solution.py:76
  20.4 1.0 %shard_map.177 = (f32[1,3200]{1,0:T(1,128)S(1)}, f32[1,3200]{1,0:T(1,128)S(1)}, f32[1,3200]{1,0:T(1,128)S(1)}, f32[1,3200]{1,0:T(1,128)S(1)}, f32[4,512]{1,0:T(4,128)S(1)}) custom-call(bf16[4,2048]{1,0:T(4,128)(2,1)S(1)} %add_convert_fusion.s0, bf16[4,2048]{1,0:T(4,128)(2,1)S(1)} %collective-permute-done.5.s1, ...), custom_call_target="tpu_custom_call" | custom-call | flops 10000000000 | tf_op jit(solution)/shard_map/pallas_call | solution.py:76
  21.3 2.4 %collective-permute-start.10 = (f32[1,3200]{1,0:T(1,128)S(1)}, f32[1,3200]{1,0:T(1,128)S(1)}, u32[]{:S(2)}, u32[]{:S(2)}) collective-permute-start(f32[1,3200]{1,0:T(1,128)S(1)} %get-tuple-element.26), channel_id=1, source_target_pairs={{0,6},{2,4},{4,2},{6,0},{1,7},{3,5},{5,3},{7,1},{8,14},{10,12},{12... | collective-permute-start | bytes 38408 | tf_op jit(solution)/shard_map/ppermute | solution.py:35
  23.7 2.1 %collective-permute-start.9 = (f32[1,3200]{1,0:T(1,128)S(1)}, f32[1,3200]{1,0:T(1,128)S(1)}, u32[]{:S(2)}, u32[]{:S(2)}) collective-permute-start(f32[1,3200]{1,0:T(1,128)S(1)} %get-tuple-element.25), channel_id=1, source_target_pairs={{0,4},{2,6},{4,0},{6,2},{1,5},{3,7},{5,1},{7,3},{8,12},{10,14},{12... | collective-permute-start | bytes 38408 | tf_op jit(solution)/shard_map/ppermute | solution.py:35
  27.4 0.9 %collective-permute-done.9.p2 = f32[1,3200]{1,0:T(1,128)S(1)} collective-permute-done((f32[1,3200]{1,0:T(1,128)S(1)}, f32[1,3200]{1,0:T(1,128)S(1)}, u32[]{:S(2)}, u32[]{:S(2)}) %collective-permute-start.9) | collective-permute-done | bytes 12832 | tf_op jit(solution)/shard_map/ppermute | solution.py:35
  28.9 2.1 %collective-permute-start.11 = (f32[1,2048]{1,0:T(1,128)S(1)}, f32[1,2048]{1,0:T(1,128)S(1)}, u32[]{:S(2)}, u32[]{:S(2)}) collective-permute-start(f32[1,2048]{1,0:T(1,128)S(1)} %shard_map.179.m0), channel_id=1, source_target_pairs={{0,2},{2,0},{4,6},{6,4},{1,3},{3,1},{5,7},{7,5},{8,10},{10,8},{12,... | collective-permute-start | bytes 24584 | tf_op jit(solution)/shard_map/ppermute | solution.py:35
  31.0 0.7 %collective-permute-start.12 = (f32[1,2048]{1,0:T(1,128)S(1)}, f32[1,2048]{1,0:T(1,128)S(1)}, u32[]{:S(2)}, u32[]{:S(2)}) collective-permute-start(f32[1,2048]{1,0:T(1,128)S(1)} %shard_map.179.m0), channel_id=1, source_target_pairs={{0,4},{2,6},{4,0},{6,2},{1,5},{3,7},{5,1},{7,3},{8,12},{10,14},{12... | collective-permute-start | bytes 24584 | tf_op jit(solution)/shard_map/ppermute | solution.py:35
  31.7 1.7 %collective-permute-start.13 = (f32[1,2048]{1,0:T(1,128)S(1)}, f32[1,2048]{1,0:T(1,128)S(1)}, u32[]{:S(2)}, u32[]{:S(2)}) collective-permute-start(f32[1,2048]{1,0:T(1,128)S(1)} %shard_map.179.m0), channel_id=1, source_target_pairs={{0,6},{2,4},{4,2},{6,0},{1,7},{3,5},{5,3},{7,1},{8,14},{10,12},{12... | collective-permute-start | bytes 24584 | tf_op jit(solution)/shard_map/ppermute | solution.py:35
  33.5 2.1 %collective-permute-done.12.m2 = f32[1,2048]{1,0:T(1,128)S(1)} collective-permute-done((f32[1,2048]{1,0:T(1,128)S(1)}, f32[1,2048]{1,0:T(1,128)S(1)}, u32[]{:S(2)}, u32[]{:S(2)}) %collective-permute-start.12) | collective-permute-done | bytes 8224 | tf_op jit(solution)/shard_map/ppermute | solution.py:35
  35.6 1.6 %collective-permute-done.13.m3 = f32[1,2048]{1,0:T(1,128)S(1)} collective-permute-done((f32[1,2048]{1,0:T(1,128)S(1)}, f32[1,2048]{1,0:T(1,128)S(1)}, u32[]{:S(2)}, u32[]{:S(2)}) %collective-permute-start.13) | collective-permute-done | bytes 8224 | tf_op jit(solution)/shard_map/ppermute | solution.py:35
  37.6 1.2 %collective-permute-done.14 = f32[4,512]{1,0:T(4,128)S(1)} collective-permute-done((f32[4,512]{1,0:T(4,128)S(1)}, f32[4,512]{1,0:T(4,128)S(1)}, u32[]{:S(2)}, u32[]{:S(2)}) %collective-permute-start.14) | collective-permute-done | bytes 8224 | tf_op jit(solution)/shard_map/ppermute | solution.py:44
  39.2 2.4 %shard_map.181.gate = bf16[2048,704]{1,0:T(8,128)(2,1)S(1)} custom-call(bf16[2,704,2048]{2,1,0:T(8,128)(2,1)} %bitcast.24), custom_call_target="tpu_custom_call" | custom-call | flops 10000000000 | tf_op jit(solution)/shard_map/pallas_call | solution.py:76
  41.6 1.9 %collective-permute-start.15 = (bf16[4,512]{1,0:T(4,128)(2,1)S(1)}, bf16[4,512]{1,0:T(4,128)(2,1)S(1)}, u32[]{:S(2)}, u32[]{:S(2)}) collective-permute-start(bf16[4,512]{1,0:T(4,128)(2,1)S(1)} %add_convert_fusion.1.s0), channel_id=1, source_target_pairs={{0,2},{1,3},{2,0},{3,1},{4,6},{5,7},{6,4},{7,5},{8,10},{9,11},{10,... | collective-permute-start | bytes 12296 | tf_op jit(solution)/shard_map/ppermute | solution.py:54
  43.6 2.2 %shard_map.182.up = bf16[2048,704]{1,0:T(8,128)(2,1)S(1)} custom-call(bf16[2,704,2048]{2,1,0:T(8,128)(2,1)} %bitcast.26), custom_call_target="tpu_custom_call" | custom-call | flops 10000000000 | tf_op jit(solution)/shard_map/pallas_call | solution.py:76
  45.9 1.4 %shard_map.183 = (f32[4,1024]{1,0:T(4,128)S(1)}, f32[4,1024]{1,0:T(4,128)S(1)}, f32[4,256]{1,0:T(4,128)S(1)}) custom-call(bf16[4,512]{1,0:T(4,128)(2,1)S(1)} %add_convert_fusion.1.s0, bf16[4,512]{1,0:T(4,128)(2,1)S(1)} %collective-permute-done.15.s1, bf16[4,512]{1,0:T(4,128)(2,1)S(1)} %collective-permute-done.16.s2, ...), custom_call_target="tpu_custom_call" | custom-call | flops 10000000000 | tf_op jit(solution)/shard_map/pallas_call | solution.py:76
  47.7 0.8 %collective-permute-done.18 = f32[4,1024]{1,0:T(4,128)S(1)} collective-permute-done((f32[4,1024]{1,0:T(4,128)S(1)}, f32[4,1024]{1,0:T(4,128)S(1)}, u32[]{:S(2)}, u32[]{:S(2)}) %collective-permute-start.18) | collective-permute-done | bytes 16416 | tf_op jit(solution)/shard_map/ppermute | solution.py:44
  48.6 1.8 %collective-permute-start.19 = (f32[4,512]{1,0:T(4,128)S(1)}, f32[4,512]{1,0:T(4,128)S(1)}, u32[]{:S(2)}, u32[]{:S(2)}) collective-permute-start(f32[4,512]{1,0:T(4,128)S(1)} %slice.21), channel_id=1, source_target_pairs={{0,4},{1,7},{2,6},{3,5},{4,0},{5,3},{6,2},{7,1},{8,12},{9,15},{10,... | collective-permute-start | bytes 24584 | tf_op jit(solution)/shard_map/ppermute | solution.py:49
  50.4 0.9 %collective-permute-start.20 = (f32[4,256]{1,0:T(4,128)S(1)}, f32[4,256]{1,0:T(4,128)S(1)}, u32[]{:S(2)}, u32[]{:S(2)}) collective-permute-start(f32[4,256]{1,0:T(4,128)S(1)} %slice.23), channel_id=1, source_target_pairs={{0,2},{1,3},{2,0},{3,1},{4,6},{5,7},{6,4},{7,5},{8,10},{9,11},{10,... | collective-permute-start | bytes 12296 | tf_op jit(solution)/shard_map/ppermute | solution.py:54
  51.3 1.9 %collective-permute-done.19 = f32[4,512]{1,0:T(4,128)S(1)} collective-permute-done((f32[4,512]{1,0:T(4,128)S(1)}, f32[4,512]{1,0:T(4,128)S(1)}, u32[]{:S(2)}, u32[]{:S(2)}) %collective-permute-start.19) | collective-permute-done | bytes 8224 | tf_op jit(solution)/shard_map/ppermute | solution.py:49
  53.3 0.7 %collective-permute-done.20 = f32[4,256]{1,0:T(4,128)S(1)} collective-permute-done((f32[4,256]{1,0:T(4,128)S(1)}, f32[4,256]{1,0:T(4,128)S(1)}, u32[]{:S(2)}, u32[]{:S(2)}) %collective-permute-start.20) | collective-permute-done | bytes 4128 | tf_op jit(solution)/shard_map/ppermute | solution.py:54
  (80 shorter events, 6.2 us)
Async XLA Ops:
  0.0 6.2 %copy-start = (bf16[2,2048,704]{1,2,0:T(8,128)(2,1)S(1)}, bf16[2,2048,704]{1,2,0:T(8,128)(2,1)}, u32[]{:S(2)}) copy-start(bf16[2,2048,704]{1,2,0:T(8,128)(2,1)} %param.20) | copy-start | bytes 17301508
  0.0 8.8 %slice-start = ((s8[5767168]{0:T(1024)(128)(4,1)}), s8[4194304]{0:T(1024)(128)(4,1)S(1)}, s32[]{:S(2)}) async-start(s8[5767168]{0:T(1024)(128)(4,1)} %bitcast.27), calls=%async_computation | async-start | bytes 8388608
  0.9 7.9 %slice-start.1 = ((s8[5767168]{0:T(1024)(128)(4,1)}), s8[1572864]{0:T(1024)(128)(4,1)S(1)}, s32[]{:S(2)}) async-start(s8[5767168]{0:T(1024)(128)(4,1)} %bitcast.27), calls=%async_computation.1 | async-start | bytes 3145728
  0.9 1.4 %collective-permute-start = (bf16[8,256]{1,0:T(8,128)(2,1)S(1)}, bf16[8,256]{1,0:T(8,128)(2,1)S(1)}, u32[]{:S(2)}, u32[]{:S(2)}) collective-permute-start(bf16[8,256]{1,0:T(8,128)(2,1)S(1)} %shard_map.172), channel_id=1, source_target_pairs={{0,1},{1,0},{2,3},{3,2},{4,5},{5,4},{6,7},{7,6},{8,9},{9,8},{10,11... | collective-permute-start | bytes 12296 | tf_op jit(solution)/shard_map/ppermute | solution.py:44
  2.3 6.5 %collective-permute-start.2 = (bf16[8,512]{1,0:T(8,128)(2,1)S(1)}, bf16[8,512]{1,0:T(8,128)(2,1)S(1)}, u32[]{:S(2)}, u32[]{:S(2)}) collective-permute-start(bf16[8,512]{1,0:T(8,128)(2,1)S(1)} %pad_maximum_fusion.c0), channel_id=1, source_target_pairs={{0,4},{1,7},{2,6},{3,5},{4,0},{5,3},{6,2},{7,1},{8,12},{9,15},{10,... | collective-permute-start | bytes 24584 | tf_op jit(solution)/shard_map/ppermute | solution.py:49
  6.2 4.6 %slice-start.2 = ((s8[5767168]{0:T(1024)(128)(4,1)}), s8[4194304]{0:T(1024)(128)(4,1)S(1)}, s32[]{:S(2)}) async-start(s8[5767168]{0:T(1024)(128)(4,1)} %bitcast.30), calls=%async_computation.2 | async-start | bytes 8388608
  7.1 3.7 %collective-permute-start.1 = (bf16[8,512]{1,0:T(8,128)(2,1)S(1)}, bf16[8,512]{1,0:T(8,128)(2,1)S(1)}, u32[]{:S(2)}, u32[]{:S(2)}) collective-permute-start(bf16[8,512]{1,0:T(8,128)(2,1)S(1)} %pad_maximum_fusion.c0), channel_id=1, source_target_pairs={{0,2},{1,3},{2,0},{3,1},{4,6},{5,7},{6,4},{7,5},{8,10},{9,11},{10,... | collective-permute-start | bytes 24584 | tf_op jit(solution)/shard_map/ppermute | solution.py:54
  8.8 2.1 %collective-permute-start.3 = (bf16[8,512]{1,0:T(8,128)(2,1)S(1)}, bf16[8,512]{1,0:T(8,128)(2,1)S(1)}, u32[]{:S(2)}, u32[]{:S(2)}) collective-permute-start(bf16[8,512]{1,0:T(8,128)(2,1)S(1)} %collective-permute-done.2.c2), channel_id=1, source_target_pairs={{0,1},{1,0},{2,3},{3,2},{4,5},{5,4},{6,7},{7,6},{8,9},{9,8},{10,11... | collective-permute-start | bytes 24584 | tf_op jit(solution)/shard_map/ppermute | solution.py:44
  9.7 8.5 %copy-start.1 = (bf16[2048,16,32]{0,2,1:T(8,128)(2,1)S(1)}, bf16[2048,16,32]{0,2,1:T(8,128)(2,1)}, u32[]{:S(2)}) copy-start(bf16[2048,16,32]{0,2,1:T(8,128)(2,1)} %param.23) | copy-start | bytes 6291460
  9.7 8.5 %copy-start.2 = (bf16[2048,16,32]{0,2,1:T(8,128)(2,1)S(1)}, bf16[2048,16,32]{0,2,1:T(8,128)(2,1)}, u32[]{:S(2)}) copy-start(bf16[2048,16,32]{0,2,1:T(8,128)(2,1)} %param.24) | copy-start | bytes 6291460
  12.2 1.2 %collective-permute-start.4 = (f32[4,2048]{1,0:T(4,128)S(1)}, f32[4,2048]{1,0:T(4,128)S(1)}, u32[]{:S(2)}, u32[]{:S(2)}) collective-permute-start(f32[4,2048]{1,0:T(4,128)S(1)} %get-tuple-element.19), channel_id=1, source_target_pairs={{0,1},{1,0},{2,3},{3,2},{4,5},{5,4},{6,7},{7,6},{8,9},{9,8},{10,11... | collective-permute-start | bytes 98312 | tf_op jit(solution)/shard_map/ppermute | solution.py:44
  13.4 4.7 %collective-permute-start.6 = (bf16[4,2048]{1,0:T(4,128)(2,1)S(1)}, bf16[4,2048]{1,0:T(4,128)(2,1)S(1)}, u32[]{:S(2)}, u32[]{:S(2)}) collective-permute-start(bf16[4,2048]{1,0:T(4,128)(2,1)S(1)} %add_convert_fusion.s0), channel_id=1, source_target_pairs={{0,4},{1,7},{2,6},{3,5},{4,0},{5,3},{6,2},{7,1},{8,12},{9,15},{10,... | collective-permute-start | bytes 49160 | tf_op jit(solution)/shard_map/ppermute | solution.py:49
  14.6 5.7 %collective-permute-start.5 = (bf16[4,2048]{1,0:T(4,128)(2,1)S(1)}, bf16[4,2048]{1,0:T(4,128)(2,1)S(1)}, u32[]{:S(2)}, u32[]{:S(2)}) collective-permute-start(bf16[4,2048]{1,0:T(4,128)(2,1)S(1)} %add_convert_fusion.s0), channel_id=1, source_target_pairs={{0,2},{1,3},{2,0},{3,1},{4,6},{5,7},{6,4},{7,5},{8,10},{9,11},{10,... | collective-permute-start | bytes 49160 | tf_op jit(solution)/shard_map/ppermute | solution.py:54
  18.2 2.2 %collective-permute-start.7 = (bf16[4,2048]{1,0:T(4,128)(2,1)S(1)}, bf16[4,2048]{1,0:T(4,128)(2,1)S(1)}, u32[]{:S(2)}, u32[]{:S(2)}) collective-permute-start(bf16[4,2048]{1,0:T(4,128)(2,1)S(1)} %collective-permute-done.6.s2), channel_id=1, source_target_pairs={{0,1},{1,0},{2,3},{3,2},{4,5},{5,4},{6,7},{7,6},{8,9},{9,8},{10,11... | collective-permute-start | bytes 49160 | tf_op jit(solution)/shard_map/ppermute | solution.py:44
  20.3 5.4 %copy-start.4 = (f32[1,64,32,128]{3,2,1,0:T(8,128)S(1)}, f32[1,64,32,128]{3,2,1,0:T(8,128)}, u32[]{:S(2)}) copy-start(f32[1,64,32,128]{3,2,1,0:T(8,128)} %param.34) | copy-start | bytes 3145732
  21.3 5.7 %collective-permute-start.10 = (f32[1,3200]{1,0:T(1,128)S(1)}, f32[1,3200]{1,0:T(1,128)S(1)}, u32[]{:S(2)}, u32[]{:S(2)}) collective-permute-start(f32[1,3200]{1,0:T(1,128)S(1)} %get-tuple-element.26), channel_id=1, source_target_pairs={{0,6},{2,4},{4,2},{6,0},{1,7},{3,5},{5,3},{7,1},{8,14},{10,12},{12... | collective-permute-start | bytes 38408 | tf_op jit(solution)/shard_map/ppermute | solution.py:35
  23.7 3.7 %collective-permute-start.8 = (f32[1,3200]{1,0:T(1,128)S(1)}, f32[1,3200]{1,0:T(1,128)S(1)}, u32[]{:S(2)}, u32[]{:S(2)}) collective-permute-start(f32[1,3200]{1,0:T(1,128)S(1)} %get-tuple-element.24), channel_id=1, source_target_pairs={{0,2},{2,0},{4,6},{6,4},{1,3},{3,1},{5,7},{7,5},{8,10},{10,8},{12,... | collective-permute-start | bytes 38408 | tf_op jit(solution)/shard_map/ppermute | solution.py:35
  23.7 4.6 %collective-permute-start.9 = (f32[1,3200]{1,0:T(1,128)S(1)}, f32[1,3200]{1,0:T(1,128)S(1)}, u32[]{:S(2)}, u32[]{:S(2)}) collective-permute-start(f32[1,3200]{1,0:T(1,128)S(1)} %get-tuple-element.25), channel_id=1, source_target_pairs={{0,4},{2,6},{4,0},{6,2},{1,5},{3,7},{5,1},{7,3},{8,12},{10,14},{12... | collective-permute-start | bytes 38408 | tf_op jit(solution)/shard_map/ppermute | solution.py:35
  28.3 8.9 %copy-start.3 = (bf16[64,32,512]{2,1,0:T(8,128)(2,1)S(1)}, bf16[64,32,512]{2,1,0:T(8,128)(2,1)}, u32[]{:S(2)}) copy-start(bf16[64,32,512]{2,1,0:T(8,128)(2,1)} %param.35) | copy-start | bytes 6291460
  28.9 4.5 %collective-permute-start.11 = (f32[1,2048]{1,0:T(1,128)S(1)}, f32[1,2048]{1,0:T(1,128)S(1)}, u32[]{:S(2)}, u32[]{:S(2)}) collective-permute-start(f32[1,2048]{1,0:T(1,128)S(1)} %shard_map.179.m0), channel_id=1, source_target_pairs={{0,2},{2,0},{4,6},{6,4},{1,3},{3,1},{5,7},{7,5},{8,10},{10,8},{12,... | collective-permute-start | bytes 24584 | tf_op jit(solution)/shard_map/ppermute | solution.py:35
  31.0 4.5 %collective-permute-start.12 = (f32[1,2048]{1,0:T(1,128)S(1)}, f32[1,2048]{1,0:T(1,128)S(1)}, u32[]{:S(2)}, u32[]{:S(2)}) collective-permute-start(f32[1,2048]{1,0:T(1,128)S(1)} %shard_map.179.m0), channel_id=1, source_target_pairs={{0,4},{2,6},{4,0},{6,2},{1,5},{3,7},{5,1},{7,3},{8,12},{10,14},{12... | collective-permute-start | bytes 24584 | tf_op jit(solution)/shard_map/ppermute | solution.py:35
  31.7 5.4 %collective-permute-start.13 = (f32[1,2048]{1,0:T(1,128)S(1)}, f32[1,2048]{1,0:T(1,128)S(1)}, u32[]{:S(2)}, u32[]{:S(2)}) collective-permute-start(f32[1,2048]{1,0:T(1,128)S(1)} %shard_map.179.m0), channel_id=1, source_target_pairs={{0,6},{2,4},{4,2},{6,0},{1,7},{3,5},{5,3},{7,1},{8,14},{10,12},{12... | collective-permute-start | bytes 24584 | tf_op jit(solution)/shard_map/ppermute | solution.py:35
  37.6 1.2 %collective-permute-start.14 = (f32[4,512]{1,0:T(4,128)S(1)}, f32[4,512]{1,0:T(4,128)S(1)}, u32[]{:S(2)}, u32[]{:S(2)}) collective-permute-start(f32[4,512]{1,0:T(4,128)S(1)} %shard_map.180), channel_id=1, source_target_pairs={{0,1},{1,0},{2,3},{3,2},{4,5},{5,4},{6,7},{7,6},{8,9},{9,8},{10,11... | collective-permute-start | bytes 24584 | tf_op jit(solution)/shard_map/ppermute | solution.py:44
  38.8 4.8 %collective-permute-start.16 = (bf16[4,512]{1,0:T(4,128)(2,1)S(1)}, bf16[4,512]{1,0:T(4,128)(2,1)S(1)}, u32[]{:S(2)}, u32[]{:S(2)}) collective-permute-start(bf16[4,512]{1,0:T(4,128)(2,1)S(1)} %add_convert_fusion.1.s0), channel_id=1, source_target_pairs={{0,4},{1,7},{2,6},{3,5},{4,0},{5,3},{6,2},{7,1},{8,12},{9,15},{10,... | collective-permute-start | bytes 12296 | tf_op jit(solution)/shard_map/ppermute | solution.py:49
  39.2 6.6 %slice-start.4 = ((s8[5767168]{0:T(1024)(128)(4,1)}), s8[4194304]{0:T(1024)(128)(4,1)S(1)}, s32[]{:S(2)}) async-start(s8[5767168]{0:T(1024)(128)(4,1)} %bitcast.32), calls=%async_computation.4 | async-start | bytes 8388608
  41.6 4.2 %slice-start.5 = ((s8[5767168]{0:T(1024)(128)(4,1)}), s8[1572864]{0:T(1024)(128)(4,1)S(1)}, s32[]{:S(2)}) async-start(s8[5767168]{0:T(1024)(128)(4,1)} %bitcast.32), calls=%async_computation.5 | async-start | bytes 3145728
  41.6 4.2 %collective-permute-start.15 = (bf16[4,512]{1,0:T(4,128)(2,1)S(1)}, bf16[4,512]{1,0:T(4,128)(2,1)S(1)}, u32[]{:S(2)}, u32[]{:S(2)}) collective-permute-start(bf16[4,512]{1,0:T(4,128)(2,1)S(1)} %add_convert_fusion.1.s0), channel_id=1, source_target_pairs={{0,2},{1,3},{2,0},{3,1},{4,6},{5,7},{6,4},{7,5},{8,10},{9,11},{10,... | collective-permute-start | bytes 12296 | tf_op jit(solution)/shard_map/ppermute | solution.py:54
  43.5 2.3 %collective-permute-start.17 = (bf16[4,512]{1,0:T(4,128)(2,1)S(1)}, bf16[4,512]{1,0:T(4,128)(2,1)S(1)}, u32[]{:S(2)}, u32[]{:S(2)}) collective-permute-start(bf16[4,512]{1,0:T(4,128)(2,1)S(1)} %collective-permute-done.16.s2), channel_id=1, source_target_pairs={{0,1},{1,0},{2,3},{3,2},{4,5},{5,4},{6,7},{7,6},{8,9},{9,8},{10,11... | collective-permute-start | bytes 12296 | tf_op jit(solution)/shard_map/ppermute | solution.py:44
  47.2 1.4 %collective-permute-start.18 = (f32[4,1024]{1,0:T(4,128)S(1)}, f32[4,1024]{1,0:T(4,128)S(1)}, u32[]{:S(2)}, u32[]{:S(2)}) collective-permute-start(f32[4,1024]{1,0:T(4,128)S(1)} %get-tuple-element.32), channel_id=1, source_target_pairs={{0,1},{1,0},{2,3},{3,2},{4,5},{5,4},{6,7},{7,6},{8,9},{9,8},{10,11... | collective-permute-start | bytes 49160 | tf_op jit(solution)/shard_map/ppermute | solution.py:44
  48.6 4.6 %collective-permute-start.19 = (f32[4,512]{1,0:T(4,128)S(1)}, f32[4,512]{1,0:T(4,128)S(1)}, u32[]{:S(2)}, u32[]{:S(2)}) collective-permute-start(f32[4,512]{1,0:T(4,128)S(1)} %slice.21), channel_id=1, source_target_pairs={{0,4},{1,7},{2,6},{3,5},{4,0},{5,3},{6,2},{7,1},{8,12},{9,15},{10,... | collective-permute-start | bytes 24584 | tf_op jit(solution)/shard_map/ppermute | solution.py:49
  50.4 3.6 %collective-permute-start.20 = (f32[4,256]{1,0:T(4,128)S(1)}, f32[4,256]{1,0:T(4,128)S(1)}, u32[]{:S(2)}, u32[]{:S(2)}) collective-permute-start(f32[4,256]{1,0:T(4,128)S(1)} %slice.23), channel_id=1, source_target_pairs={{0,2},{1,3},{2,0},{3,1},{4,6},{5,7},{6,4},{7,5},{8,10},{9,11},{10,... | collective-permute-start | bytes 12296 | tf_op jit(solution)/shard_map/ppermute | solution.py:54
  53.2 1.2 %collective-permute-start.21 = (f32[4,256]{1,0:T(4,128)S(1)}, f32[4,256]{1,0:T(4,128)S(1)}, u32[]{:S(2)}, u32[]{:S(2)}) collective-permute-start(f32[4,256]{1,0:T(4,128)S(1)} %slice.24), channel_id=1, source_target_pairs={{0,1},{1,0},{2,3},{3,2},{4,5},{5,4},{6,7},{7,6},{8,9},{9,8},{10,11... | collective-permute-start | bytes 12296 | tf_op jit(solution)/shard_map/ppermute | solution.py:44
  (10 other events, 20.6 us)

commit v4 on v3

--- a/solution.py
+++ b/solution.py
@@ -446,9 +446,11 @@
         [pltpu.VMEM((kv * tp, seqs, width), F32), pltpu.VMEM((kv * tp, seqs, width), F32)],
     )
     total = keep + swap_tp(give)
-    far = swap_far(total[:, : 2 * width])
-    near = swap_near(total[:, 2 * width : 3 * width])
-    rest = total[:, 3 * width :] + far[:, :width] + near + swap_tp(far[:, width:])
+    sent = total.astype(BF16)
+    far = swap_far(sent[:, : 2 * width])
+    near = swap_near(sent[:, 2 * width : 3 * width])
+    passed = swap_tp(far[:, width:]).astype(F32)
+    rest = total[:, 3 * width :] + far[:, :width].astype(F32) + near.astype(F32) + passed
     return (base + 0.5 * rest).astype(BF16)
 
 

time: 55.2 us -> 55.1 us (level)
  no operation moved by 1% of the time
where the time goes in v4:
time: 55.1 us; the launch traced here: 54.9 us
  starting transfers between devices  23.6 us (43%)
  waiting for transfers between devices  15.1 us (27%)
  Pallas kernels  13.2 us (24%)
  local copies, waits for them, and re-layouts  2.06 us (4%)
  other arithmetic  0.62 us (1%)
    pallas_call x12, Pallas kernels, run(): pl.pallas_call(body, out_shape=outs, in_specs=in_specs or [VMEM] * len(ar...  13.2 us
    ppermute x6, starting transfers between devices, swap_kv(): got[d] = lax.ppermute(values[d], 'kv', [(i, i ^ d) for i in range(kv)])  8.98 us
    ppermute x4, starting transfers between devices, swap_far(): return lax.ppermute(value, ('kv', 'tp'), pairs)  7.33 us
    ppermute x4, starting transfers between devices, swap_near(): return lax.ppermute(value, ('kv', 'tp'), pairs)  6.02 us
    ppermute x6, waiting for transfers between devices, swap_kv(): got[d] = lax.ppermute(values[d], 'kv', [(i, i ^ d) for i in range(kv)])  5.02 us
    ppermute x8, waiting for transfers between devices, swap_tp(): return lax.ppermute(value, 'tp', [(0, 1), (1, 0)])  4.29 us
    ppermute x4, waiting for transfers between devices, swap_far(): return lax.ppermute(value, ('kv', 'tp'), pairs)  3.86 us
    ppermute x4, waiting for transfers between devices, swap_near(): return lax.ppermute(value, ('kv', 'tp'), pairs)  1.92 us
  transfers between devices with their start and end apart: 22, of which 13 were waited for; matrix products, arithmetic and copies ran while one was open for 2% of the time, Pallas kernels for 14%

profile of v4, /device:TPU:0, one launch (start us, length us, event | category | flops | bytes accessed | tf_op | source)
XLA Modules:
  0.0 54.9 jit_solution(11608471945510535849)
XLA Ops:
  0.0 0.9 %shard_map.172 = bf16[8,256]{1,0:T(8,128)(2,1)S(1)} custom-call(bf16[4,256]{1,0:T(4,128)(2,1)} %rows.1, bf16[3,256]{1,0:T(4,128)(2,1)} %gains.1), custom_call_target="tpu_custom_call" | custom-call | flops 10000000000 | tf_op jit(solution)/shard_map/pallas_call | solution.py:76
  1.5 0.8 %collective-permute-done = bf16[8,256]{1,0:T(8,128)(2,1)S(1)} collective-permute-done((bf16[8,256]{1,0:T(8,128)(2,1)S(1)}, bf16[8,256]{1,0:T(8,128)(2,1)S(1)}, u32[]{:S(2)}, u32[]{:S(2)}) %collective-permute-start) | collective-permute-done | bytes 4128 | tf_op jit(solution)/shard_map/ppermute | solution.py:44
  2.3 3.9 %collective-permute-start.2 = (bf16[8,512]{1,0:T(8,128)(2,1)S(1)}, bf16[8,512]{1,0:T(8,128)(2,1)S(1)}, u32[]{:S(2)}, u32[]{:S(2)}) collective-permute-start(bf16[8,512]{1,0:T(8,128)(2,1)S(1)} %pad_maximum_fusion.c0), channel_id=1, source_target_pairs={{0,4},{1,7},{2,6},{3,5},{4,0},{5,3},{6,2},{7,1},{8,12},{9,15},{10,... | collective-permute-start | bytes 24584 | tf_op jit(solution)/shard_map/ppermute | solution.py:49
  6.2 0.9 %shard_map.173.gate = bf16[2048,704]{1,0:T(8,128)(2,1)S(1)} custom-call(bf16[2,704,2048]{2,1,0:T(8,128)(2,1)S(1)} %bitcast.25), custom_call_target="tpu_custom_call" | custom-call | flops 10000000000 | tf_op jit(solution)/shard_map/pallas_call | solution.py:76
  7.1 1.6 %collective-permute-start.1 = (bf16[8,512]{1,0:T(8,128)(2,1)S(1)}, bf16[8,512]{1,0:T(8,128)(2,1)S(1)}, u32[]{:S(2)}, u32[]{:S(2)}) collective-permute-start(bf16[8,512]{1,0:T(8,128)(2,1)S(1)} %pad_maximum_fusion.c0), channel_id=1, source_target_pairs={{0,2},{1,3},{2,0},{3,1},{4,6},{5,7},{6,4},{7,5},{8,10},{9,11},{10,... | collective-permute-start | bytes 24584 | tf_op jit(solution)/shard_map/ppermute | solution.py:54
  8.8 0.9 %shard_map.174.up = bf16[2048,704]{1,0:T(8,128)(2,1)S(1)} custom-call(bf16[2,704,2048]{2,1,0:T(8,128)(2,1)S(1)} %bitcast.29), custom_call_target="tpu_custom_call" | custom-call | flops 10000000000 | tf_op jit(solution)/shard_map/pallas_call | solution.py:76
  9.7 1.1 %collective-permute-done.1.c1 = bf16[8,512]{1,0:T(8,128)(2,1)S(1)} collective-permute-done((bf16[8,512]{1,0:T(8,128)(2,1)S(1)}, bf16[8,512]{1,0:T(8,128)(2,1)S(1)}, u32[]{:S(2)}, u32[]{:S(2)}) %collective-permute-start.1) | collective-permute-done | bytes 8224 | tf_op jit(solution)/shard_map/ppermute | solution.py:54
  10.9 1.3 %shard_map.175 = (f32[4,2048]{1,0:T(4,128)S(1)}, bf16[8,2048]{1,0:T(8,128)(2,1)S(1)}) custom-call(bf16[8,512]{1,0:T(8,128)(2,1)S(1)} %pad_maximum_fusion.c0, bf16[8,512]{1,0:T(8,128)(2,1)S(1)} %collective-permute-done.1.c1, bf16[8,512]{1,0:T(8,128)(2,1)S(1)} %collective-permute-done.2.c2, bf16[8,512]{1,0:T(8,128)(2,1)S(1)} %collective-permute-done.3.c3, ...), custom_call_target="tpu_custom_call" | custom-call | flops 10000000000 | tf_op jit(solution)/shard_map/pallas_call | solution.py:76
  12.3 1.2 %collective-permute-done.4 = f32[4,2048]{1,0:T(4,128)S(1)} collective-permute-done((f32[4,2048]{1,0:T(4,128)S(1)}, f32[4,2048]{1,0:T(4,128)S(1)}, u32[]{:S(2)}, u32[]{:S(2)}) %collective-permute-start.4) | collective-permute-done | bytes 32800 | tf_op jit(solution)/shard_map/ppermute | solution.py:44
  13.4 1.1 %collective-permute-start.6 = (bf16[4,2048]{1,0:T(4,128)(2,1)S(1)}, bf16[4,2048]{1,0:T(4,128)(2,1)S(1)}, u32[]{:S(2)}, u32[]{:S(2)}) collective-permute-start(bf16[4,2048]{1,0:T(4,128)(2,1)S(1)} %add_convert_fusion.s0), channel_id=1, source_target_pairs={{0,4},{1,7},{2,6},{3,5},{4,0},{5,3},{6,2},{7,1},{8,12},{9,15},{10,... | collective-permute-start | bytes 49160 | tf_op jit(solution)/shard_map/ppermute | solution.py:49
  14.6 1.6 %collective-permute-start.5 = (bf16[4,2048]{1,0:T(4,128)(2,1)S(1)}, bf16[4,2048]{1,0:T(4,128)(2,1)S(1)}, u32[]{:S(2)}, u32[]{:S(2)}) collective-permute-start(bf16[4,2048]{1,0:T(4,128)(2,1)S(1)} %add_convert_fusion.s0), channel_id=1, source_target_pairs={{0,2},{1,3},{2,0},{3,1},{4,6},{5,7},{6,4},{7,5},{8,10},{9,11},{10,... | collective-permute-start | bytes 49160 | tf_op jit(solution)/shard_map/ppermute | solution.py:54
  16.2 2.0 %collective-permute-done.6.s2 = bf16[4,2048]{1,0:T(4,128)(2,1)S(1)} collective-permute-done((bf16[4,2048]{1,0:T(4,128)(2,1)S(1)}, bf16[4,2048]{1,0:T(4,128)(2,1)S(1)}, u32[]{:S(2)}, u32[]{:S(2)}) %collective-permute-start.6) | collective-permute-done | bytes 16416 | tf_op jit(solution)/shard_map/ppermute | solution.py:49
  18.2 1.1 %shard_map.176 = (bf16[2048,512]{1,0:T(8,128)(2,1)S(1)}, bf16[2048,512]{1,0:T(8,128)(2,1)S(1)}) custom-call(bf16[512,2048]{1,0:T(8,128)(2,1)S(1)} %bitcast.34, bf16[512,2048]{1,0:T(8,128)(2,1)S(1)} %bitcast.35), custom_call_target="tpu_custom_call" | custom-call | flops 10000000000 | tf_op jit(solution)/shard_map/pallas_call | solution.py:76
  20.4 1.0 %shard_map.177 = (f32[1,3200]{1,0:T(1,128)S(1)}, f32[1,3200]{1,0:T(1,128)S(1)}, f32[1,3200]{1,0:T(1,128)S(1)}, f32[1,3200]{1,0:T(1,128)S(1)}, f32[4,512]{1,0:T(4,128)S(1)}) custom-call(bf16[4,2048]{1,0:T(4,128)(2,1)S(1)} %add_convert_fusion.s0, bf16[4,2048]{1,0:T(4,128)(2,1)S(1)} %collective-permute-done.5.s1, ...), custom_call_target="tpu_custom_call" | custom-call | flops 10000000000 | tf_op jit(solution)/shard_map/pallas_call | solution.py:76
  21.3 2.4 %collective-permute-start.10 = (f32[1,3200]{1,0:T(1,128)S(1)}, f32[1,3200]{1,0:T(1,128)S(1)}, u32[]{:S(2)}, u32[]{:S(2)}) collective-permute-start(f32[1,3200]{1,0:T(1,128)S(1)} %get-tuple-element.26), channel_id=1, source_target_pairs={{0,6},{2,4},{4,2},{6,0},{1,7},{3,5},{5,3},{7,1},{8,14},{10,12},{12... | collective-permute-start | bytes 38408 | tf_op jit(solution)/shard_map/ppermute | solution.py:35
  23.7 2.1 %collective-permute-start.9 = (f32[1,3200]{1,0:T(1,128)S(1)}, f32[1,3200]{1,0:T(1,128)S(1)}, u32[]{:S(2)}, u32[]{:S(2)}) collective-permute-start(f32[1,3200]{1,0:T(1,128)S(1)} %get-tuple-element.25), channel_id=1, source_target_pairs={{0,4},{2,6},{4,0},{6,2},{1,5},{3,7},{5,1},{7,3},{8,12},{10,14},{12... | collective-permute-start | bytes 38408 | tf_op jit(solution)/shard_map/ppermute | solution.py:35
  27.4 0.9 %collective-permute-done.9.p2 = f32[1,3200]{1,0:T(1,128)S(1)} collective-permute-done((f32[1,3200]{1,0:T(1,128)S(1)}, f32[1,3200]{1,0:T(1,128)S(1)}, u32[]{:S(2)}, u32[]{:S(2)}) %collective-permute-start.9) | collective-permute-done | bytes 12832 | tf_op jit(solution)/shard_map/ppermute | solution.py:35
  28.9 2.1 %collective-permute-start.11 = (f32[1,2048]{1,0:T(1,128)S(1)}, f32[1,2048]{1,0:T(1,128)S(1)}, u32[]{:S(2)}, u32[]{:S(2)}) collective-permute-start(f32[1,2048]{1,0:T(1,128)S(1)} %shard_map.179.m0), channel_id=1, source_target_pairs={{0,2},{2,0},{4,6},{6,4},{1,3},{3,1},{5,7},{7,5},{8,10},{10,8},{12,... | collective-permute-start | bytes 24584 | tf_op jit(solution)/shard_map/ppermute | solution.py:35
  31.0 0.7 %collective-permute-start.12 = (f32[1,2048]{1,0:T(1,128)S(1)}, f32[1,2048]{1,0:T(1,128)S(1)}, u32[]{:S(2)}, u32[]{:S(2)}) collective-permute-start(f32[1,2048]{1,0:T(1,128)S(1)} %shard_map.179.m0), channel_id=1, source_target_pairs={{0,4},{2,6},{4,0},{6,2},{1,5},{3,7},{5,1},{7,3},{8,12},{10,14},{12... | collective-permute-start | bytes 24584 | tf_op jit(solution)/shard_map/ppermute | solution.py:35
  31.7 1.7 %collective-permute-start.13 = (f32[1,2048]{1,0:T(1,128)S(1)}, f32[1,2048]{1,0:T(1,128)S(1)}, u32[]{:S(2)}, u32[]{:S(2)}) collective-permute-start(f32[1,2048]{1,0:T(1,128)S(1)} %shard_map.179.m0), channel_id=1, source_target_pairs={{0,6},{2,4},{4,2},{6,0},{1,7},{3,5},{5,3},{7,1},{8,14},{10,12},{12... | collective-permute-start | bytes 24584 | tf_op jit(solution)/shard_map/ppermute | solution.py:35
  33.5 2.1 %collective-permute-done.12.m2 = f32[1,2048]{1,0:T(1,128)S(1)} collective-permute-done((f32[1,2048]{1,0:T(1,128)S(1)}, f32[1,2048]{1,0:T(1,128)S(1)}, u32[]{:S(2)}, u32[]{:S(2)}) %collective-permute-start.12) | collective-permute-done | bytes 8224 | tf_op jit(solution)/shard_map/ppermute | solution.py:35
  35.6 1.6 %collective-permute-done.13.m3 = f32[1,2048]{1,0:T(1,128)S(1)} collective-permute-done((f32[1,2048]{1,0:T(1,128)S(1)}, f32[1,2048]{1,0:T(1,128)S(1)}, u32[]{:S(2)}, u32[]{:S(2)}) %collective-permute-start.13) | collective-permute-done | bytes 8224 | tf_op jit(solution)/shard_map/ppermute | solution.py:35
  37.6 1.2 %collective-permute-done.14 = f32[4,512]{1,0:T(4,128)S(1)} collective-permute-done((f32[4,512]{1,0:T(4,128)S(1)}, f32[4,512]{1,0:T(4,128)S(1)}, u32[]{:S(2)}, u32[]{:S(2)}) %collective-permute-start.14) | collective-permute-done | bytes 8224 | tf_op jit(solution)/shard_map/ppermute | solution.py:44
  39.2 2.4 %shard_map.181.gate = bf16[2048,704]{1,0:T(8,128)(2,1)S(1)} custom-call(bf16[2,704,2048]{2,1,0:T(8,128)(2,1)} %bitcast.24), custom_call_target="tpu_custom_call" | custom-call | flops 10000000000 | tf_op jit(solution)/shard_map/pallas_call | solution.py:76
  41.6 1.9 %collective-permute-start.15 = (bf16[4,512]{1,0:T(4,128)(2,1)S(1)}, bf16[4,512]{1,0:T(4,128)(2,1)S(1)}, u32[]{:S(2)}, u32[]{:S(2)}) collective-permute-start(bf16[4,512]{1,0:T(4,128)(2,1)S(1)} %add_convert_fusion.1.s0), channel_id=1, source_target_pairs={{0,2},{1,3},{2,0},{3,1},{4,6},{5,7},{6,4},{7,5},{8,10},{9,11},{10,... | collective-permute-start | bytes 12296 | tf_op jit(solution)/shard_map/ppermute | solution.py:54
  43.6 2.2 %shard_map.182.up = bf16[2048,704]{1,0:T(8,128)(2,1)S(1)} custom-call(bf16[2,704,2048]{2,1,0:T(8,128)(2,1)} %bitcast.26), custom_call_target="tpu_custom_call" | custom-call | flops 10000000000 | tf_op jit(solution)/shard_map/pallas_call | solution.py:76
  45.9 1.4 %shard_map.183 = (f32[4,1024]{1,0:T(4,128)S(1)}, f32[4,1024]{1,0:T(4,128)S(1)}, f32[4,256]{1,0:T(4,128)S(1)}) custom-call(bf16[4,512]{1,0:T(4,128)(2,1)S(1)} %add_convert_fusion.1.s0, bf16[4,512]{1,0:T(4,128)(2,1)S(1)} %collective-permute-done.15.s1, bf16[4,512]{1,0:T(4,128)(2,1)S(1)} %collective-permute-done.16.s2, ...), custom_call_target="tpu_custom_call" | custom-call | flops 10000000000 | tf_op jit(solution)/shard_map/pallas_call | solution.py:76
  47.7 0.8 %collective-permute-done.18 = f32[4,1024]{1,0:T(4,128)S(1)} collective-permute-done((f32[4,1024]{1,0:T(4,128)S(1)}, f32[4,1024]{1,0:T(4,128)S(1)}, u32[]{:S(2)}, u32[]{:S(2)}) %collective-permute-start.18) | collective-permute-done | bytes 16416 | tf_op jit(solution)/shard_map/ppermute | solution.py:44
  48.6 1.9 %collective-permute-start.19 = (bf16[4,512]{1,0:T(4,128)(2,1)S(1)}, bf16[4,512]{1,0:T(4,128)(2,1)S(1)}, u32[]{:S(2)}, u32[]{:S(2)}) collective-permute-start(bf16[4,512]{1,0:T(4,128)(2,1)S(1)} %slice.21), channel_id=1, source_target_pairs={{0,4},{1,7},{2,6},{3,5},{4,0},{5,3},{6,2},{7,1},{8,12},{9,15},{10,... | collective-permute-start | bytes 12296 | tf_op jit(solution)/shard_map/ppermute | solution.py:49
  50.4 0.9 %collective-permute-start.20 = (bf16[4,256]{1,0:T(4,128)(2,1)S(1)}, bf16[4,256]{1,0:T(4,128)(2,1)S(1)}, u32[]{:S(2)}, u32[]{:S(2)}) collective-permute-start(bf16[4,256]{1,0:T(4,128)(2,1)S(1)} %slice.23), channel_id=1, source_target_pairs={{0,2},{1,3},{2,0},{3,1},{4,6},{5,7},{6,4},{7,5},{8,10},{9,11},{10,... | collective-permute-start | bytes 6152 | tf_op jit(solution)/shard_map/ppermute | solution.py:54
  51.3 1.9 %collective-permute-done.19 = bf16[4,512]{1,0:T(4,128)(2,1)S(1)} collective-permute-done((bf16[4,512]{1,0:T(4,128)(2,1)S(1)}, bf16[4,512]{1,0:T(4,128)(2,1)S(1)}, u32[]{:S(2)}, u32[]{:S(2)}) %collective-permute-start.19) | collective-permute-done | bytes 4128 | tf_op jit(solution)/shard_map/ppermute | solution.py:49
  53.3 0.8 %collective-permute-done.20 = bf16[4,256]{1,0:T(4,128)(2,1)S(1)} collective-permute-done((bf16[4,256]{1,0:T(4,128)(2,1)S(1)}, bf16[4,256]{1,0:T(4,128)(2,1)S(1)}, u32[]{:S(2)}, u32[]{:S(2)}) %collective-permute-start.20) | collective-permute-done | bytes 2080 | tf_op jit(solution)/shard_map/ppermute | solution.py:54
  (80 shorter events, 6.2 us)
Async XLA Ops:
  0.0 6.2 %copy-start = (bf16[2,2048,704]{1,2,0:T(8,128)(2,1)S(1)}, bf16[2,2048,704]{1,2,0:T(8,128)(2,1)}, u32[]{:S(2)}) copy-start(bf16[2,2048,704]{1,2,0:T(8,128)(2,1)} %param.20) | copy-start | bytes 17301508
  0.0 8.8 %slice-start = ((s8[5767168]{0:T(1024)(128)(4,1)}), s8[4194304]{0:T(1024)(128)(4,1)S(1)}, s32[]{:S(2)}) async-start(s8[5767168]{0:T(1024)(128)(4,1)} %bitcast.27), calls=%async_computation | async-start | bytes 8388608
  0.9 7.9 %slice-start.1 = ((s8[5767168]{0:T(1024)(128)(4,1)}), s8[1572864]{0:T(1024)(128)(4,1)S(1)}, s32[]{:S(2)}) async-start(s8[5767168]{0:T(1024)(128)(4,1)} %bitcast.27), calls=%async_computation.1 | async-start | bytes 3145728
  0.9 1.4 %collective-permute-start = (bf16[8,256]{1,0:T(8,128)(2,1)S(1)}, bf16[8,256]{1,0:T(8,128)(2,1)S(1)}, u32[]{:S(2)}, u32[]{:S(2)}) collective-permute-start(bf16[8,256]{1,0:T(8,128)(2,1)S(1)} %shard_map.172), channel_id=1, source_target_pairs={{0,1},{1,0},{2,3},{3,2},{4,5},{5,4},{6,7},{7,6},{8,9},{9,8},{10,11... | collective-permute-start | bytes 12296 | tf_op jit(solution)/shard_map/ppermute | solution.py:44
  2.3 6.5 %collective-permute-start.2 = (bf16[8,512]{1,0:T(8,128)(2,1)S(1)}, bf16[8,512]{1,0:T(8,128)(2,1)S(1)}, u32[]{:S(2)}, u32[]{:S(2)}) collective-permute-start(bf16[8,512]{1,0:T(8,128)(2,1)S(1)} %pad_maximum_fusion.c0), channel_id=1, source_target_pairs={{0,4},{1,7},{2,6},{3,5},{4,0},{5,3},{6,2},{7,1},{8,12},{9,15},{10,... | collective-permute-start | bytes 24584 | tf_op jit(solution)/shard_map/ppermute | solution.py:49
  6.2 4.6 %slice-start.2 = ((s8[5767168]{0:T(1024)(128)(4,1)}), s8[4194304]{0:T(1024)(128)(4,1)S(1)}, s32[]{:S(2)}) async-start(s8[5767168]{0:T(1024)(128)(4,1)} %bitcast.30), calls=%async_computation.2 | async-start | bytes 8388608
  7.1 3.7 %collective-permute-start.1 = (bf16[8,512]{1,0:T(8,128)(2,1)S(1)}, bf16[8,512]{1,0:T(8,128)(2,1)S(1)}, u32[]{:S(2)}, u32[]{:S(2)}) collective-permute-start(bf16[8,512]{1,0:T(8,128)(2,1)S(1)} %pad_maximum_fusion.c0), channel_id=1, source_target_pairs={{0,2},{1,3},{2,0},{3,1},{4,6},{5,7},{6,4},{7,5},{8,10},{9,11},{10,... | collective-permute-start | bytes 24584 | tf_op jit(solution)/shard_map/ppermute | solution.py:54
  8.8 2.1 %collective-permute-start.3 = (bf16[8,512]{1,0:T(8,128)(2,1)S(1)}, bf16[8,512]{1,0:T(8,128)(2,1)S(1)}, u32[]{:S(2)}, u32[]{:S(2)}) collective-permute-start(bf16[8,512]{1,0:T(8,128)(2,1)S(1)} %collective-permute-done.2.c2), channel_id=1, source_target_pairs={{0,1},{1,0},{2,3},{3,2},{4,5},{5,4},{6,7},{7,6},{8,9},{9,8},{10,11... | collective-permute-start | bytes 24584 | tf_op jit(solution)/shard_map/ppermute | solution.py:44
  9.7 8.5 %copy-start.1 = (bf16[2048,16,32]{0,2,1:T(8,128)(2,1)S(1)}, bf16[2048,16,32]{0,2,1:T(8,128)(2,1)}, u32[]{:S(2)}) copy-start(bf16[2048,16,32]{0,2,1:T(8,128)(2,1)} %param.23) | copy-start | bytes 6291460
  9.7 8.5 %copy-start.2 = (bf16[2048,16,32]{0,2,1:T(8,128)(2,1)S(1)}, bf16[2048,16,32]{0,2,1:T(8,128)(2,1)}, u32[]{:S(2)}) copy-start(bf16[2048,16,32]{0,2,1:T(8,128)(2,1)} %param.24) | copy-start | bytes 6291460
  12.2 1.2 %collective-permute-start.4 = (f32[4,2048]{1,0:T(4,128)S(1)}, f32[4,2048]{1,0:T(4,128)S(1)}, u32[]{:S(2)}, u32[]{:S(2)}) collective-permute-start(f32[4,2048]{1,0:T(4,128)S(1)} %get-tuple-element.19), channel_id=1, source_target_pairs={{0,1},{1,0},{2,3},{3,2},{4,5},{5,4},{6,7},{7,6},{8,9},{9,8},{10,11... | collective-permute-start | bytes 98312 | tf_op jit(solution)/shard_map/ppermute | solution.py:44
  13.4 4.7 %collective-permute-start.6 = (bf16[4,2048]{1,0:T(4,128)(2,1)S(1)}, bf16[4,2048]{1,0:T(4,128)(2,1)S(1)}, u32[]{:S(2)}, u32[]{:S(2)}) collective-permute-start(bf16[4,2048]{1,0:T(4,128)(2,1)S(1)} %add_convert_fusion.s0), channel_id=1, source_target_pairs={{0,4},{1,7},{2,6},{3,5},{4,0},{5,3},{6,2},{7,1},{8,12},{9,15},{10,... | collective-permute-start | bytes 49160 | tf_op jit(solution)/shard_map/ppermute | solution.py:49
  14.6 5.7 %collective-permute-start.5 = (bf16[4,2048]{1,0:T(4,128)(2,1)S(1)}, bf16[4,2048]{1,0:T(4,128)(2,1)S(1)}, u32[]{:S(2)}, u32[]{:S(2)}) collective-permute-start(bf16[4,2048]{1,0:T(4,128)(2,1)S(1)} %add_convert_fusion.s0), channel_id=1, source_target_pairs={{0,2},{1,3},{2,0},{3,1},{4,6},{5,7},{6,4},{7,5},{8,10},{9,11},{10,... | collective-permute-start | bytes 49160 | tf_op jit(solution)/shard_map/ppermute | solution.py:54
  18.2 2.2 %collective-permute-start.7 = (bf16[4,2048]{1,0:T(4,128)(2,1)S(1)}, bf16[4,2048]{1,0:T(4,128)(2,1)S(1)}, u32[]{:S(2)}, u32[]{:S(2)}) collective-permute-start(bf16[4,2048]{1,0:T(4,128)(2,1)S(1)} %collective-permute-done.6.s2), channel_id=1, source_target_pairs={{0,1},{1,0},{2,3},{3,2},{4,5},{5,4},{6,7},{7,6},{8,9},{9,8},{10,11... | collective-permute-start | bytes 49160 | tf_op jit(solution)/shard_map/ppermute | solution.py:44
  20.3 5.4 %copy-start.4 = (f32[1,64,32,128]{3,2,1,0:T(8,128)S(1)}, f32[1,64,32,128]{3,2,1,0:T(8,128)}, u32[]{:S(2)}) copy-start(f32[1,64,32,128]{3,2,1,0:T(8,128)} %param.34) | copy-start | bytes 3145732
  21.3 5.7 %collective-permute-start.10 = (f32[1,3200]{1,0:T(1,128)S(1)}, f32[1,3200]{1,0:T(1,128)S(1)}, u32[]{:S(2)}, u32[]{:S(2)}) collective-permute-start(f32[1,3200]{1,0:T(1,128)S(1)} %get-tuple-element.26), channel_id=1, source_target_pairs={{0,6},{2,4},{4,2},{6,0},{1,7},{3,5},{5,3},{7,1},{8,14},{10,12},{12... | collective-permute-start | bytes 38408 | tf_op jit(solution)/shard_map/ppermute | solution.py:35
  23.7 3.7 %collective-permute-start.8 = (f32[1,3200]{1,0:T(1,128)S(1)}, f32[1,3200]{1,0:T(1,128)S(1)}, u32[]{:S(2)}, u32[]{:S(2)}) collective-permute-start(f32[1,3200]{1,0:T(1,128)S(1)} %get-tuple-element.24), channel_id=1, source_target_pairs={{0,2},{2,0},{4,6},{6,4},{1,3},{3,1},{5,7},{7,5},{8,10},{10,8},{12,... | collective-permute-start | bytes 38408 | tf_op jit(solution)/shard_map/ppermute | solution.py:35
  23.7 4.6 %collective-permute-start.9 = (f32[1,3200]{1,0:T(1,128)S(1)}, f32[1,3200]{1,0:T(1,128)S(1)}, u32[]{:S(2)}, u32[]{:S(2)}) collective-permute-start(f32[1,3200]{1,0:T(1,128)S(1)} %get-tuple-element.25), channel_id=1, source_target_pairs={{0,4},{2,6},{4,0},{6,2},{1,5},{3,7},{5,1},{7,3},{8,12},{10,14},{12... | collective-permute-start | bytes 38408 | tf_op jit(solution)/shard_map/ppermute | solution.py:35
  28.3 8.9 %copy-start.3 = (bf16[64,32,512]{2,1,0:T(8,128)(2,1)S(1)}, bf16[64,32,512]{2,1,0:T(8,128)(2,1)}, u32[]{:S(2)}) copy-start(bf16[64,32,512]{2,1,0:T(8,128)(2,1)} %param.35) | copy-start | bytes 6291460
  28.9 4.5 %collective-permute-start.11 = (f32[1,2048]{1,0:T(1,128)S(1)}, f32[1,2048]{1,0:T(1,128)S(1)}, u32[]{:S(2)}, u32[]{:S(2)}) collective-permute-start(f32[1,2048]{1,0:T(1,128)S(1)} %shard_map.179.m0), channel_id=1, source_target_pairs={{0,2},{2,0},{4,6},{6,4},{1,3},{3,1},{5,7},{7,5},{8,10},{10,8},{12,... | collective-permute-start | bytes 24584 | tf_op jit(solution)/shard_map/ppermute | solution.py:35
  31.0 4.5 %collective-permute-start.12 = (f32[1,2048]{1,0:T(1,128)S(1)}, f32[1,2048]{1,0:T(1,128)S(1)}, u32[]{:S(2)}, u32[]{:S(2)}) collective-permute-start(f32[1,2048]{1,0:T(1,128)S(1)} %shard_map.179.m0), channel_id=1, source_target_pairs={{0,4},{2,6},{4,0},{6,2},{1,5},{3,7},{5,1},{7,3},{8,12},{10,14},{12... | collective-permute-start | bytes 24584 | tf_op jit(solution)/shard_map/ppermute | solution.py:35
  31.7 5.4 %collective-permute-start.13 = (f32[1,2048]{1,0:T(1,128)S(1)}, f32[1,2048]{1,0:T(1,128)S(1)}, u32[]{:S(2)}, u32[]{:S(2)}) collective-permute-start(f32[1,2048]{1,0:T(1,128)S(1)} %shard_map.179.m0), channel_id=1, source_target_pairs={{0,6},{2,4},{4,2},{6,0},{1,7},{3,5},{5,3},{7,1},{8,14},{10,12},{12... | collective-permute-start | bytes 24584 | tf_op jit(solution)/shard_map/ppermute | solution.py:35
  37.6 1.2 %collective-permute-start.14 = (f32[4,512]{1,0:T(4,128)S(1)}, f32[4,512]{1,0:T(4,128)S(1)}, u32[]{:S(2)}, u32[]{:S(2)}) collective-permute-start(f32[4,512]{1,0:T(4,128)S(1)} %shard_map.180), channel_id=1, source_target_pairs={{0,1},{1,0},{2,3},{3,2},{4,5},{5,4},{6,7},{7,6},{8,9},{9,8},{10,11... | collective-permute-start | bytes 24584 | tf_op jit(solution)/shard_map/ppermute | solution.py:44
  38.8 4.8 %collective-permute-start.16 = (bf16[4,512]{1,0:T(4,128)(2,1)S(1)}, bf16[4,512]{1,0:T(4,128)(2,1)S(1)}, u32[]{:S(2)}, u32[]{:S(2)}) collective-permute-start(bf16[4,512]{1,0:T(4,128)(2,1)S(1)} %add_convert_fusion.1.s0), channel_id=1, source_target_pairs={{0,4},{1,7},{2,6},{3,5},{4,0},{5,3},{6,2},{7,1},{8,12},{9,15},{10,... | collective-permute-start | bytes 12296 | tf_op jit(solution)/shard_map/ppermute | solution.py:49
  39.2 6.6 %slice-start.4 = ((s8[5767168]{0:T(1024)(128)(4,1)}), s8[4194304]{0:T(1024)(128)(4,1)S(1)}, s32[]{:S(2)}) async-start(s8[5767168]{0:T(1024)(128)(4,1)} %bitcast.32), calls=%async_computation.4 | async-start | bytes 8388608
  41.6 4.2 %slice-start.5 = ((s8[5767168]{0:T(1024)(128)(4,1)}), s8[1572864]{0:T(1024)(128)(4,1)S(1)}, s32[]{:S(2)}) async-start(s8[5767168]{0:T(1024)(128)(4,1)} %bitcast.32), calls=%async_computation.5 | async-start | bytes 3145728
  41.6 4.2 %collective-permute-start.15 = (bf16[4,512]{1,0:T(4,128)(2,1)S(1)}, bf16[4,512]{1,0:T(4,128)(2,1)S(1)}, u32[]{:S(2)}, u32[]{:S(2)}) collective-permute-start(bf16[4,512]{1,0:T(4,128)(2,1)S(1)} %add_convert_fusion.1.s0), channel_id=1, source_target_pairs={{0,2},{1,3},{2,0},{3,1},{4,6},{5,7},{6,4},{7,5},{8,10},{9,11},{10,... | collective-permute-start | bytes 12296 | tf_op jit(solution)/shard_map/ppermute | solution.py:54
  43.5 2.3 %collective-permute-start.17 = (bf16[4,512]{1,0:T(4,128)(2,1)S(1)}, bf16[4,512]{1,0:T(4,128)(2,1)S(1)}, u32[]{:S(2)}, u32[]{:S(2)}) collective-permute-start(bf16[4,512]{1,0:T(4,128)(2,1)S(1)} %collective-permute-done.16.s2), channel_id=1, source_target_pairs={{0,1},{1,0},{2,3},{3,2},{4,5},{5,4},{6,7},{7,6},{8,9},{9,8},{10,11... | collective-permute-start | bytes 12296 | tf_op jit(solution)/shard_map/ppermute | solution.py:44
  47.2 1.4 %collective-permute-start.18 = (f32[4,1024]{1,0:T(4,128)S(1)}, f32[4,1024]{1,0:T(4,128)S(1)}, u32[]{:S(2)}, u32[]{:S(2)}) collective-permute-start(f32[4,1024]{1,0:T(4,128)S(1)} %get-tuple-element.32), channel_id=1, source_target_pairs={{0,1},{1,0},{2,3},{3,2},{4,5},{5,4},{6,7},{7,6},{8,9},{9,8},{10,11... | collective-permute-start | bytes 49160 | tf_op jit(solution)/shard_map/ppermute | solution.py:44
  48.6 4.6 %collective-permute-start.19 = (bf16[4,512]{1,0:T(4,128)(2,1)S(1)}, bf16[4,512]{1,0:T(4,128)(2,1)S(1)}, u32[]{:S(2)}, u32[]{:S(2)}) collective-permute-start(bf16[4,512]{1,0:T(4,128)(2,1)S(1)} %slice.21), channel_id=1, source_target_pairs={{0,4},{1,7},{2,6},{3,5},{4,0},{5,3},{6,2},{7,1},{8,12},{9,15},{10,... | collective-permute-start | bytes 12296 | tf_op jit(solution)/shard_map/ppermute | solution.py:49
  50.4 3.6 %collective-permute-start.20 = (bf16[4,256]{1,0:T(4,128)(2,1)S(1)}, bf16[4,256]{1,0:T(4,128)(2,1)S(1)}, u32[]{:S(2)}, u32[]{:S(2)}) collective-permute-start(bf16[4,256]{1,0:T(4,128)(2,1)S(1)} %slice.23), channel_id=1, source_target_pairs={{0,2},{1,3},{2,0},{3,1},{4,6},{5,7},{6,4},{7,5},{8,10},{9,11},{10,... | collective-permute-start | bytes 6152 | tf_op jit(solution)/shard_map/ppermute | solution.py:54
  53.2 1.2 %collective-permute-start.21 = (bf16[4,256]{1,0:T(4,128)(2,1)S(1)}, bf16[4,256]{1,0:T(4,128)(2,1)S(1)}, u32[]{:S(2)}, u32[]{:S(2)}) collective-permute-start(bf16[4,256]{1,0:T(4,128)(2,1)S(1)} %slice.24), channel_id=1, source_target_pairs={{0,1},{1,0},{2,3},{3,2},{4,5},{5,4},{6,7},{7,6},{8,9},{9,8},{10,11... | collective-permute-start | bytes 6152 | tf_op jit(solution)/shard_map/ppermute | solution.py:44
  (10 other events, 20.6 us)
